TPU v7x, 512 devices: a whole 4x4x16 slice. The times are simulated.
512 devices in a mesh: fs: 16 (over y, x), tp: 32 (over z, core).
Axes of the slice: x: 4, y: 4, z: 16, core: 2. Of those that a mesh axis runs over, the one named last changes fastest.
Arguments:
- tokens: bfloat16 [16384, 2048], P(('fs', 'tp')), may hold values from -6 to 6
- norm_gain: float32 [2048], P('fs'), may hold values from 0.1 to 1.9
- gate_master: float32 [2048, 8192], P('fs', 'tp'), may hold values from -0.125 to 0.125
- up_master: float32 [2048, 8192], P('fs', 'tp'), may hold values from -0.125 to 0.125
- down_master: float32 [2048, 8192], P('fs', 'tp'), may hold values from -0.125 to 0.125
Outputs:
- mixed: bfloat16 [16384, 2048], P(('fs', 'tp'))
- gate_ready: bfloat16 [2048, 8192], P(None, 'tp')
- up_ready: bfloat16 [2048, 8192], P(None, 'tp')
- down_ready: bfloat16 [2048, 8192], P(None, 'tp')
All inputs are finite; a program needn't handle non-finite values.
Results may differ from a plain program's by a relative error of at most 0.0095.
Values may be sent and summed in bfloat16 or wider, within the bound.
No kernel may reach another device: no remote copies, remote signals or barrier semaphores. Data moves between devices by JAX's collectives and lax.ppermute only.
A program may use at most 64 MiB of HBM per device.

v0:
```python
import jax
import jax.numpy as jnp
from jax import lax
from jax.sharding import Mesh
from jax.sharding import PartitionSpec as P

TP = ("tp_0", "tp_1")
FS_TP = ("fs", "tp_0", "tp_1")


def in_one_piece(arrays, axis, dim, along):
    both = jnp.concatenate(arrays, axis=along)
    whole, at, gathered = (lax.all_gather(both, axis, axis=dim, tiled=True), 0, [])
    for a in arrays:
        gathered.append(lax.slice_in_dim(whole, at, at + a.shape[along], axis=along))
        at += a.shape[along]
    return tuple(gathered)


def laid_out(parts, dim):
    dims = list(parts.shape[1:])
    dims[dim] *= parts.shape[0]
    return jnp.moveaxis(parts, 0, dim).reshape(dims)


def copy_for_each(array, axis):
    copies = jnp.broadcast_to(array, (lax.axis_size(axis), *array.shape))
    return lax.all_to_all(copies, axis, split_axis=0, concat_axis=0, tiled=True)


def collect(array, axis, dim):
    return laid_out(copy_for_each(array, axis), dim)


def own_block(parts, axes, sequence):
    inside = parts.shape[1:]
    parts = parts.reshape(*(lax.axis_size(a) for a in axes), *inside)
    parts = jnp.moveaxis(parts, sequence, range(len(axes))).reshape(-1, *inside)
    for k in sequence:
        parts = lax.psum_scatter(parts, axes[k], scatter_dimension=0, tiled=True)
    return parts[0]


def split_up(array, dim, length):
    dims = array.shape
    parts = array.reshape(*dims[:dim], length, dims[dim] // length, *dims[dim + 1 :])
    return jnp.moveaxis(parts, dim, 0)


def sum_by_axis(array, axes, sequence, dim):
    length = lax.axis_size(axes)
    return own_block(split_up(array, dim, length), axes, sequence)


def expand_rows(rows, gate_ready, up_ready):
    rows_wide = rows.astype(jnp.float32)
    row_scale = lax.rsqrt(jnp.mean(rows_wide * rows_wide, axis=1, keepdims=True) + 1e-06)
    gate_proj = row_scale * jnp.dot(rows, gate_ready, preferred_element_type=jnp.float32)
    up_proj = row_scale * jnp.dot(rows, up_ready, preferred_element_type=jnp.float32)
    return (jax.nn.silu(gate_proj) * up_proj).astype(jnp.bfloat16)


def body(tokens, norm_gain, gate_master, up_master, down_master):
    gate_local = (norm_gain[:, None] * gate_master).astype(jnp.bfloat16)
    up_local = (norm_gain[:, None] * up_master).astype(jnp.bfloat16)
    down_local = down_master.astype(jnp.bfloat16)
    gate_ready, up_ready = in_one_piece((gate_local, up_local), "fs", 0, 1)
    gathered = lax.all_gather(tokens, TP, axis=0, tiled=True)
    hidden = expand_rows(gathered, gate_ready, up_ready)
    down_ready = collect(down_local, "fs", 0)
    partial_value = lax.dot_general(
        hidden, down_ready, (((1,), (1,)), ((), ())), preferred_element_type=jnp.float32
    )
    summed = sum_by_axis(partial_value.astype(jnp.bfloat16), TP, (1, 0), 0).astype(jnp.float32)
    mixed = (tokens.astype(jnp.float32) + 0.5 * summed).astype(jnp.bfloat16)
    return (mixed, gate_ready, up_ready, down_ready)


def solution(mesh):
    split = Mesh(mesh.devices.reshape(mesh.shape["fs"], 16, 2), ("fs", "tp_0", "tp_1"))
    placed = (P(FS_TP, None), P("fs"), P("fs", TP), P("fs", TP), P("fs", TP))
    return jax.shard_map(
        body,
        mesh=split,
        in_specs=placed,
        out_specs=(P(FS_TP, None), P(None, TP), P(None, TP), P(None, TP)),
        check_vma=False,
    )
```

profile of v0, /device:TPU:6, one launch (start us, length us, event | category | flops | bytes accessed | tf_op | source)
XLA Modules:
  0.0 275.8 jit_solution(10192223352747149037)
XLA Ops:
  7.2 0.0 all-gather.5.cloned.1.call-start
  7.2 1.1 multiply_convert_fusion.1
  8.3 0.7 pad_maximum_fusion
  9.0 0.0 all-gather.5.cloned.1.call-update
  9.0 0.0 all-gather.3.cloned.1.call-start
  9.0 0.7 all-gather.3.cloned.1.call-update
  9.7 0.9 convert_element_type.33
  10.6 1.1 broadcast_in_dim.2
  11.7 9.3 %all-to-all-start = ((bf16[16,128,256]{2,1,0:T(8,128)(2,1)}), bf16[16,128,256]{2,1,0:T(8,128)(2,1)S(1)}, u32[]{:S(2)}, u32[]{:S(2)}) async-start(bf16[16,128,256]{2,1,0:T(8,128)(2,1)} %broadcast_in_dim.2), calls=%async_computation | async-start | bytes 2097152 | tf_op jit(solution)/shard_map/all_to_all | solution.py:28
  21.0 0.0 reduce-scatter.3.cloned.1.call-start
  21.0 54.8 %all-gather.5.cloned.1.call-done = bf16[2048,512]{1,0:T(8,128)(2,1)} async-done(((bf16[128,512]{1,0:T(8,128)(2,1)}), bf16[2048,512]{1,0:T(8,128)(2,1)}) %all-gather.5.cloned.1.call-update) | async-done | bytes 2097168 | tf_op jit(solution)/shard_map/all_gather | solution.py:13
  75.9 1.7 fusion.13
  77.6 0.0 copy-start.1
  77.6 0.0 copy-start.2
  77.6 73.6 %all-gather.3.cloned.1.call-done = bf16[1024,2048]{1,0:T(8,128)(2,1)} async-done(((bf16[32,2048]{1,0:T(8,128)(2,1)}), bf16[1024,2048]{1,0:T(8,128)(2,1)}) %all-gather.3.cloned.1.call-update) | async-done | bytes 4194320 | tf_op jit(solution)/shard_map/all_gather | solution.py:68
  151.2 0.0 copy-start
  151.2 3.2 %multiply_reduce_fusion = f32[1024]{0:T(1024)S(1)} fusion(bf16[1024,2048]{1,0:T(8,128)(2,1)} %all-gather.3.cloned.1.call-done), kind=kLoop, calls=%fused_computation | loop fusion | flops 6290432 | bytes 4198400 | tf_op jit(solution)/shard_map/reduce_sum | solution.py:57
  154.4 0.2 copy-done
  154.6 2.4 fusion.1
  157.0 0.0 copy-done.1
  157.0 0.0 all-to-all-done
  157.0 0.0 copy-done.2
  157.0 7.0 %convolution_convert_fusion = bf16[1024,2048]{1,0:T(8,128)(2,1)} fusion(bf16[2048,256]{1,0:T(8,128)(2,1)S(1)} %bitcast.26, bf16[2048,256]{1,0:T(8,128)(2,1)S(1)} %get-tuple-element.14, bf16[1024,2048]{1,0:T(8,128)(2,1)} %all-gather.3.cloned.1.call-done, f32[1024,256]{0,1:T(8,128)} %fusion.1, f32[1024]{0:T(1024)S(1)} %add_rsqrt_fusion), kind=kOutput, calls=%fused_computation.1 | convolution fusion | flops 2151415808 | bytes 11538432 | tf_op jit(solution)/shard_map/dot_general | solution.py:71
  164.0 4.7 %copy.9 = bf16[2,16,32,2048]{3,2,1,0:T(8,128)(2,1)} copy(bf16[2,16,32,2048]{3,2,0,1:T(8,128)(2,1)} %bitcast.25) | data formatting | bytes 8388608 | tf_op jit(solution)/shard_map/transpose | solution.py:38
  168.8 0.0 copy-start.3
  168.8 0.0 reduce-scatter.3.cloned.1.call-update
  168.8 0.0 reduce-scatter.5.cloned.1.call-start
  168.9 19.5 %reduce-scatter.3.cloned.1.call-done = bf16[16,32,2048]{2,1,0:T(8,128)(2,1)} async-done(((bf16[32,32,2048]{2,1,0:T(8,128)(2,1)}), bf16[16,32,2048]{2,1,0:T(8,128)(2,1)}) %reduce-scatter.3.cloned.1.call-update) | async-done | bytes 2097168 | tf_op jit(solution)/shard_map/reduce_scatter | solution.py:40
  188.4 0.0 reduce-scatter.5.cloned.1.call-update
  188.4 78.3 %reduce-scatter.5.cloned.1.call-done = bf16[1,32,2048]{2,1,0:T(8,128)(2,1)} async-done(((bf16[16,32,2048]{2,1,0:T(8,128)(2,1)}), bf16[1,32,2048]{2,1,0:T(8,128)(2,1)}) %reduce-scatter.5.cloned.1.call-update) | async-done | bytes 131088 | tf_op jit(solution)/shard_map/reduce_scatter | solution.py:40
  266.7 0.0 copy-done.3
  266.7 1.6 fusion.11
  268.3 1.0 copy.11
  (1 shorter events, 0.0 us)
Async XLA Ops:
  7.2 68.7 %all-gather.5.cloned.1.call-start = ((), (), s32[]{:S(2)}) async-start(), calls=%async_computation.4 | async-start | bytes 2228224 | tf_op jit(solution)/shard_map/all_gather | solution.py:13
  9.0 142.2 %all-gather.3.cloned.1.call-start = ((), (), s32[]{:S(2)}) async-start(), calls=%async_computation.3 | async-start | bytes 4325376 | tf_op jit(solution)/shard_map/all_gather | solution.py:68
  11.7 145.3 %all-to-all-start = ((bf16[16,128,256]{2,1,0:T(8,128)(2,1)}), bf16[16,128,256]{2,1,0:T(8,128)(2,1)S(1)}, u32[]{:S(2)}, u32[]{:S(2)}) async-start(bf16[16,128,256]{2,1,0:T(8,128)(2,1)} %broadcast_in_dim.2), calls=%async_computation | async-start | bytes 2097152 | tf_op jit(solution)/shard_map/all_to_all | solution.py:28
  21.0 167.4 %reduce-scatter.3.cloned.1.call-start = ((), (), s32[]{:S(2)}) async-start(), calls=%async_computation.5 | async-start | bytes 6291456 | tf_op jit(solution)/shard_map/reduce_scatter | solution.py:40
  77.6 79.4 %copy-start.1 = (bf16[2048,256]{1,0:T(8,128)(2,1)}, bf16[2048,256]{1,0:T(8,128)(2,1)S(1)}, u32[]{:S(2)}) copy-start(bf16[2048,256]{1,0:T(8,128)(2,1)S(1)} %get-tuple-element.13) | copy-start | bytes 3145732
  77.6 79.4 %copy-start.2 = (bf16[2048,256]{1,0:T(8,128)(2,1)}, bf16[2048,256]{1,0:T(8,128)(2,1)S(1)}, u32[]{:S(2)}) copy-start(bf16[2048,256]{1,0:T(8,128)(2,1)S(1)} %get-tuple-element.14) | copy-start | bytes 3145732
  151.2 3.4 %copy-start = (bf16[1024,2048]{1,0:T(8,128)(2,1)S(1)}, bf16[1024,2048]{1,0:T(8,128)(2,1)}, u32[]{:S(2)}) copy-start(bf16[1024,2048]{1,0:T(8,128)(2,1)} %all-gather.3.cloned.1.call-done) | copy-start | bytes 12582916
  168.8 97.9 %copy-start.3 = (bf16[32,2048]{1,0:T(8,128)(2,1)S(1)}, bf16[32,2048]{1,0:T(8,128)(2,1)}, u32[]{:S(2)}) copy-start(bf16[32,2048]{1,0:T(8,128)(2,1)} %param.5) | copy-start | bytes 393220
  168.8 97.9 %reduce-scatter.5.cloned.1.call-start = ((), (), s32[]{:S(2)}) async-start(), calls=%async_computation.6 | async-start | bytes 2228224 | tf_op jit(solution)/shard_map/reduce_scatter | solution.py:40
Sparse Core Ops, SparseCore 0:
  11.6 64.2 all-gather.4
  78.0 73.1 all-gather.2
  168.9 19.3 reduce-scatter.2
  191.0 75.5 reduce-scatter.4
where the time goes:
time: 276 us
  waiting for transfers between devices  227 us (82%)
  between operations  13.8 us (5%)
  starting transfers between devices  9.44 us (3%)
  matrix products  9.4 us (3%)
  local copies, waits for them, and re-layouts  8.68 us (3%)
  other arithmetic  7.48 us (3%)
    reduce_scatter x2, waiting for transfers between devices, own_block(): parts = lax.psum_scatter(parts, axes[k], scatter_dimension=0, tiled=True)  97.8 us
    all_gather x1, waiting for transfers between devices, body(): gathered = lax.all_gather(tokens, TP, axis=0, tiled=True)  73.6 us
    all_gather x1, waiting for transfers between devices, in_one_piece(): lax.all_gather(both, axis, axis=dim, tiled=True)  54.8 us
    all_to_all x1, starting transfers between devices, copy_for_each(): return lax.all_to_all(copies, axis, split_axis=0, concat_axis=0, tiled=True)  9.28 us
    dot_general x1, matrix products, body(): lax.dot_general(hidden, down_ready, (((1,), (1,)), ((), ())), preferred_e...  7.04 us
  transfers between devices with their start and end apart: 5, of which 4 were waited for; matrix products, arithmetic and copies ran while one was open for 3% of the time, Pallas kernels for 0%

commit v1 on v0

v1 whole, which is shorter than its diff:
```python
import jax
import jax.numpy as jnp
from jax import lax
from jax.sharding import Mesh
from jax.sharding import PartitionSpec as P

TP = ("z", "c")
ROWS = ("fs", "z", "c")


def move(array, by):
    planes = lax.axis_size("z")
    return lax.ppermute(array, "z", [(i, (i + by) % planes) for i in range(planes)])


def partial_sums(rows, weights):
    wide = rows.astype(jnp.float32)
    row_scale = lax.rsqrt(jnp.mean(wide * wide, axis=1, keepdims=True) + 1e-06)
    total = None
    for gate, up, down in weights:
        gate_proj = row_scale * jnp.dot(rows, gate, preferred_element_type=jnp.float32)
        up_proj = row_scale * jnp.dot(rows, up, preferred_element_type=jnp.float32)
        hidden = (jax.nn.silu(gate_proj) * up_proj).astype(jnp.bfloat16)
        share = lax.dot_general(hidden, down, (((1,), (1,)), ((), ())), preferred_element_type=jnp.float32)
        total = share if total is None else total + share
    return total


def unpacked(packed):
    return tuple(packed[:, k].reshape(-1, packed.shape[-1]) for k in range(3))


def body(tokens, norm_gain, gate_master, up_master, down_master):
    rows = tokens.shape[0]
    gain = norm_gain[:, None]
    shard = jnp.stack([(gain * gate_master).astype(jnp.bfloat16), (gain * up_master).astype(jnp.bfloat16), down_master.astype(jnp.bfloat16)])
    copies = jnp.broadcast_to(shard, (lax.axis_size("fs"), *shard.shape))
    packed = lax.all_to_all(copies, "fs", split_axis=0, concat_axis=0, tiled=True)

    far = move(tokens, 8)
    above = move(tokens, -4)
    below = move(tokens, 4)
    next_a = move(jnp.concatenate([tokens, far]), -1)
    prev_a = move(jnp.concatenate([tokens, far]), 1)
    next_b = move(jnp.concatenate([above, below]), -1)
    prev_b = move(jnp.concatenate([above, below]), 1)
    next2 = move(jnp.concatenate([tokens, above]), -2)
    prev2 = move(jnp.concatenate([tokens, below]), 2)

    partner = lax.ppermute(packed, "c", [(0, 1), (1, 0)])
    own_weights = unpacked(packed)
    weights = (own_weights, unpacked(partner))

    own = partial_sums(jnp.concatenate([tokens, far, above, below]), weights)
    ones = partial_sums(jnp.concatenate([next_a, next_b, prev_a, prev_b]), weights).astype(jnp.bfloat16)
    to_next = move(ones[: 4 * rows], 1)
    to_prev = move(ones[4 * rows :], -1)
    twos = partial_sums(jnp.concatenate([next2, prev2]), weights).astype(jnp.bfloat16)
    to_next2 = move(twos[: 2 * rows], 2)
    to_prev2 = move(twos[2 * rows :], -2)

    def block(array, k):
        return array[k * rows : (k + 1) * rows].astype(jnp.float32)

    sum_far = block(own, 1) + block(to_next, 1) + block(to_prev, 1)
    back_far = move(sum_far.astype(jnp.bfloat16), 8)
    sum_above = block(own, 2) + block(to_next, 2) + block(to_prev, 2) + block(to_next2, 1)
    back_above = move(sum_above.astype(jnp.bfloat16), 4)
    sum_below = block(own, 3) + block(to_next, 3) + block(to_prev, 3) + block(to_prev2, 1)
    back_below = move(sum_below.astype(jnp.bfloat16), -4)
    here = block(own, 0) + block(to_next, 0) + block(to_prev, 0) + block(to_next2, 0) + block(to_prev2, 0)
    summed = here + back_far.astype(jnp.float32) + back_above.astype(jnp.float32) + back_below.astype(jnp.float32)
    mixed = (tokens.astype(jnp.float32) + 0.5 * summed).astype(jnp.bfloat16)
    return (mixed, *own_weights)


def solution(mesh):
    split = Mesh(mesh.devices.reshape(mesh.shape["fs"], 16, 2), ROWS)
    placed = (P(ROWS, None), P("fs"), P("fs", TP), P("fs", TP), P("fs", TP))
    return jax.shard_map(
        body,
        mesh=split,
        in_specs=placed,
        out_specs=(P(ROWS, None), P(None, TP), P(None, TP), P(None, TP)),
        check_vma=False,
    )
```

time: 276 us -> 192 us (0.70)
  the two profiles are of different devices: /device:TPU:6 before, /device:TPU:66 now
where the time goes in v1:
time: 192 us; the launch traced here: 191 us
  starting transfers between devices  85 us (44%)
  waiting for transfers between devices  65.5 us (34%)
  matrix products  23.3 us (12%)
  local copies, waits for them, and re-layouts  11 us (6%)
  other arithmetic  5.48 us (3%)
    ppermute x16, starting transfers between devices, move(): lax.ppermute(array, 'z', [(i, (i + by) % planes) for i in range(planes)])  75.5 us
    ppermute x16, waiting for transfers between devices, move(): lax.ppermute(array, 'z', [(i, (i + by) % planes) for i in range(planes)])  65.5 us
    dot_general x6, matrix products, partial_sums(): lax.dot_general(hidden, down, (((1,), (1,)), ((), ())), preferred_element...  19 us
    all_to_all x1, starting transfers between devices, body(): lax.all_to_all(copies, 'fs', split_axis=0, concat_axis=0, tiled=True)  7.61 us
    dot_general x6, matrix products, partial_sums(): up_proj = row_scale * jnp.dot(rows, up, preferred_element_type=jnp.float32)  4.37 us
    slice x2, local copies, waits for them, and re-layouts, unpacked(): return tuple((packed[:, k].reshape(-1, packed.shape[-1]) for k in range(3)))  4.37 us
  transfers between devices with their start and end apart: 18, of which 7 were waited for; matrix products, arithmetic and copies ran while one was open for 13% of the time, Pallas kernels for 0%

profile of v1, /device:TPU:66, one launch (start us, length us, event | category | flops | bytes accessed | tf_op | source)
XLA Modules:
  0.0 191.4 jit_solution(8323383739784795795)
XLA Ops:
  0.6 1.1 fusion.24
  1.8 2.1 %broadcast_in_dim.2 = bf16[16,3,128,256]{3,2,1,0:T(8,128)(2,1)} broadcast(bf16[3,128,256]{2,1,0:T(8,128)(2,1)S(1)} %pad_maximum_fusion.2), dimensions={1,2,3} | broadcast | bytes 3342336 | tf_op jit(solution)/shard_map/broadcast_in_dim | solution.py:37
  3.9 7.6 %all-to-all-start = ((bf16[16,3,128,256]{3,2,1,0:T(8,128)(2,1)}), bf16[16,3,128,256]{3,2,1,0:T(8,128)(2,1)}, u32[]{:S(2)}, u32[]{:S(2)}) async-start(bf16[16,3,128,256]{3,2,1,0:T(8,128)(2,1)} %broadcast_in_dim.2), calls=%async_computation | async-start | bytes 6291456 | tf_op jit(solution)/shard_map/all_to_all | solution.py:38
  11.5 10.9 %collective-permute-start.1 = (bf16[32,2048]{1,0:T(8,128)(2,1)S(1)}, bf16[32,2048]{1,0:T(8,128)(2,1)S(1)}, u32[]{:S(2)}, u32[]{:S(2)}) collective-permute-start(bf16[32,2048]{1,0:T(8,128)(2,1)S(1)} %copy-done.11), channel_id=1, source_target_pairs={{0,24},{2,26},{4,28},{6,30},{8,0},{10,2},{12,4},{14,6},{16,8},{18,... | collective-permute-start | bytes 393224 | tf_op jit(solution)/shard_map/ppermute | solution.py:13
  22.4 1.9 %collective-permute-start.2 = (bf16[32,2048]{1,0:T(8,128)(2,1)S(1)}, bf16[32,2048]{1,0:T(8,128)(2,1)S(1)}, u32[]{:S(2)}, u32[]{:S(2)}) collective-permute-start(bf16[32,2048]{1,0:T(8,128)(2,1)S(1)} %copy-done.11), channel_id=1, source_target_pairs={{0,8},{2,10},{4,12},{6,14},{8,16},{10,18},{12,20},{14,22},{16,24},... | collective-permute-start | bytes 393224 | tf_op jit(solution)/shard_map/ppermute | solution.py:13
  24.4 10.8 %collective-permute-start = (bf16[32,2048]{1,0:T(8,128)(2,1)S(1)}, bf16[32,2048]{1,0:T(8,128)(2,1)S(1)}, u32[]{:S(2)}, u32[]{:S(2)}) collective-permute-start(bf16[32,2048]{1,0:T(8,128)(2,1)S(1)} %copy-done.11), channel_id=1, source_target_pairs={{0,16},{2,18},{4,20},{6,22},{8,24},{10,26},{12,28},{14,30},{16,0},... | collective-permute-start | bytes 393224 | tf_op jit(solution)/shard_map/ppermute | solution.py:13
  35.2 14.9 %collective-permute-done = bf16[32,2048]{1,0:T(8,128)(2,1)S(1)} collective-permute-done((bf16[32,2048]{1,0:T(8,128)(2,1)S(1)}, bf16[32,2048]{1,0:T(8,128)(2,1)S(1)}, u32[]{:S(2)}, u32[]{:S(2)}) %collective-permute-start) | collective-permute-done | bytes 131104 | tf_op jit(solution)/shard_map/ppermute | solution.py:13
  50.2 1.9 %collective-permute-start.4 = (bf16[64,2048]{1,0:T(8,128)(2,1)S(1)}, bf16[64,2048]{1,0:T(8,128)(2,1)S(1)}, u32[]{:S(2)}, u32[]{:S(2)}) collective-permute-start(bf16[64,2048]{1,0:T(8,128)(2,1)S(1)} %get-tuple-element.21), channel_id=1, source_target_pairs={{0,30},{2,0},{4,2},{6,4},{8,6},{10,8},{12,10},{14,12},{16,14},{18,... | collective-permute-start | bytes 786440 | tf_op jit(solution)/shard_map/ppermute | solution.py:13
  52.1 3.9 %collective-permute-start.6 = (bf16[64,2048]{1,0:T(8,128)(2,1)S(1)}, bf16[64,2048]{1,0:T(8,128)(2,1)S(1)}, u32[]{:S(2)}, u32[]{:S(2)}) collective-permute-start(bf16[64,2048]{1,0:T(8,128)(2,1)S(1)} %get-tuple-element.21), channel_id=1, source_target_pairs={{0,2},{2,4},{4,6},{6,8},{8,10},{10,12},{12,14},{14,16},{16,18},{18... | collective-permute-start | bytes 786440 | tf_op jit(solution)/shard_map/ppermute | solution.py:13
  56.1 6.2 %collective-permute-start.5 = (bf16[64,2048]{1,0:T(8,128)(2,1)S(1)}, bf16[64,2048]{1,0:T(8,128)(2,1)S(1)}, u32[]{:S(2)}, u32[]{:S(2)}) collective-permute-start(bf16[64,2048]{1,0:T(8,128)(2,1)S(1)} %get-tuple-element.17), channel_id=1, source_target_pairs={{0,30},{2,0},{4,2},{6,4},{8,6},{10,8},{12,10},{14,12},{16,14},{18,... | collective-permute-start | bytes 786440 | tf_op jit(solution)/shard_map/ppermute | solution.py:13
  62.4 1.9 %collective-permute-start.7 = (bf16[64,2048]{1,0:T(8,128)(2,1)S(1)}, bf16[64,2048]{1,0:T(8,128)(2,1)S(1)}, u32[]{:S(2)}, u32[]{:S(2)}) collective-permute-start(bf16[64,2048]{1,0:T(8,128)(2,1)S(1)} %get-tuple-element.17), channel_id=1, source_target_pairs={{0,2},{2,4},{4,6},{6,8},{8,10},{10,12},{12,14},{14,16},{16,18},{18... | collective-permute-start | bytes 786440 | tf_op jit(solution)/shard_map/ppermute | solution.py:13
  64.3 5.4 %collective-permute-start.10 = (bf16[64,2048]{1,0:T(8,128)(2,1)S(1)}, bf16[64,2048]{1,0:T(8,128)(2,1)S(1)}, u32[]{:S(2)}, u32[]{:S(2)}) collective-permute-start(bf16[64,2048]{1,0:T(8,128)(2,1)S(1)} %get-tuple-element.26), channel_id=1, source_target_pairs={{0,28},{2,30},{4,0},{6,2},{8,4},{10,6},{12,8},{14,10},{16,12},{18,... | collective-permute-start | bytes 786440 | tf_op jit(solution)/shard_map/ppermute | solution.py:13
  69.7 0.2 multiply_reduce_fusion.2
  69.9 10.8 %collective-permute-done.10 = bf16[64,2048]{1,0:T(8,128)(2,1)S(1)} collective-permute-done((bf16[64,2048]{1,0:T(8,128)(2,1)S(1)}, bf16[64,2048]{1,0:T(8,128)(2,1)S(1)}, u32[]{:S(2)}, u32[]{:S(2)}) %collective-permute-start.10) | collective-permute-done | bytes 262176 | tf_op jit(solution)/shard_map/ppermute | solution.py:13
  80.7 2.4 %collective-permute-start.11 = (bf16[64,2048]{1,0:T(8,128)(2,1)S(1)}, bf16[64,2048]{1,0:T(8,128)(2,1)S(1)}, u32[]{:S(2)}, u32[]{:S(2)}) collective-permute-start(bf16[64,2048]{1,0:T(8,128)(2,1)S(1)} %get-tuple-element.25), channel_id=1, source_target_pairs={{0,4},{2,6},{4,8},{6,10},{8,12},{10,14},{12,16},{14,18},{16,20},{1... | collective-permute-start | bytes 786440 | tf_op jit(solution)/shard_map/ppermute | solution.py:13
  83.2 12.6 %collective-permute-done.11 = bf16[64,2048]{1,0:T(8,128)(2,1)S(1)} collective-permute-done((bf16[64,2048]{1,0:T(8,128)(2,1)S(1)}, bf16[64,2048]{1,0:T(8,128)(2,1)S(1)}, u32[]{:S(2)}, u32[]{:S(2)}) %collective-permute-start.11) | collective-permute-done | bytes 262176 | tf_op jit(solution)/shard_map/ppermute | solution.py:13
  95.9 1.9 %collective-permute-start.3 = (bf16[16,3,128,256]{3,2,1,0:T(8,128)(2,1)}, bf16[16,3,128,256]{3,2,1,0:T(8,128)(2,1)}, u32[]{:S(2)}, u32[]{:S(2)}) collective-permute-start(bf16[16,3,128,256]{3,2,1,0:T(8,128)(2,1)} %all-to-all-done), channel_id=1, source_target_pairs={{0,1},{1,0},{2,3},{3,2},{4,5},{5,4},{6,7},{7,6},{8,9},{9,8},{10,11... | collective-permute-start | bytes 9437192 | tf_op jit(solution)/shard_map/ppermute | solution.py:50
  97.8 0.2 multiply_reduce_fusion.1
  98.0 0.3 multiply_reduce_fusion
  98.4 2.2 %fusion.43 = (bf16[16,1,128,256]{3,2,1,0:T(8,128)(2,1)S(1)}, bf16[16,1,128,256]{3,2,1,0:T(8,128)(2,1)S(1)}, bf16[16,1,128,256]{3,2,1,0:T(8,128)(2,1)S(1)}) fusion(bf16[16,3,128,256]{3,2,1,0:T(8,128)(2,1)} %all-to-all-done), kind=kLoop, calls=%fused_computation.94 | loop fusion | bytes 6291456 | tf_op jit(solution)/shard_map/slice | solution.py:30
  100.6 1.2 convolution_multiply_fusion.6
  101.8 1.0 convolution_multiply_fusion.10
  102.8 0.4 convolution_multiply_fusion.2
  103.3 3.0 %fusion.27 = f32[128,2048]{1,0:T(8,128)} fusion(bf16[2048,256]{1,0:T(8,128)(2,1)S(1)} %bitcast.59, f32[128,256]{1,0:T(8,128)} %convolution_multiply_fusion.6, bf16[128,2048]{1,0:T(8,128)(2,1)} %copy-done.5, bf16[2048,256]{1,0:T(8,128)(2,1)S(1)} %bitcast.55, f32[128]{0:T(128)S(1)} %add_rsqrt_fusion.1), kind=kOutput, calls=%fused_computation.60 | convolution fusion | flops 268664832 | bytes 3801600 | tf_op jit(solution)/shard_map/dot_general | solution.py:24
  106.3 3.0 %fusion.26 = f32[128,2048]{1,0:T(8,128)} fusion(bf16[2048,256]{1,0:T(8,128)(2,1)S(1)} %bitcast.60, f32[128,256]{1,0:T(8,128)} %convolution_multiply_fusion.10, bf16[128,2048]{1,0:T(8,128)(2,1)} %copy-done.8, bf16[2048,256]{1,0:T(8,128)(2,1)S(1)} %bitcast.56, f32[128]{0:T(128)S(1)} %add_rsqrt_fusion.2), kind=kOutput, calls=%fused_computation.59 | convolution fusion | flops 268664832 | bytes 3801600 | tf_op jit(solution)/shard_map/dot_general | solution.py:24
  109.3 2.7 %fusion.19 = f32[256,2048]{1,0:T(8,128)} fusion(bf16[2048,256]{1,0:T(8,128)(2,1)S(1)} %bitcast.61, f32[256,256]{1,0:T(8,128)S(1)} %convolution_multiply_fusion.2, bf16[256,2048]{1,0:T(8,128)(2,1)S(1)} %constant_dynamic-update-slice_fusion.8, bf16[2048,256]{1,0:T(8,128)(2,1)S(1)} %bitcast.57, f32[256]{0:T(256)S(1)} %add_rsqrt_fusion), kind=kOutput, calls=%fused_computation.46 | convolution fusion | flops 537329664 | bytes 5506048 | tf_op jit(solution)/shard_map/dot_general | solution.py:24
  112.0 2.2 %fusion.42 = (bf16[16,1,128,256]{3,2,1,0:T(8,128)(2,1)S(1)}, bf16[16,1,128,256]{3,2,1,0:T(8,128)(2,1)S(1)}, bf16[16,1,128,256]{3,2,1,0:T(8,128)(2,1)S(1)}) fusion(bf16[16,3,128,256]{3,2,1,0:T(8,128)(2,1)} %collective-permute-done.3), kind=kLoop, calls=%fused_computation.93 | loop fusion | bytes 6291456 | tf_op jit(solution)/shard_map/slice | solution.py:30
  114.2 1.0 convolution_multiply_fusion.4
  115.2 0.4 convolution_multiply_fusion
  115.6 3.2 %fusion.1 = bf16[128,2048]{1,0:T(8,128)(2,1)} fusion(f32[128,2048]{1,0:T(8,128)} %fusion.27, bf16[2048,256]{1,0:T(8,128)(2,1)S(1)} %bitcast.49, f32[128,256]{1,0:T(8,128)} %convolution_multiply_fusion.4, bf16[128,2048]{1,0:T(8,128)(2,1)} %copy-done.5, bf16[2048,256]{1,0:T(8,128)(2,1)S(1)} %bitcast.46, f32[128]{0:T(128)S(1)} %add_rsqrt_fusion.1), kind=kOutput, calls=%fused_computation.4 | convolution fusion | flops 269189120 | bytes 4325888 | tf_op jit(solution)/shard_map/dot_general | solution.py:24
  118.8 1.9 fusion.45
  120.7 1.9 collective-permute-start.12
  122.6 5.4 %collective-permute-start.13 = (bf16[64,2048]{1,0:T(8,128)(2,1)}, bf16[64,2048]{1,0:T(8,128)(2,1)}, u32[]{:S(2)}, u32[]{:S(2)}) collective-permute-start(bf16[64,2048]{1,0:T(8,128)(2,1)} %get-tuple-element.16), channel_id=1, source_target_pairs={{0,28},{2,30},{4,0},{6,2},{8,4},{10,6},{12,8},{14,10},{16,12},{18,... | collective-permute-start | bytes 786440 | tf_op jit(solution)/shard_map/ppermute | solution.py:13
  128.0 3.9 %fusion = bf16[256,2048]{1,0:T(8,128)(2,1)} fusion(f32[256,2048]{1,0:T(8,128)} %fusion.19, bf16[2048,256]{1,0:T(8,128)(2,1)S(1)} %bitcast.50, f32[256,256]{1,0:T(8,128)S(1)} %convolution_multiply_fusion, bf16[256,2048]{1,0:T(8,128)(2,1)S(1)} %constant_dynamic-update-slice_fusion.8, bf16[2048,256]{1,0:T(8,128)(2,1)S(1)} %bitcast.47, f32[256]{0:T(256)S(1)} %add_rsqrt_fusion), kind=kOutput, calls=%fused_computation.1 | convolution fusion | flops 538378240 | bytes 6554624 | tf_op jit(solution)/shard_map/dot_general | solution.py:24
  131.9 2.4 %fusion.44 = (bf16[128,2048]{1,0:T(8,128)(2,1)}, bf16[128,2048]{1,0:T(8,128)(2,1)}) fusion(bf16[256,2048]{1,0:T(8,128)(2,1)} %fusion), kind=kLoop, calls=%fused_computation.95 | loop fusion | bytes 2097152 | tf_op jit(solution)/shard_map/slice | solution.py:56
  134.3 1.9 collective-permute-start.8
  136.2 3.9 %collective-permute-start.9 = (bf16[128,2048]{1,0:T(8,128)(2,1)}, bf16[128,2048]{1,0:T(8,128)(2,1)}, u32[]{:S(2)}, u32[]{:S(2)}) collective-permute-start(bf16[128,2048]{1,0:T(8,128)(2,1)} %get-tuple-element.14), channel_id=1, source_target_pairs={{0,30},{2,0},{4,2},{6,4},{8,6},{10,8},{12,10},{14,12},{16,14},{18,... | collective-permute-start | bytes 1572872 | tf_op jit(solution)/shard_map/ppermute | solution.py:13
  140.1 0.3 convolution_multiply_fusion.8
  140.5 3.2 %convolution_add_fusion.2 = f32[128,2048]{1,0:T(8,128)} fusion(f32[128,2048]{1,0:T(8,128)} %fusion.26, bf16[2048,256]{1,0:T(8,128)(2,1)S(1)} %bitcast.51, f32[128,256]{1,0:T(8,128)S(1)} %convolution_multiply_fusion.8, bf16[128,2048]{1,0:T(8,128)(2,1)S(1)} %copy-done.10, bf16[2048,256]{1,0:T(8,128)(2,1)S(1)} %bitcast.48, f32[128]{0:T(128)S(1)} %add_rsqrt_fusion.2), kind=kOutput, calls=%fused_computation.3 | convolution fusion | flops 268926976 | bytes 4850176 | tf_op jit(solution)/shard_map/dot_general | solution.py:24
  143.6 6.9 %collective-permute-done.8 = bf16[128,2048]{1,0:T(8,128)(2,1)} collective-permute-done((bf16[128,2048]{1,0:T(8,128)(2,1)}, bf16[128,2048]{1,0:T(8,128)(2,1)}, u32[]{:S(2)}, u32[]{:S(2)}) %collective-permute-start.8) | collective-permute-done | bytes 524320 | tf_op jit(solution)/shard_map/ppermute | solution.py:13
  150.5 2.0 %collective-permute-done.9 = bf16[128,2048]{1,0:T(8,128)(2,1)} collective-permute-done((bf16[128,2048]{1,0:T(8,128)(2,1)}, bf16[128,2048]{1,0:T(8,128)(2,1)}, u32[]{:S(2)}, u32[]{:S(2)}) %collective-permute-start.9) | collective-permute-done | bytes 524320 | tf_op jit(solution)/shard_map/ppermute | solution.py:13
  152.5 1.6 fusion.9
  154.2 6.3 %collective-permute-start.14 = (bf16[32,2048]{1,0:T(8,128)(2,1)S(1)}, bf16[32,2048]{1,0:T(8,128)(2,1)S(1)}, u32[]{:S(2)}, u32[]{:S(2)}) collective-permute-start(bf16[32,2048]{1,0:T(8,128)(2,1)S(1)} %get-tuple-element.10), channel_id=1, source_target_pairs={{0,16},{2,18},{4,20},{6,22},{8,24},{10,26},{12,28},{14,30},{16,0},... | collective-permute-start | bytes 393224 | tf_op jit(solution)/shard_map/ppermute | solution.py:13
  160.5 8.7 %collective-permute-start.15 = (bf16[32,2048]{1,0:T(8,128)(2,1)S(1)}, bf16[32,2048]{1,0:T(8,128)(2,1)S(1)}, u32[]{:S(2)}, u32[]{:S(2)}) collective-permute-start(bf16[32,2048]{1,0:T(8,128)(2,1)S(1)} %get-tuple-element.12), channel_id=1, source_target_pairs={{0,8},{2,10},{4,12},{6,14},{8,16},{10,18},{12,20},{14,22},{16,24},... | collective-permute-start | bytes 393224 | tf_op jit(solution)/shard_map/ppermute | solution.py:13
  169.2 1.9 %collective-permute-start.16 = (bf16[32,2048]{1,0:T(8,128)(2,1)S(1)}, bf16[32,2048]{1,0:T(8,128)(2,1)S(1)}, u32[]{:S(2)}, u32[]{:S(2)}) collective-permute-start(bf16[32,2048]{1,0:T(8,128)(2,1)S(1)} %get-tuple-element.11), channel_id=1, source_target_pairs={{0,24},{2,26},{4,28},{6,30},{8,0},{10,2},{12,4},{14,6},{16,8},{18,... | collective-permute-start | bytes 393224 | tf_op jit(solution)/shard_map/ppermute | solution.py:13
  171.2 7.5 %collective-permute-done.15 = bf16[32,2048]{1,0:T(8,128)(2,1)S(1)} collective-permute-done((bf16[32,2048]{1,0:T(8,128)(2,1)S(1)}, bf16[32,2048]{1,0:T(8,128)(2,1)S(1)}, u32[]{:S(2)}, u32[]{:S(2)}) %collective-permute-start.15) | collective-permute-done | bytes 131104 | tf_op jit(solution)/shard_map/ppermute | solution.py:13
  178.7 10.8 %collective-permute-done.16 = bf16[32,2048]{1,0:T(8,128)(2,1)S(1)} collective-permute-done((bf16[32,2048]{1,0:T(8,128)(2,1)S(1)}, bf16[32,2048]{1,0:T(8,128)(2,1)S(1)}, u32[]{:S(2)}, u32[]{:S(2)}) %collective-permute-start.16) | collective-permute-done | bytes 131104 | tf_op jit(solution)/shard_map/ppermute | solution.py:13
  189.4 2.0 %fusion.18 = bf16[32,2048]{1,0:T(8,128)(2,1)} fusion(f32[128,2048]{1,0:T(8,128)} %convolution_add_fusion.2, bf16[32,2048]{1,0:T(8,128)(2,1)S(1)} %collective-permute-done.16, bf16[32,2048]{1,0:T(8,128)(2,1)S(1)} %collective-permute-done.15, bf16[32,2048]{1,0:T(8,128)(2,1)S(1)} %collective-permute-done.14, bf16[32,2048]{1,0:T(8,128)(2,1)S(1)} %copy-done.11, ...), kind=kLoop, calls=%fused_computation.42 | loop fusion | flops 1179648 | bytes 1441792 | tf_op jit(solution)/shard_map/convert_element_type | solution.py:73
  (50 shorter events, 0.4 us)
Async XLA Ops:
  3.9 7.6 %copy-start.11 = (bf16[32,2048]{1,0:T(8,128)(2,1)S(1)}, bf16[32,2048]{1,0:T(8,128)(2,1)}, u32[]{:S(2)}) copy-start(bf16[32,2048]{1,0:T(8,128)(2,1)} %param.5) | copy-start | bytes 393220
  3.9 92.0 %all-to-all-start = ((bf16[16,3,128,256]{3,2,1,0:T(8,128)(2,1)}), bf16[16,3,128,256]{3,2,1,0:T(8,128)(2,1)}, u32[]{:S(2)}, u32[]{:S(2)}) async-start(bf16[16,3,128,256]{3,2,1,0:T(8,128)(2,1)} %broadcast_in_dim.2), calls=%async_computation | async-start | bytes 6291456 | tf_op jit(solution)/shard_map/all_to_all | solution.py:38
  11.5 44.5 %collective-permute-start.1 = (bf16[32,2048]{1,0:T(8,128)(2,1)S(1)}, bf16[32,2048]{1,0:T(8,128)(2,1)S(1)}, u32[]{:S(2)}, u32[]{:S(2)}) collective-permute-start(bf16[32,2048]{1,0:T(8,128)(2,1)S(1)} %copy-done.11), channel_id=1, source_target_pairs={{0,24},{2,26},{4,28},{6,30},{8,0},{10,2},{12,4},{14,6},{16,8},{18,... | collective-permute-start | bytes 393224 | tf_op jit(solution)/shard_map/ppermute | solution.py:13
  22.4 33.6 %collective-permute-start.2 = (bf16[32,2048]{1,0:T(8,128)(2,1)S(1)}, bf16[32,2048]{1,0:T(8,128)(2,1)S(1)}, u32[]{:S(2)}, u32[]{:S(2)}) collective-permute-start(bf16[32,2048]{1,0:T(8,128)(2,1)S(1)} %copy-done.11), channel_id=1, source_target_pairs={{0,8},{2,10},{4,12},{6,14},{8,16},{10,18},{12,20},{14,22},{16,24},... | collective-permute-start | bytes 393224 | tf_op jit(solution)/shard_map/ppermute | solution.py:13
  24.4 25.8 %collective-permute-start = (bf16[32,2048]{1,0:T(8,128)(2,1)S(1)}, bf16[32,2048]{1,0:T(8,128)(2,1)S(1)}, u32[]{:S(2)}, u32[]{:S(2)}) collective-permute-start(bf16[32,2048]{1,0:T(8,128)(2,1)S(1)} %copy-done.11), channel_id=1, source_target_pairs={{0,16},{2,18},{4,20},{6,22},{8,24},{10,26},{12,28},{14,30},{16,0},... | collective-permute-start | bytes 393224 | tf_op jit(solution)/shard_map/ppermute | solution.py:13
  50.2 33.0 %collective-permute-start.4 = (bf16[64,2048]{1,0:T(8,128)(2,1)S(1)}, bf16[64,2048]{1,0:T(8,128)(2,1)S(1)}, u32[]{:S(2)}, u32[]{:S(2)}) collective-permute-start(bf16[64,2048]{1,0:T(8,128)(2,1)S(1)} %get-tuple-element.21), channel_id=1, source_target_pairs={{0,30},{2,0},{4,2},{6,4},{8,6},{10,8},{12,10},{14,12},{16,14},{18,... | collective-permute-start | bytes 786440 | tf_op jit(solution)/shard_map/ppermute | solution.py:13
  52.1 43.7 %collective-permute-start.6 = (bf16[64,2048]{1,0:T(8,128)(2,1)S(1)}, bf16[64,2048]{1,0:T(8,128)(2,1)S(1)}, u32[]{:S(2)}, u32[]{:S(2)}) collective-permute-start(bf16[64,2048]{1,0:T(8,128)(2,1)S(1)} %get-tuple-element.21), channel_id=1, source_target_pairs={{0,2},{2,4},{4,6},{6,8},{8,10},{10,12},{12,14},{14,16},{16,18},{18... | collective-permute-start | bytes 786440 | tf_op jit(solution)/shard_map/ppermute | solution.py:13
  56.1 39.7 %copy-start.8 = (bf16[128,2048]{1,0:T(8,128)(2,1)}, bf16[128,2048]{1,0:T(8,128)(2,1)S(1)}, u32[]{:S(2)}) copy-start(bf16[128,2048]{1,0:T(8,128)(2,1)S(1)} %get-tuple-element.18) | copy-start | bytes 1572868
  56.1 39.7 %collective-permute-start.5 = (bf16[64,2048]{1,0:T(8,128)(2,1)S(1)}, bf16[64,2048]{1,0:T(8,128)(2,1)S(1)}, u32[]{:S(2)}, u32[]{:S(2)}) collective-permute-start(bf16[64,2048]{1,0:T(8,128)(2,1)S(1)} %get-tuple-element.17), channel_id=1, source_target_pairs={{0,30},{2,0},{4,2},{6,4},{8,6},{10,8},{12,10},{14,12},{16,14},{18,... | collective-permute-start | bytes 786440 | tf_op jit(solution)/shard_map/ppermute | solution.py:13
  62.4 35.6 %collective-permute-start.7 = (bf16[64,2048]{1,0:T(8,128)(2,1)S(1)}, bf16[64,2048]{1,0:T(8,128)(2,1)S(1)}, u32[]{:S(2)}, u32[]{:S(2)}) collective-permute-start(bf16[64,2048]{1,0:T(8,128)(2,1)S(1)} %get-tuple-element.17), channel_id=1, source_target_pairs={{0,2},{2,4},{4,6},{6,8},{8,10},{10,12},{12,14},{14,16},{16,18},{18... | collective-permute-start | bytes 786440 | tf_op jit(solution)/shard_map/ppermute | solution.py:13
  64.3 16.4 %collective-permute-start.10 = (bf16[64,2048]{1,0:T(8,128)(2,1)S(1)}, bf16[64,2048]{1,0:T(8,128)(2,1)S(1)}, u32[]{:S(2)}, u32[]{:S(2)}) collective-permute-start(bf16[64,2048]{1,0:T(8,128)(2,1)S(1)} %get-tuple-element.26), channel_id=1, source_target_pairs={{0,28},{2,30},{4,0},{6,2},{8,4},{10,6},{12,8},{14,10},{16,12},{18,... | collective-permute-start | bytes 786440 | tf_op jit(solution)/shard_map/ppermute | solution.py:13
  80.7 15.0 %collective-permute-start.11 = (bf16[64,2048]{1,0:T(8,128)(2,1)S(1)}, bf16[64,2048]{1,0:T(8,128)(2,1)S(1)}, u32[]{:S(2)}, u32[]{:S(2)}) collective-permute-start(bf16[64,2048]{1,0:T(8,128)(2,1)S(1)} %get-tuple-element.25), channel_id=1, source_target_pairs={{0,4},{2,6},{4,8},{6,10},{8,12},{10,14},{12,16},{14,18},{16,20},{1... | collective-permute-start | bytes 786440 | tf_op jit(solution)/shard_map/ppermute | solution.py:13
  95.8 2.6 %copy-start.5 = (bf16[128,2048]{1,0:T(8,128)(2,1)}, bf16[128,2048]{1,0:T(8,128)(2,1)S(1)}, u32[]{:S(2)}) copy-start(bf16[128,2048]{1,0:T(8,128)(2,1)S(1)} %constant_dynamic-update-slice_fusion.12) | copy-start | bytes 1572868
  95.9 16.1 %collective-permute-start.3 = (bf16[16,3,128,256]{3,2,1,0:T(8,128)(2,1)}, bf16[16,3,128,256]{3,2,1,0:T(8,128)(2,1)}, u32[]{:S(2)}, u32[]{:S(2)}) collective-permute-start(bf16[16,3,128,256]{3,2,1,0:T(8,128)(2,1)} %all-to-all-done), channel_id=1, source_target_pairs={{0,1},{1,0},{2,3},{3,2},{4,5},{5,4},{6,7},{7,6},{8,9},{9,8},{10,11... | collective-permute-start | bytes 9437192 | tf_op jit(solution)/shard_map/ppermute | solution.py:50
  98.3 2.3 %copy-start.6 = (bf16[128,2048]{1,0:T(8,128)(2,1)S(1)}, bf16[128,2048]{1,0:T(8,128)(2,1)}, u32[]{:S(2)}) copy-start(bf16[128,2048]{1,0:T(8,128)(2,1)} %copy-done.5) | copy-start | bytes 1572868
  98.3 3.5 %copy-start.9 = (bf16[128,2048]{1,0:T(8,128)(2,1)S(1)}, bf16[128,2048]{1,0:T(8,128)(2,1)}, u32[]{:S(2)}) copy-start(bf16[128,2048]{1,0:T(8,128)(2,1)} %copy-done.8) | copy-start | bytes 1572868
  100.6 2.7 %copy-start = (bf16[16,1,128,256]{3,2,1,0:T(8,128)(2,1)}, bf16[16,1,128,256]{3,2,1,0:T(8,128)(2,1)S(1)}, u32[]{:S(2)}) copy-start(bf16[16,1,128,256]{3,2,1,0:T(8,128)(2,1)S(1)} %get-tuple-element.9) | copy-start | bytes 3145732
  100.6 8.7 %copy-start.3 = (bf16[16,1,128,256]{3,2,1,0:T(8,128)(2,1)}, bf16[16,1,128,256]{3,2,1,0:T(8,128)(2,1)S(1)}, u32[]{:S(2)}) copy-start(bf16[16,1,128,256]{3,2,1,0:T(8,128)(2,1)S(1)} %get-tuple-element.7) | copy-start | bytes 3145732
  100.6 8.7 %copy-start.4 = (bf16[16,1,128,256]{3,2,1,0:T(8,128)(2,1)}, bf16[16,1,128,256]{3,2,1,0:T(8,128)(2,1)S(1)}, u32[]{:S(2)}) copy-start(bf16[16,1,128,256]{3,2,1,0:T(8,128)(2,1)S(1)} %get-tuple-element.8) | copy-start | bytes 3145732
  112.0 2.2 %copy-start.7 = (bf16[128,2048]{1,0:T(8,128)(2,1)S(1)}, bf16[128,2048]{1,0:T(8,128)(2,1)}, u32[]{:S(2)}) copy-start(bf16[128,2048]{1,0:T(8,128)(2,1)} %copy-done.5) | copy-start | bytes 1572868
  114.2 1.0 copy-start.1
  120.7 22.9 %collective-permute-start.12 = (bf16[64,2048]{1,0:T(8,128)(2,1)}, bf16[64,2048]{1,0:T(8,128)(2,1)}, u32[]{:S(2)}, u32[]{:S(2)}) collective-permute-start(bf16[64,2048]{1,0:T(8,128)(2,1)} %get-tuple-element.15), channel_id=1, source_target_pairs={{0,4},{2,6},{4,8},{6,10},{8,12},{10,14},{12,16},{14,18},{16,20},{1... | collective-permute-start | bytes 786440 | tf_op jit(solution)/shard_map/ppermute | solution.py:13
  122.6 21.0 %collective-permute-start.13 = (bf16[64,2048]{1,0:T(8,128)(2,1)}, bf16[64,2048]{1,0:T(8,128)(2,1)}, u32[]{:S(2)}, u32[]{:S(2)}) collective-permute-start(bf16[64,2048]{1,0:T(8,128)(2,1)} %get-tuple-element.16), channel_id=1, source_target_pairs={{0,28},{2,30},{4,0},{6,2},{8,4},{10,6},{12,8},{14,10},{16,12},{18,... | collective-permute-start | bytes 786440 | tf_op jit(solution)/shard_map/ppermute | solution.py:13
  131.9 8.3 %copy-start.2 = (bf16[16,1,128,256]{3,2,1,0:T(8,128)(2,1)S(1)}, bf16[16,1,128,256]{3,2,1,0:T(8,128)(2,1)}, u32[]{:S(2)}) copy-start(bf16[16,1,128,256]{3,2,1,0:T(8,128)(2,1)} %copy-done.1) | copy-start | bytes 3145732
  131.9 8.3 %copy-start.10 = (bf16[128,2048]{1,0:T(8,128)(2,1)S(1)}, bf16[128,2048]{1,0:T(8,128)(2,1)}, u32[]{:S(2)}) copy-start(bf16[128,2048]{1,0:T(8,128)(2,1)} %copy-done.8) | copy-start | bytes 1572868
  134.3 16.2 %collective-permute-start.8 = (bf16[128,2048]{1,0:T(8,128)(2,1)}, bf16[128,2048]{1,0:T(8,128)(2,1)}, u32[]{:S(2)}, u32[]{:S(2)}) collective-permute-start(bf16[128,2048]{1,0:T(8,128)(2,1)} %get-tuple-element.13), channel_id=1, source_target_pairs={{0,2},{2,4},{4,6},{6,8},{8,10},{10,12},{12,14},{14,16},{16,18},{18... | collective-permute-start | bytes 1572872 | tf_op jit(solution)/shard_map/ppermute | solution.py:13
  136.2 16.4 %collective-permute-start.9 = (bf16[128,2048]{1,0:T(8,128)(2,1)}, bf16[128,2048]{1,0:T(8,128)(2,1)}, u32[]{:S(2)}, u32[]{:S(2)}) collective-permute-start(bf16[128,2048]{1,0:T(8,128)(2,1)} %get-tuple-element.14), channel_id=1, source_target_pairs={{0,30},{2,0},{4,2},{6,4},{8,6},{10,8},{12,10},{14,12},{16,14},{18,... | collective-permute-start | bytes 1572872 | tf_op jit(solution)/shard_map/ppermute | solution.py:13
  154.2 17.0 %collective-permute-start.14 = (bf16[32,2048]{1,0:T(8,128)(2,1)S(1)}, bf16[32,2048]{1,0:T(8,128)(2,1)S(1)}, u32[]{:S(2)}, u32[]{:S(2)}) collective-permute-start(bf16[32,2048]{1,0:T(8,128)(2,1)S(1)} %get-tuple-element.10), channel_id=1, source_target_pairs={{0,16},{2,18},{4,20},{6,22},{8,24},{10,26},{12,28},{14,30},{16,0},... | collective-permute-start | bytes 393224 | tf_op jit(solution)/shard_map/ppermute | solution.py:13
  160.5 18.2 %collective-permute-start.15 = (bf16[32,2048]{1,0:T(8,128)(2,1)S(1)}, bf16[32,2048]{1,0:T(8,128)(2,1)S(1)}, u32[]{:S(2)}, u32[]{:S(2)}) collective-permute-start(bf16[32,2048]{1,0:T(8,128)(2,1)S(1)} %get-tuple-element.12), channel_id=1, source_target_pairs={{0,8},{2,10},{4,12},{6,14},{8,16},{10,18},{12,20},{14,22},{16,24},... | collective-permute-start | bytes 393224 | tf_op jit(solution)/shard_map/ppermute | solution.py:13
  169.2 20.2 %collective-permute-start.16 = (bf16[32,2048]{1,0:T(8,128)(2,1)S(1)}, bf16[32,2048]{1,0:T(8,128)(2,1)S(1)}, u32[]{:S(2)}, u32[]{:S(2)}) collective-permute-start(bf16[32,2048]{1,0:T(8,128)(2,1)S(1)} %get-tuple-element.11), channel_id=1, source_target_pairs={{0,24},{2,26},{4,28},{6,30},{8,0},{10,2},{12,4},{14,6},{16,8},{18,... | collective-permute-start | bytes 393224 | tf_op jit(solution)/shard_map/ppermute | solution.py:13

commit v2 on v1

v2 whole, which is shorter than its diff:
```python
import jax
import jax.numpy as jnp
from jax import lax
from jax.experimental import pallas as pl
from jax.experimental.pallas import tpu as pltpu
from jax.sharding import Mesh
from jax.sharding import PartitionSpec as P


TP = ("z", "c")
ROWS = ("fs", "z", "c")
VMEM = pl.BlockSpec(memory_space=pltpu.VMEM)


def move(array, by):
    planes = lax.axis_size("z")
    return lax.ppermute(array, "z", [(i, (i + by) % planes) for i in range(planes)])


def sums_kernel(rows_ref, own_ref, partner_ref, out_ref):
    rows = rows_ref[...]
    width = rows.shape[1]
    wide = rows.astype(jnp.float32)
    row_scale = lax.rsqrt(jnp.mean(wide * wide, axis=1, keepdims=True) + 1e-06)
    hidden = []
    for ref in (own_ref, partner_ref):
        gate = ref[:, 0].reshape(width, -1)
        up = ref[:, 1].reshape(width, -1)
        gate_proj = row_scale * jnp.dot(rows, gate, preferred_element_type=jnp.float32)
        up_proj = row_scale * jnp.dot(rows, up, preferred_element_type=jnp.float32)
        hidden.append((gate_proj / (1.0 + jnp.exp(-gate_proj)) * up_proj).astype(jnp.bfloat16))
    total = None
    for ref, part in zip((own_ref, partner_ref), hidden):
        down = ref[:, 2].reshape(width, -1)
        share = lax.dot_general(part, down, (((1,), (1,)), ((), ())), preferred_element_type=jnp.float32)
        total = share if total is None else total + share
    out_ref[...] = total.astype(out_ref.dtype)


def partial_sums(rows, own, partner, dtype):
    units = 2 * own.shape[-1]
    count, width = rows.shape
    return pl.pallas_call(
        sums_kernel,
        out_shape=jax.ShapeDtypeStruct((count, width), dtype),
        in_specs=[VMEM, VMEM, VMEM],
        out_specs=VMEM,
        compiler_params=pltpu.CompilerParams(vmem_limit_bytes=32 * 1024 * 1024),
        cost_estimate=pl.CostEstimate(flops=6 * count * width * units, bytes_accessed=6 * width * units, transcendentals=count * units),
        name="sums",
    )(rows, own, partner)


def step(tokens, norm_gain, gate_master, up_master, down_master):
    rows = tokens.shape[0]
    gain = norm_gain[:, None]
    shard = jnp.stack([(gain * gate_master).astype(jnp.bfloat16), (gain * up_master).astype(jnp.bfloat16), down_master.astype(jnp.bfloat16)])
    copies = jnp.broadcast_to(shard, (lax.axis_size("fs"), *shard.shape))
    packed = lax.all_to_all(copies, "fs", split_axis=0, concat_axis=0, tiled=True)

    far = move(tokens, 8)
    above = move(tokens, -4)
    below = move(tokens, 4)
    held = jnp.concatenate([tokens, far, above, below])
    from_next = move(held, -1)
    from_prev = move(held, 1)
    from_next2 = move(jnp.concatenate([tokens, above]), -2)
    from_prev2 = move(jnp.concatenate([tokens, below]), 2)

    partner = lax.ppermute(packed, "c", [(0, 1), (1, 0)])

    ones = partial_sums(jnp.concatenate([from_next, from_prev]), packed, partner, jnp.bfloat16)
    to_next = move(ones[: 4 * rows], 1)
    to_prev = move(ones[4 * rows :], -1)
    twos = partial_sums(jnp.concatenate([from_next2, from_prev2]), packed, partner, jnp.bfloat16)
    to_next2 = move(twos[: 2 * rows], 2)
    to_prev2 = move(twos[2 * rows :], -2)
    own = partial_sums(held, packed, partner, jnp.float32)

    def block(array, k):
        return array[k * rows : (k + 1) * rows].astype(jnp.float32)

    sum_far = block(own, 1) + block(to_next, 1) + block(to_prev, 1)
    back_far = move(sum_far.astype(jnp.bfloat16), 8)
    sum_above = block(own, 2) + block(to_next, 2) + block(to_prev, 2) + block(to_next2, 1)
    back_above = move(sum_above.astype(jnp.bfloat16), 4)
    sum_below = block(own, 3) + block(to_next, 3) + block(to_prev, 3) + block(to_prev2, 1)
    back_below = move(sum_below.astype(jnp.bfloat16), -4)
    here = block(own, 0) + block(to_next, 0) + block(to_prev, 0) + block(to_next2, 0) + block(to_prev2, 0)
    summed = here + back_far.astype(jnp.float32) + back_above.astype(jnp.float32) + back_below.astype(jnp.float32)
    mixed = (tokens.astype(jnp.float32) + 0.5 * summed).astype(jnp.bfloat16)
    return (mixed, *(packed[:, k].reshape(-1, packed.shape[-1]) for k in range(3)))


def solution(mesh):
    split = Mesh(mesh.devices.reshape(mesh.shape["fs"], 16, 2), ROWS)
    placed = (P(ROWS, None), P("fs"), P("fs", TP), P("fs", TP), P("fs", TP))
    return jax.shard_map(
        step,
        mesh=split,
        in_specs=placed,
        out_specs=(P(ROWS, None), P(None, TP), P(None, TP), P(None, TP)),
        check_vma=False,
    )
```

time: 192 us -> 193 us (level)
  the two profiles are of different devices: /device:TPU:66 before, /device:TPU:6 now
where the time goes in v2:
time: 193 us; the launch traced here: 189 us
  starting transfers between devices  80.5 us (42%)
  waiting for transfers between devices  53.5 us (28%)
  blocking collectives  44.7 us (23%)
  Pallas kernels  4.85 us (3%)
  other arithmetic  2.32 us (1%)
  local copies, waits for them, and re-layouts  2.31 us (1%)
    ppermute x14, starting transfers between devices, move(): lax.ppermute(array, 'z', [(i, (i + by) % planes) for i in range(planes)])  78.6 us
    ppermute x14, waiting for transfers between devices, move(): lax.ppermute(array, 'z', [(i, (i + by) % planes) for i in range(planes)])  53.5 us
    all_to_all x1, blocking collectives, step(): lax.all_to_all(copies, 'fs', split_axis=0, concat_axis=0, tiled=True)  44.7 us
    pallas_call x3, Pallas kernels, partial_sums(): pl.pallas_call(sums_kernel, out_shape=jax.ShapeDtypeStruct((count, width)...  4.85 us
  transfers between devices with their start and end apart: 15, of which 8 were waited for; matrix products, arithmetic and copies ran while one was open for 1% of the time, Pallas kernels for 2%

profile of v2, /device:TPU:6, one launch (start us, length us, event | category | flops | bytes accessed | tf_op | source)
XLA Modules:
  0.0 189.1 jit_solution(15713515658146530095)
XLA Ops:
  0.6 1.1 fusion.17
  1.8 0.4 broadcast_in_dim.4
  2.2 0.0 copy-start
  2.2 44.7 %all_to_all.5.own_ref = bf16[16,3,128,256]{3,2,1,0:T(8,128)(2,1)S(1)} all-to-all(bf16[16,3,128,256]{3,2,1,0:T(8,128)(2,1)S(1)} %broadcast_in_dim.4), channel_id=1, replica_groups=mesh['fs'=16,'z'=16,'c'=2] {'fs'}, dimensions={0} | all-to-all | bytes 6291456 | tf_op jit(solution)/shard_map/all_to_all | solution.py:59
  46.9 1.9 %collective-permute-start.3 = (bf16[16,3,128,256]{3,2,1,0:T(8,128)(2,1)S(1)}, bf16[16,3,128,256]{3,2,1,0:T(8,128)(2,1)S(1)}, u32[]{:S(2)}, u32[]{:S(2)}) collective-permute-start(bf16[16,3,128,256]{3,2,1,0:T(8,128)(2,1)S(1)} %all_to_all.5.own_ref), channel_id=1, source_target_pairs={{0,1},{1,0},{2,3},{3,2},{4,5},{5,4},{6,7},{7,6},{8,9},{9,8},{10,11... | collective-permute-start | bytes 9437192 | tf_op jit(solution)/shard_map/ppermute | solution.py:70
  48.8 0.0 copy-done
  48.8 12.4 %collective-permute-start.1 = (bf16[32,2048]{1,0:T(8,128)(2,1)S(1)}, bf16[32,2048]{1,0:T(8,128)(2,1)S(1)}, u32[]{:S(2)}, u32[]{:S(2)}) collective-permute-start(bf16[32,2048]{1,0:T(8,128)(2,1)S(1)} %copy-done), channel_id=1, source_target_pairs={{0,24},{2,26},{4,28},{6,30},{8,0},{10,2},{12,4},{14,6},{16,8},{18,... | collective-permute-start | bytes 393224 | tf_op jit(solution)/shard_map/ppermute | solution.py:17
  61.2 4.9 %collective-permute-start = (bf16[32,2048]{1,0:T(8,128)(2,1)S(1)}, bf16[32,2048]{1,0:T(8,128)(2,1)S(1)}, u32[]{:S(2)}, u32[]{:S(2)}) collective-permute-start(bf16[32,2048]{1,0:T(8,128)(2,1)S(1)} %copy-done), channel_id=1, source_target_pairs={{0,16},{2,18},{4,20},{6,22},{8,24},{10,26},{12,28},{14,30},{16,0},... | collective-permute-start | bytes 393224 | tf_op jit(solution)/shard_map/ppermute | solution.py:17
  66.1 7.8 %collective-permute-start.2 = (bf16[32,2048]{1,0:T(8,128)(2,1)S(1)}, bf16[32,2048]{1,0:T(8,128)(2,1)S(1)}, u32[]{:S(2)}, u32[]{:S(2)}) collective-permute-start(bf16[32,2048]{1,0:T(8,128)(2,1)S(1)} %copy-done), channel_id=1, source_target_pairs={{0,8},{2,10},{4,12},{6,14},{8,16},{10,18},{12,20},{14,22},{16,24},... | collective-permute-start | bytes 393224 | tf_op jit(solution)/shard_map/ppermute | solution.py:17
  74.0 10.0 %collective-permute-done = bf16[32,2048]{1,0:T(8,128)(2,1)S(1)} collective-permute-done((bf16[32,2048]{1,0:T(8,128)(2,1)S(1)}, bf16[32,2048]{1,0:T(8,128)(2,1)S(1)}, u32[]{:S(2)}, u32[]{:S(2)}) %collective-permute-start) | collective-permute-done | bytes 131104 | tf_op jit(solution)/shard_map/ppermute | solution.py:17
  83.9 0.0 collective-permute-done.1
  84.0 0.0 collective-permute-done.2
  84.0 14.7 %collective-permute-start.4 = (bf16[128,2048]{1,0:T(8,128)(2,1)S(1)}, bf16[128,2048]{1,0:T(8,128)(2,1)S(1)}, u32[]{:S(2)}, u32[]{:S(2)}) collective-permute-start(bf16[128,2048]{1,0:T(8,128)(2,1)S(1)} %constant_dynamic-update-slice_fusion.rows_ref), channel_id=1, source_target_pairs={{0,30},{2,0},{4,2},{6,4},{8,6},{10,8},{12,10},{14,12},{16,14},{18,... | collective-permute-start | bytes 1572872 | tf_op jit(solution)/shard_map/ppermute | solution.py:17
  98.7 1.9 %collective-permute-start.5 = (bf16[128,2048]{1,0:T(8,128)(2,1)S(1)}, bf16[128,2048]{1,0:T(8,128)(2,1)S(1)}, u32[]{:S(2)}, u32[]{:S(2)}) collective-permute-start(bf16[128,2048]{1,0:T(8,128)(2,1)S(1)} %constant_dynamic-update-slice_fusion.rows_ref), channel_id=1, source_target_pairs={{0,2},{2,4},{4,6},{6,8},{8,10},{10,12},{12,14},{14,16},{16,18},{18... | collective-permute-start | bytes 1572872 | tf_op jit(solution)/shard_map/ppermute | solution.py:17
  100.7 3.4 %collective-permute-start.8 = (bf16[64,2048]{1,0:T(8,128)(2,1)S(1)}, bf16[64,2048]{1,0:T(8,128)(2,1)S(1)}, u32[]{:S(2)}, u32[]{:S(2)}) collective-permute-start(bf16[64,2048]{1,0:T(8,128)(2,1)S(1)} %get-tuple-element.14), channel_id=1, source_target_pairs={{0,28},{2,30},{4,0},{6,2},{8,4},{10,6},{12,8},{14,10},{16,12},{18,... | collective-permute-start | bytes 786440 | tf_op jit(solution)/shard_map/ppermute | solution.py:17
  104.1 3.4 %collective-permute-start.9 = (bf16[64,2048]{1,0:T(8,128)(2,1)S(1)}, bf16[64,2048]{1,0:T(8,128)(2,1)S(1)}, u32[]{:S(2)}, u32[]{:S(2)}) collective-permute-start(bf16[64,2048]{1,0:T(8,128)(2,1)S(1)} %get-tuple-element.15), channel_id=1, source_target_pairs={{0,4},{2,6},{4,8},{6,10},{8,12},{10,14},{12,16},{14,18},{16,20},{1... | collective-permute-start | bytes 786440 | tf_op jit(solution)/shard_map/ppermute | solution.py:17
  107.4 13.9 %collective-permute-done.8 = bf16[64,2048]{1,0:T(8,128)(2,1)S(1)} collective-permute-done((bf16[64,2048]{1,0:T(8,128)(2,1)S(1)}, bf16[64,2048]{1,0:T(8,128)(2,1)S(1)}, u32[]{:S(2)}, u32[]{:S(2)}) %collective-permute-start.8) | collective-permute-done | bytes 262176 | tf_op jit(solution)/shard_map/ppermute | solution.py:17
  121.3 3.9 %collective-permute-done.9 = bf16[64,2048]{1,0:T(8,128)(2,1)S(1)} collective-permute-done((bf16[64,2048]{1,0:T(8,128)(2,1)S(1)}, bf16[64,2048]{1,0:T(8,128)(2,1)S(1)}, u32[]{:S(2)}, u32[]{:S(2)}) %collective-permute-start.9) | collective-permute-done | bytes 262176 | tf_op jit(solution)/shard_map/ppermute | solution.py:17
  125.3 0.0 collective-permute-done.4
  125.3 0.0 collective-permute-done.5
  125.3 0.1 pad_maximum_fusion.rows_ref
  125.4 0.0 collective-permute-done.3.partner_ref
  125.4 1.9 %sums.4 = bf16[256,2048]{1,0:T(8,128)(2,1)S(1)} custom-call(bf16[256,2048]{1,0:T(8,128)(2,1)S(1)} %pad_maximum_fusion.rows_ref, bf16[16,3,128,256]{3,2,1,0:T(8,128)(2,1)S(1)} %all_to_all.5.own_ref, bf16[16,3,128,256]{3,2,1,0:T(8,128)(2,1)S(1)} %collective-permute-done.3.partner_ref), custom_call_target="tpu_custom_call" | custom-call | flops 1610612736 | bytes 6291456 | tf_op jit(solution)/shard_map/sums/pallas_call | solution.py:43
  127.4 0.1 fusion.20
  127.5 4.7 %collective-permute-start.6 = (bf16[128,2048]{1,0:T(8,128)(2,1)S(1)}, bf16[128,2048]{1,0:T(8,128)(2,1)S(1)}, u32[]{:S(2)}, u32[]{:S(2)}) collective-permute-start(bf16[128,2048]{1,0:T(8,128)(2,1)S(1)} %get-tuple-element.10), channel_id=1, source_target_pairs={{0,2},{2,4},{4,6},{6,8},{8,10},{10,12},{12,14},{14,16},{16,18},{18... | collective-permute-start | bytes 1572872 | tf_op jit(solution)/shard_map/ppermute | solution.py:17
  132.2 2.3 %collective-permute-start.7 = (bf16[128,2048]{1,0:T(8,128)(2,1)S(1)}, bf16[128,2048]{1,0:T(8,128)(2,1)S(1)}, u32[]{:S(2)}, u32[]{:S(2)}) collective-permute-start(bf16[128,2048]{1,0:T(8,128)(2,1)S(1)} %get-tuple-element.11), channel_id=1, source_target_pairs={{0,30},{2,0},{4,2},{6,4},{8,6},{10,8},{12,10},{14,12},{16,14},{18,... | collective-permute-start | bytes 1572872 | tf_op jit(solution)/shard_map/ppermute | solution.py:17
  134.6 1.5 sums.5
  136.1 3.0 %collective-permute-start.10 = (bf16[64,2048]{1,0:T(8,128)(2,1)S(1)}, bf16[64,2048]{1,0:T(8,128)(2,1)S(1)}, u32[]{:S(2)}, u32[]{:S(2)}) collective-permute-start(bf16[64,2048]{1,0:T(8,128)(2,1)S(1)} %get-tuple-element.12), channel_id=1, source_target_pairs={{0,4},{2,6},{4,8},{6,10},{8,12},{10,14},{12,16},{14,18},{16,20},{1... | collective-permute-start | bytes 786440 | tf_op jit(solution)/shard_map/ppermute | solution.py:17
  139.1 5.0 %collective-permute-start.11 = (bf16[64,2048]{1,0:T(8,128)(2,1)S(1)}, bf16[64,2048]{1,0:T(8,128)(2,1)S(1)}, u32[]{:S(2)}, u32[]{:S(2)}) collective-permute-start(bf16[64,2048]{1,0:T(8,128)(2,1)S(1)} %get-tuple-element.13), channel_id=1, source_target_pairs={{0,28},{2,30},{4,0},{6,2},{8,4},{10,6},{12,8},{14,10},{16,12},{18,... | collective-permute-start | bytes 786440 | tf_op jit(solution)/shard_map/ppermute | solution.py:17
  144.0 1.5 sums.3
  145.5 4.2 %collective-permute-done.10 = bf16[64,2048]{1,0:T(8,128)(2,1)S(1)} collective-permute-done((bf16[64,2048]{1,0:T(8,128)(2,1)S(1)}, bf16[64,2048]{1,0:T(8,128)(2,1)S(1)}, u32[]{:S(2)}, u32[]{:S(2)}) %collective-permute-start.10) | collective-permute-done | bytes 262176 | tf_op jit(solution)/shard_map/ppermute | solution.py:17
  149.7 7.9 %collective-permute-done.11 = bf16[64,2048]{1,0:T(8,128)(2,1)S(1)} collective-permute-done((bf16[64,2048]{1,0:T(8,128)(2,1)S(1)}, bf16[64,2048]{1,0:T(8,128)(2,1)S(1)}, u32[]{:S(2)}, u32[]{:S(2)}) %collective-permute-start.11) | collective-permute-done | bytes 262176 | tf_op jit(solution)/shard_map/ppermute | solution.py:17
  157.7 0.0 collective-permute-done.6
  157.7 0.0 collective-permute-done.7
  157.7 0.2 fusion.7
  157.8 5.4 %collective-permute-start.12 = (bf16[32,2048]{1,0:T(8,128)(2,1)S(1)}, bf16[32,2048]{1,0:T(8,128)(2,1)S(1)}, u32[]{:S(2)}, u32[]{:S(2)}) collective-permute-start(bf16[32,2048]{1,0:T(8,128)(2,1)S(1)} %get-tuple-element.7), channel_id=1, source_target_pairs={{0,16},{2,18},{4,20},{6,22},{8,24},{10,26},{12,28},{14,30},{16,0},... | collective-permute-start | bytes 393224 | tf_op jit(solution)/shard_map/ppermute | solution.py:17
  163.2 7.2 %collective-permute-start.13 = (bf16[32,2048]{1,0:T(8,128)(2,1)S(1)}, bf16[32,2048]{1,0:T(8,128)(2,1)S(1)}, u32[]{:S(2)}, u32[]{:S(2)}) collective-permute-start(bf16[32,2048]{1,0:T(8,128)(2,1)S(1)} %get-tuple-element.9), channel_id=1, source_target_pairs={{0,8},{2,10},{4,12},{6,14},{8,16},{10,18},{12,20},{14,22},{16,24},... | collective-permute-start | bytes 393224 | tf_op jit(solution)/shard_map/ppermute | solution.py:17
  170.5 2.5 %collective-permute-start.14 = (bf16[32,2048]{1,0:T(8,128)(2,1)S(1)}, bf16[32,2048]{1,0:T(8,128)(2,1)S(1)}, u32[]{:S(2)}, u32[]{:S(2)}) collective-permute-start(bf16[32,2048]{1,0:T(8,128)(2,1)S(1)} %get-tuple-element.8), channel_id=1, source_target_pairs={{0,24},{2,26},{4,28},{6,30},{8,0},{10,2},{12,4},{14,6},{16,8},{18,... | collective-permute-start | bytes 393224 | tf_op jit(solution)/shard_map/ppermute | solution.py:17
  173.0 1.8 fusion.19
  174.8 7.4 %collective-permute-done.12 = bf16[32,2048]{1,0:T(8,128)(2,1)S(1)} collective-permute-done((bf16[32,2048]{1,0:T(8,128)(2,1)S(1)}, bf16[32,2048]{1,0:T(8,128)(2,1)S(1)}, u32[]{:S(2)}, u32[]{:S(2)}) %collective-permute-start.12) | collective-permute-done | bytes 131104 | tf_op jit(solution)/shard_map/ppermute | solution.py:17
  182.2 0.9 collective-permute-done.13
  183.0 5.2 %collective-permute-done.14 = bf16[32,2048]{1,0:T(8,128)(2,1)S(1)} collective-permute-done((bf16[32,2048]{1,0:T(8,128)(2,1)S(1)}, bf16[32,2048]{1,0:T(8,128)(2,1)S(1)}, u32[]{:S(2)}, u32[]{:S(2)}) %collective-permute-start.14) | collective-permute-done | bytes 131104 | tf_op jit(solution)/shard_map/ppermute | solution.py:17
  188.3 0.8 fusion.16
  (8 shorter events, 0.2 us)
Async XLA Ops:
  2.2 46.6 %copy-start = (bf16[32,2048]{1,0:T(8,128)(2,1)S(1)}, bf16[32,2048]{1,0:T(8,128)(2,1)}, u32[]{:S(2)}) copy-start(bf16[32,2048]{1,0:T(8,128)(2,1)} %param.5) | copy-start | bytes 393220
  46.9 78.6 %collective-permute-start.3 = (bf16[16,3,128,256]{3,2,1,0:T(8,128)(2,1)S(1)}, bf16[16,3,128,256]{3,2,1,0:T(8,128)(2,1)S(1)}, u32[]{:S(2)}, u32[]{:S(2)}) collective-permute-start(bf16[16,3,128,256]{3,2,1,0:T(8,128)(2,1)S(1)} %all_to_all.5.own_ref), channel_id=1, source_target_pairs={{0,1},{1,0},{2,3},{3,2},{4,5},{5,4},{6,7},{7,6},{8,9},{9,8},{10,11... | collective-permute-start | bytes 9437192 | tf_op jit(solution)/shard_map/ppermute | solution.py:70
  48.8 35.2 %collective-permute-start.1 = (bf16[32,2048]{1,0:T(8,128)(2,1)S(1)}, bf16[32,2048]{1,0:T(8,128)(2,1)S(1)}, u32[]{:S(2)}, u32[]{:S(2)}) collective-permute-start(bf16[32,2048]{1,0:T(8,128)(2,1)S(1)} %copy-done), channel_id=1, source_target_pairs={{0,24},{2,26},{4,28},{6,30},{8,0},{10,2},{12,4},{14,6},{16,8},{18,... | collective-permute-start | bytes 393224 | tf_op jit(solution)/shard_map/ppermute | solution.py:17
  61.2 22.7 %collective-permute-start = (bf16[32,2048]{1,0:T(8,128)(2,1)S(1)}, bf16[32,2048]{1,0:T(8,128)(2,1)S(1)}, u32[]{:S(2)}, u32[]{:S(2)}) collective-permute-start(bf16[32,2048]{1,0:T(8,128)(2,1)S(1)} %copy-done), channel_id=1, source_target_pairs={{0,16},{2,18},{4,20},{6,22},{8,24},{10,26},{12,28},{14,30},{16,0},... | collective-permute-start | bytes 393224 | tf_op jit(solution)/shard_map/ppermute | solution.py:17
  66.1 17.9 %collective-permute-start.2 = (bf16[32,2048]{1,0:T(8,128)(2,1)S(1)}, bf16[32,2048]{1,0:T(8,128)(2,1)S(1)}, u32[]{:S(2)}, u32[]{:S(2)}) collective-permute-start(bf16[32,2048]{1,0:T(8,128)(2,1)S(1)} %copy-done), channel_id=1, source_target_pairs={{0,8},{2,10},{4,12},{6,14},{8,16},{10,18},{12,20},{14,22},{16,24},... | collective-permute-start | bytes 393224 | tf_op jit(solution)/shard_map/ppermute | solution.py:17
  84.0 41.3 %collective-permute-start.4 = (bf16[128,2048]{1,0:T(8,128)(2,1)S(1)}, bf16[128,2048]{1,0:T(8,128)(2,1)S(1)}, u32[]{:S(2)}, u32[]{:S(2)}) collective-permute-start(bf16[128,2048]{1,0:T(8,128)(2,1)S(1)} %constant_dynamic-update-slice_fusion.rows_ref), channel_id=1, source_target_pairs={{0,30},{2,0},{4,2},{6,4},{8,6},{10,8},{12,10},{14,12},{16,14},{18,... | collective-permute-start | bytes 1572872 | tf_op jit(solution)/shard_map/ppermute | solution.py:17
  98.7 26.6 %collective-permute-start.5 = (bf16[128,2048]{1,0:T(8,128)(2,1)S(1)}, bf16[128,2048]{1,0:T(8,128)(2,1)S(1)}, u32[]{:S(2)}, u32[]{:S(2)}) collective-permute-start(bf16[128,2048]{1,0:T(8,128)(2,1)S(1)} %constant_dynamic-update-slice_fusion.rows_ref), channel_id=1, source_target_pairs={{0,2},{2,4},{4,6},{6,8},{8,10},{10,12},{12,14},{14,16},{16,18},{18... | collective-permute-start | bytes 1572872 | tf_op jit(solution)/shard_map/ppermute | solution.py:17
  100.7 20.6 %collective-permute-start.8 = (bf16[64,2048]{1,0:T(8,128)(2,1)S(1)}, bf16[64,2048]{1,0:T(8,128)(2,1)S(1)}, u32[]{:S(2)}, u32[]{:S(2)}) collective-permute-start(bf16[64,2048]{1,0:T(8,128)(2,1)S(1)} %get-tuple-element.14), channel_id=1, source_target_pairs={{0,28},{2,30},{4,0},{6,2},{8,4},{10,6},{12,8},{14,10},{16,12},{18,... | collective-permute-start | bytes 786440 | tf_op jit(solution)/shard_map/ppermute | solution.py:17
  104.1 21.2 %collective-permute-start.9 = (bf16[64,2048]{1,0:T(8,128)(2,1)S(1)}, bf16[64,2048]{1,0:T(8,128)(2,1)S(1)}, u32[]{:S(2)}, u32[]{:S(2)}) collective-permute-start(bf16[64,2048]{1,0:T(8,128)(2,1)S(1)} %get-tuple-element.15), channel_id=1, source_target_pairs={{0,4},{2,6},{4,8},{6,10},{8,12},{10,14},{12,16},{14,18},{16,20},{1... | collective-permute-start | bytes 786440 | tf_op jit(solution)/shard_map/ppermute | solution.py:17
  127.5 30.2 %collective-permute-start.6 = (bf16[128,2048]{1,0:T(8,128)(2,1)S(1)}, bf16[128,2048]{1,0:T(8,128)(2,1)S(1)}, u32[]{:S(2)}, u32[]{:S(2)}) collective-permute-start(bf16[128,2048]{1,0:T(8,128)(2,1)S(1)} %get-tuple-element.10), channel_id=1, source_target_pairs={{0,2},{2,4},{4,6},{6,8},{8,10},{10,12},{12,14},{14,16},{16,18},{18... | collective-permute-start | bytes 1572872 | tf_op jit(solution)/shard_map/ppermute | solution.py:17
  132.2 25.4 %collective-permute-start.7 = (bf16[128,2048]{1,0:T(8,128)(2,1)S(1)}, bf16[128,2048]{1,0:T(8,128)(2,1)S(1)}, u32[]{:S(2)}, u32[]{:S(2)}) collective-permute-start(bf16[128,2048]{1,0:T(8,128)(2,1)S(1)} %get-tuple-element.11), channel_id=1, source_target_pairs={{0,30},{2,0},{4,2},{6,4},{8,6},{10,8},{12,10},{14,12},{16,14},{18,... | collective-permute-start | bytes 1572872 | tf_op jit(solution)/shard_map/ppermute | solution.py:17
  136.1 13.7 %collective-permute-start.10 = (bf16[64,2048]{1,0:T(8,128)(2,1)S(1)}, bf16[64,2048]{1,0:T(8,128)(2,1)S(1)}, u32[]{:S(2)}, u32[]{:S(2)}) collective-permute-start(bf16[64,2048]{1,0:T(8,128)(2,1)S(1)} %get-tuple-element.12), channel_id=1, source_target_pairs={{0,4},{2,6},{4,8},{6,10},{8,12},{10,14},{12,16},{14,18},{16,20},{1... | collective-permute-start | bytes 786440 | tf_op jit(solution)/shard_map/ppermute | solution.py:17
  139.1 18.6 %collective-permute-start.11 = (bf16[64,2048]{1,0:T(8,128)(2,1)S(1)}, bf16[64,2048]{1,0:T(8,128)(2,1)S(1)}, u32[]{:S(2)}, u32[]{:S(2)}) collective-permute-start(bf16[64,2048]{1,0:T(8,128)(2,1)S(1)} %get-tuple-element.13), channel_id=1, source_target_pairs={{0,28},{2,30},{4,0},{6,2},{8,4},{10,6},{12,8},{14,10},{16,12},{18,... | collective-permute-start | bytes 786440 | tf_op jit(solution)/shard_map/ppermute | solution.py:17
  157.8 24.3 %collective-permute-start.12 = (bf16[32,2048]{1,0:T(8,128)(2,1)S(1)}, bf16[32,2048]{1,0:T(8,128)(2,1)S(1)}, u32[]{:S(2)}, u32[]{:S(2)}) collective-permute-start(bf16[32,2048]{1,0:T(8,128)(2,1)S(1)} %get-tuple-element.7), channel_id=1, source_target_pairs={{0,16},{2,18},{4,20},{6,22},{8,24},{10,26},{12,28},{14,30},{16,0},... | collective-permute-start | bytes 393224 | tf_op jit(solution)/shard_map/ppermute | solution.py:17
  163.2 19.8 %collective-permute-start.13 = (bf16[32,2048]{1,0:T(8,128)(2,1)S(1)}, bf16[32,2048]{1,0:T(8,128)(2,1)S(1)}, u32[]{:S(2)}, u32[]{:S(2)}) collective-permute-start(bf16[32,2048]{1,0:T(8,128)(2,1)S(1)} %get-tuple-element.9), channel_id=1, source_target_pairs={{0,8},{2,10},{4,12},{6,14},{8,16},{10,18},{12,20},{14,22},{16,24},... | collective-permute-start | bytes 393224 | tf_op jit(solution)/shard_map/ppermute | solution.py:17
  170.5 17.8 %collective-permute-start.14 = (bf16[32,2048]{1,0:T(8,128)(2,1)S(1)}, bf16[32,2048]{1,0:T(8,128)(2,1)S(1)}, u32[]{:S(2)}, u32[]{:S(2)}) collective-permute-start(bf16[32,2048]{1,0:T(8,128)(2,1)S(1)} %get-tuple-element.8), channel_id=1, source_target_pairs={{0,24},{2,26},{4,28},{6,30},{8,0},{10,2},{12,4},{14,6},{16,8},{18,... | collective-permute-start | bytes 393224 | tf_op jit(solution)/shard_map/ppermute | solution.py:17

commit v3 on v2

v3 whole, which is shorter than its diff:
```python
import jax
import jax.numpy as jnp
from jax import lax
from jax.experimental import pallas as pl
from jax.experimental.pallas import tpu as pltpu
from jax.sharding import Mesh
from jax.sharding import PartitionSpec as P


TP = ("z", "c")
ROWS = ("fs", "z", "c")
VMEM = pl.BlockSpec(memory_space=pltpu.VMEM)
PARAMS = pltpu.CompilerParams(vmem_limit_bytes=32 * 1024 * 1024)


def local(kernel, outs, *args, flops=0, transcendentals=0):
    moved = sum(a.size * a.dtype.itemsize for a in (*args, *outs))
    return pl.pallas_call(
        kernel,
        out_shape=outs,
        in_specs=[VMEM] * len(args),
        out_specs=tuple(VMEM for _ in outs),
        compiler_params=PARAMS,
        cost_estimate=pl.CostEstimate(flops=flops, bytes_accessed=moved, transcendentals=transcendentals),
    )(*args)


def move(array, by):
    planes = lax.axis_size("z")
    return lax.ppermute(array, "z", [(i, (i + by) % planes) for i in range(planes)])


def copies_kernel(gain_hbm, gate_hbm, up_hbm, down_hbm, out_hbm, gain_ref, wide_ref, shard_ref, in_sems, out_sems):
    loads = [pltpu.make_async_copy(gain_hbm, gain_ref, in_sems.at[3])]
    for k, source in enumerate((gate_hbm, up_hbm, down_hbm)):
        loads.append(pltpu.make_async_copy(source, wide_ref.at[k], in_sems.at[k]))
    for load in loads:
        load.start()
    loads[0].wait()
    count = gate_hbm.shape[0]
    gain = jnp.transpose(jnp.broadcast_to(gain_ref[...], (count, count)))
    gain = jnp.concatenate([gain] * (gate_hbm.shape[1] // count), axis=1)
    stores = []
    for k in range(3):
        loads[1 + k].wait()
        value = wide_ref[k]
        shard_ref[k] = (value if k == 2 else gain * value).astype(jnp.bfloat16)
    for i in range(out_hbm.shape[0]):
        stores.append(pltpu.make_async_copy(shard_ref, out_hbm.at[i], out_sems.at[i]))
        stores[-1].start()
    for store in stores:
        store.wait()


def weight_copies(norm_gain, gate_master, up_master, down_master, count):
    shape = (3, *gate_master.shape)
    anywhere = pl.BlockSpec(memory_space=pltpu.HBM)
    return pl.pallas_call(
        copies_kernel,
        out_shape=jax.ShapeDtypeStruct((count, *shape), jnp.bfloat16),
        in_specs=[anywhere] * 4,
        out_specs=anywhere,
        scratch_shapes=[
            pltpu.VMEM((1, norm_gain.shape[0]), jnp.float32),
            pltpu.VMEM(shape, jnp.float32),
            pltpu.VMEM(shape, jnp.bfloat16),
            pltpu.SemaphoreType.DMA((4,)),
            pltpu.SemaphoreType.DMA((count,)),
        ],
        compiler_params=pltpu.CompilerParams(vmem_limit_bytes=66846720),
        cost_estimate=pl.CostEstimate(flops=1000000, bytes_accessed=4000000, transcendentals=0),
        name="prepare",
    )(norm_gain.reshape(1, -1), gate_master, up_master, down_master)


def pack_kernel(*refs):
    *parts, out_ref = refs
    at = 0
    for ref in parts:
        out_ref[at : at + ref.shape[0]] = ref[...]
        at += ref.shape[0]


def pack(*parts):
    count = sum(p.shape[0] for p in parts)
    return local(pack_kernel, (jax.ShapeDtypeStruct((count, parts[0].shape[1]), parts[0].dtype),), *parts)[0]


def sums_kernel(count, *refs):
    rows_refs, (own_ref, partner_ref), out_refs = refs[:count], refs[count : count + 2], refs[count + 2 :]
    rows = jnp.concatenate([ref[...] for ref in rows_refs], axis=0)
    width = rows.shape[1]
    wide = rows.astype(jnp.float32)
    row_scale = lax.rsqrt(jnp.mean(wide * wide, axis=1, keepdims=True) + 1e-06)
    hidden = []
    for ref in (own_ref, partner_ref):
        gate = ref[:, 0].reshape(width, -1)
        up = ref[:, 1].reshape(width, -1)
        gate_proj = row_scale * jnp.dot(rows, gate, preferred_element_type=jnp.float32)
        up_proj = row_scale * jnp.dot(rows, up, preferred_element_type=jnp.float32)
        hidden.append((gate_proj / (1.0 + jnp.exp(-gate_proj)) * up_proj).astype(jnp.bfloat16))
    total = None
    for ref, part in zip((own_ref, partner_ref), hidden):
        down = ref[:, 2].reshape(width, -1)
        share = lax.dot_general(part, down, (((1,), (1,)), ((), ())), preferred_element_type=jnp.float32)
        total = share if total is None else total + share
    at = 0
    for ref in out_refs:
        ref[...] = total[at : at + ref.shape[0]].astype(ref.dtype)
        at += ref.shape[0]


def partial_sums(parts, weights, outs, dtype):
    units = 2 * weights[0].shape[-1]
    count, width = sum(p.shape[0] for p in parts), parts[0].shape[1]
    return local(
        lambda *refs: sums_kernel(len(parts), *refs),
        tuple(jax.ShapeDtypeStruct((count // outs, width), dtype) for _ in range(outs)),
        *parts,
        *weights,
        flops=6 * count * width * units,
        transcendentals=count * units,
    )


def fold_kernel(terms, *refs):
    inputs, outputs = refs[: len(refs) - len(terms)], refs[len(refs) - len(terms) :]
    for out_ref, pairs in zip(outputs, terms):
        rows = out_ref.shape[0]
        total = None
        for which, k in pairs:
            value = inputs[which][k * rows : (k + 1) * rows].astype(jnp.float32)
            total = value if total is None else total + value
        out_ref[...] = total.astype(out_ref.dtype)


def mix_kernel(tokens_ref, own_ref, next_ref, prev_ref, next2_ref, prev2_ref, far_ref, above_ref, below_ref, out_ref):
    rows = tokens_ref.shape[0]
    total = own_ref[:rows]
    for ref in (next_ref, prev_ref, next2_ref, prev2_ref, far_ref, above_ref, below_ref):
        total = total + ref[:rows].astype(jnp.float32)
    out_ref[...] = (tokens_ref[...].astype(jnp.float32) + 0.5 * total).astype(out_ref.dtype)


def step(tokens, norm_gain, gate_master, up_master, down_master):
    far = move(tokens, 8)
    copies = weight_copies(norm_gain, gate_master, up_master, down_master, lax.axis_size("fs"))
    packed = lax.all_to_all(copies, "fs", split_axis=0, concat_axis=0, tiled=True)
    above = move(tokens, -4)
    below = move(tokens, 4)
    held = pack(tokens, far, above, below)
    from_next = move(held, -1)
    from_prev = move(held, 1)
    from_next2 = move(pack(tokens, above), -2)
    from_prev2 = move(pack(tokens, below), 2)

    partner = lax.ppermute(packed, "c", [(0, 1), (1, 0)])
    weights = (packed, partner)

    ones_next, ones_prev = partial_sums((from_next, from_prev), weights, 2, jnp.bfloat16)
    to_next = move(ones_next, 1)
    to_prev = move(ones_prev, -1)
    twos_next, twos_prev = partial_sums((from_next2, from_prev2), weights, 2, jnp.bfloat16)
    to_next2 = move(twos_next, 2)
    to_prev2 = move(twos_prev, -2)
    (own,) = partial_sums((held,), weights, 1, jnp.float32)

    block = jax.ShapeDtypeStruct(tokens.shape, jnp.bfloat16)
    (sum_far,) = local(lambda *refs: fold_kernel((((0, 1), (1, 1), (2, 1)),), *refs), (block,), own, to_next, to_prev)
    back_far = move(sum_far, 8)
    terms = (((0, 2), (1, 2), (2, 2), (3, 1)), ((0, 3), (1, 3), (2, 3), (4, 1)))
    sum_above, sum_below = local(lambda *refs: fold_kernel(terms, *refs), (block, block), own, to_next, to_prev, to_next2, to_prev2)
    back_above = move(sum_above, 4)
    back_below = move(sum_below, -4)
    (mixed,) = local(mix_kernel, (block,), tokens, own, to_next, to_prev, to_next2, to_prev2, back_far, back_above, back_below)
    return (mixed, *(packed[:, k].reshape(-1, packed.shape[-1]) for k in range(3)))


def solution(mesh):
    split = Mesh(mesh.devices.reshape(mesh.shape["fs"], 16, 2), ROWS)
    placed = (P(ROWS, None), P("fs"), P("fs", TP), P("fs", TP), P("fs", TP))
    return jax.shard_map(
        step,
        mesh=split,
        in_specs=placed,
        out_specs=(P(ROWS, None), P(None, TP), P(None, TP), P(None, TP)),
        check_vma=False,
    )
```

time: 193 us -> 184 us (0.953)
  the two profiles are of different devices: /device:TPU:6 before, /device:TPU:64 now
where the time goes in v3:
time: 184 us
  starting transfers between devices  78 us (42%)
  waiting for transfers between devices  47.6 us (26%)
  blocking collectives  46.8 us (25%)
  Pallas kernels  8.74 us (5%)
    ppermute x14, starting transfers between devices, move(): lax.ppermute(array, 'z', [(i, (i + by) % planes) for i in range(planes)])  76.1 us
    ppermute x14, waiting for transfers between devices, move(): lax.ppermute(array, 'z', [(i, (i + by) % planes) for i in range(planes)])  47.6 us
    all_to_all x1, blocking collectives, step(): lax.all_to_all(copies, 'fs', split_axis=0, concat_axis=0, tiled=True)  46.8 us
    pallas_call x9, Pallas kernels, local(): pl.pallas_call(kernel, out_shape=outs, in_specs=[VMEM] * len(args), out_s...  5.87 us
  transfers between devices with their start and end apart: 15, of which 7 were waited for; matrix products, arithmetic and copies ran while one was open for 1% of the time, Pallas kernels for 3%

profile of v3, /device:TPU:64, one launch (start us, length us, event | category | flops | bytes accessed | tf_op | source)
XLA Modules:
  0.0 183.7 jit_solution(17908554669521742272)
XLA Ops:
  0.6 2.9 %prepare.1 = bf16[16,3,128,256]{3,2,1,0:T(8,128)(2,1)} custom-call(f32[1,128]{1,0:T(1,128)} %bitcast.7, f32[128,256]{1,0:T(8,128)} %gate_hbm.1, f32[128,256]{1,0:T(8,128)} %up_hbm.1, f32[128,256]{1,0:T(8,128)} %down_hbm.1), custom_call_target="tpu_custom_call" | custom-call | flops 1000000 | bytes 4000000 | tf_op jit(solution)/shard_map/prepare/pallas_call | solution.py:58
  3.5 0.0 copy-start
  3.5 46.8 %all_to_all.5.refs_1_.refs_2_ = bf16[16,3,128,256]{3,2,1,0:T(8,128)(2,1)S(1)} all-to-all(bf16[16,3,128,256]{3,2,1,0:T(8,128)(2,1)} %prepare.1), channel_id=1, replica_groups=mesh['fs'=16,'z'=16,'c'=2] {'fs'}, dimensions={0} | all-to-all | bytes 6291456 | tf_op jit(solution)/shard_map/all_to_all | solution.py:148
  50.3 1.9 %collective-permute-start.3 = (bf16[16,3,128,256]{3,2,1,0:T(8,128)(2,1)S(1)}, bf16[16,3,128,256]{3,2,1,0:T(8,128)(2,1)S(1)}, u32[]{:S(2)}, u32[]{:S(2)}) collective-permute-start(bf16[16,3,128,256]{3,2,1,0:T(8,128)(2,1)S(1)} %all_to_all.5.refs_1_.refs_2_), channel_id=1, source_target_pairs={{0,1},{1,0},{2,3},{3,2},{4,5},{5,4},{6,7},{7,6},{8,9},{9,8},{10,11... | collective-permute-start | bytes 9437192 | tf_op jit(solution)/shard_map/ppermute | solution.py:157
  52.2 0.0 copy-done
  52.2 10.9 %collective-permute-start.1 = (bf16[32,2048]{1,0:T(8,128)(2,1)S(1)}, bf16[32,2048]{1,0:T(8,128)(2,1)S(1)}, u32[]{:S(2)}, u32[]{:S(2)}) collective-permute-start(bf16[32,2048]{1,0:T(8,128)(2,1)S(1)} %copy-done), channel_id=1, source_target_pairs={{0,24},{2,26},{4,28},{6,30},{8,0},{10,2},{12,4},{14,6},{16,8},{18,... | collective-permute-start | bytes 393224 | tf_op jit(solution)/shard_map/ppermute | solution.py:30
  63.2 1.9 %collective-permute-start.2 = (bf16[32,2048]{1,0:T(8,128)(2,1)S(1)}, bf16[32,2048]{1,0:T(8,128)(2,1)S(1)}, u32[]{:S(2)}, u32[]{:S(2)}) collective-permute-start(bf16[32,2048]{1,0:T(8,128)(2,1)S(1)} %copy-done), channel_id=1, source_target_pairs={{0,8},{2,10},{4,12},{6,14},{8,16},{10,18},{12,20},{14,22},{16,24},... | collective-permute-start | bytes 393224 | tf_op jit(solution)/shard_map/ppermute | solution.py:30
  65.1 10.8 %collective-permute-start = (bf16[32,2048]{1,0:T(8,128)(2,1)S(1)}, bf16[32,2048]{1,0:T(8,128)(2,1)S(1)}, u32[]{:S(2)}, u32[]{:S(2)}) collective-permute-start(bf16[32,2048]{1,0:T(8,128)(2,1)S(1)} %copy-done), channel_id=1, source_target_pairs={{0,16},{2,18},{4,20},{6,22},{8,24},{10,26},{12,28},{14,30},{16,0},... | collective-permute-start | bytes 393224 | tf_op jit(solution)/shard_map/ppermute | solution.py:30
  75.9 0.0 collective-permute-done.1.refs_2_.refs_1_
  76.0 8.2 %collective-permute-done.2.refs_3_.refs_1_ = bf16[32,2048]{1,0:T(8,128)(2,1)S(1)} collective-permute-done((bf16[32,2048]{1,0:T(8,128)(2,1)S(1)}, bf16[32,2048]{1,0:T(8,128)(2,1)S(1)}, u32[]{:S(2)}, u32[]{:S(2)}) %collective-permute-start.2) | collective-permute-done | bytes 131104 | tf_op jit(solution)/shard_map/ppermute | solution.py:30
  84.1 8.1 %collective-permute-done.refs_1_ = bf16[32,2048]{1,0:T(8,128)(2,1)S(1)} collective-permute-done((bf16[32,2048]{1,0:T(8,128)(2,1)S(1)}, bf16[32,2048]{1,0:T(8,128)(2,1)S(1)}, u32[]{:S(2)}, u32[]{:S(2)}) %collective-permute-start) | collective-permute-done | bytes 131104 | tf_op jit(solution)/shard_map/ppermute | solution.py:30
  92.2 1.9 %collective-permute-start.4 = (bf16[128,2048]{1,0:T(8,128)(2,1)S(1)}, bf16[128,2048]{1,0:T(8,128)(2,1)S(1)}, u32[]{:S(2)}, u32[]{:S(2)}) collective-permute-start(bf16[128,2048]{1,0:T(8,128)(2,1)S(1)} %shard_map.84.refs_0_), channel_id=1, source_target_pairs={{0,30},{2,0},{4,2},{6,4},{8,6},{10,8},{12,10},{14,12},{16,14},{18,... | collective-permute-start | bytes 1572872 | tf_op jit(solution)/shard_map/ppermute | solution.py:30
  94.2 3.9 %collective-permute-start.5 = (bf16[128,2048]{1,0:T(8,128)(2,1)S(1)}, bf16[128,2048]{1,0:T(8,128)(2,1)S(1)}, u32[]{:S(2)}, u32[]{:S(2)}) collective-permute-start(bf16[128,2048]{1,0:T(8,128)(2,1)S(1)} %shard_map.84.refs_0_), channel_id=1, source_target_pairs={{0,2},{2,4},{4,6},{6,8},{8,10},{10,12},{12,14},{14,16},{16,18},{18... | collective-permute-start | bytes 1572872 | tf_op jit(solution)/shard_map/ppermute | solution.py:30
  98.1 7.6 %collective-permute-start.8 = (bf16[64,2048]{1,0:T(8,128)(2,1)S(1)}, bf16[64,2048]{1,0:T(8,128)(2,1)S(1)}, u32[]{:S(2)}, u32[]{:S(2)}) collective-permute-start(bf16[64,2048]{1,0:T(8,128)(2,1)S(1)} %shard_map.87), channel_id=1, source_target_pairs={{0,28},{2,30},{4,0},{6,2},{8,4},{10,6},{12,8},{14,10},{16,12},{18,... | collective-permute-start | bytes 786440 | tf_op jit(solution)/shard_map/ppermute | solution.py:30
  105.8 1.9 %collective-permute-start.9 = (bf16[64,2048]{1,0:T(8,128)(2,1)S(1)}, bf16[64,2048]{1,0:T(8,128)(2,1)S(1)}, u32[]{:S(2)}, u32[]{:S(2)}) collective-permute-start(bf16[64,2048]{1,0:T(8,128)(2,1)S(1)} %shard_map.88), channel_id=1, source_target_pairs={{0,4},{2,6},{4,8},{6,10},{8,12},{10,14},{12,16},{14,18},{16,20},{1... | collective-permute-start | bytes 786440 | tf_op jit(solution)/shard_map/ppermute | solution.py:30
  107.7 1.0 collective-permute-done.4.refs_0_
  108.7 8.2 %collective-permute-done.5.refs_1_ = bf16[128,2048]{1,0:T(8,128)(2,1)S(1)} collective-permute-done((bf16[128,2048]{1,0:T(8,128)(2,1)S(1)}, bf16[128,2048]{1,0:T(8,128)(2,1)S(1)}, u32[]{:S(2)}, u32[]{:S(2)}) %collective-permute-start.5) | collective-permute-done | bytes 524320 | tf_op jit(solution)/shard_map/ppermute | solution.py:30
  116.9 0.0 collective-permute-done.3.refs_2_.refs_3_
  116.9 1.9 %shard_map.86 = (bf16[128,2048]{1,0:T(8,128)(2,1)S(1)}, bf16[128,2048]{1,0:T(8,128)(2,1)S(1)}) custom-call(bf16[128,2048]{1,0:T(8,128)(2,1)S(1)} %collective-permute-done.4.refs_0_, bf16[128,2048]{1,0:T(8,128)(2,1)S(1)} %collective-permute-done.5.refs_1_, bf16[16,3,128,256]{3,2,1,0:T(8,128)(2,1)S(1)} %all_to_all.5.refs_1_.refs_2_, ...), custom_call_target="tpu_custom_call" | custom-call | flops 1610612736 | bytes 8388608 | tf_op jit(solution)/shard_map/pallas_call | solution.py:18
  118.9 2.4 %collective-permute-start.6 = (bf16[128,2048]{1,0:T(8,128)(2,1)S(1)}, bf16[128,2048]{1,0:T(8,128)(2,1)S(1)}, u32[]{:S(2)}, u32[]{:S(2)}) collective-permute-start(bf16[128,2048]{1,0:T(8,128)(2,1)S(1)} %get-tuple-element.10), channel_id=1, source_target_pairs={{0,2},{2,4},{4,6},{6,8},{8,10},{10,12},{12,14},{14,16},{16,18},{18... | collective-permute-start | bytes 1572872 | tf_op jit(solution)/shard_map/ppermute | solution.py:30
  121.2 3.5 %collective-permute-start.7 = (bf16[128,2048]{1,0:T(8,128)(2,1)S(1)}, bf16[128,2048]{1,0:T(8,128)(2,1)S(1)}, u32[]{:S(2)}, u32[]{:S(2)}) collective-permute-start(bf16[128,2048]{1,0:T(8,128)(2,1)S(1)} %get-tuple-element.11), channel_id=1, source_target_pairs={{0,30},{2,0},{4,2},{6,4},{8,6},{10,8},{12,10},{14,12},{16,14},{18,... | collective-permute-start | bytes 1572872 | tf_op jit(solution)/shard_map/ppermute | solution.py:30
  124.7 0.0 collective-permute-done.8.refs_0_
  124.7 0.0 collective-permute-done.9.refs_1_
  124.7 1.5 shard_map.89
  126.2 6.8 %collective-permute-start.10 = (bf16[64,2048]{1,0:T(8,128)(2,1)S(1)}, bf16[64,2048]{1,0:T(8,128)(2,1)S(1)}, u32[]{:S(2)}, u32[]{:S(2)}) collective-permute-start(bf16[64,2048]{1,0:T(8,128)(2,1)S(1)} %get-tuple-element.12), channel_id=1, source_target_pairs={{0,4},{2,6},{4,8},{6,10},{8,12},{10,14},{12,16},{14,18},{16,20},{1... | collective-permute-start | bytes 786440 | tf_op jit(solution)/shard_map/ppermute | solution.py:30
  133.0 4.6 %collective-permute-start.11 = (bf16[64,2048]{1,0:T(8,128)(2,1)S(1)}, bf16[64,2048]{1,0:T(8,128)(2,1)S(1)}, u32[]{:S(2)}, u32[]{:S(2)}) collective-permute-start(bf16[64,2048]{1,0:T(8,128)(2,1)S(1)} %get-tuple-element.13), channel_id=1, source_target_pairs={{0,28},{2,30},{4,0},{6,2},{8,4},{10,6},{12,8},{14,10},{16,12},{18,... | collective-permute-start | bytes 786440 | tf_op jit(solution)/shard_map/ppermute | solution.py:30
  137.7 1.5 shard_map.85.refs_0_.own_ref
  139.1 6.5 %collective-permute-done.10.refs_3_.next2_ref = bf16[64,2048]{1,0:T(8,128)(2,1)S(1)} collective-permute-done((bf16[64,2048]{1,0:T(8,128)(2,1)S(1)}, bf16[64,2048]{1,0:T(8,128)(2,1)S(1)}, u32[]{:S(2)}, u32[]{:S(2)}) %collective-permute-start.10) | collective-permute-done | bytes 262176 | tf_op jit(solution)/shard_map/ppermute | solution.py:30
  145.7 2.0 %collective-permute-done.11.refs_4_.prev2_ref = bf16[64,2048]{1,0:T(8,128)(2,1)S(1)} collective-permute-done((bf16[64,2048]{1,0:T(8,128)(2,1)S(1)}, bf16[64,2048]{1,0:T(8,128)(2,1)S(1)}, u32[]{:S(2)}, u32[]{:S(2)}) %collective-permute-start.11) | collective-permute-done | bytes 262176 | tf_op jit(solution)/shard_map/ppermute | solution.py:30
  147.7 0.0 collective-permute-done.6.refs_1_.next_ref
  147.7 0.0 collective-permute-done.7.refs_2_.prev_ref
  147.7 0.1 shard_map.91
  147.8 10.5 %collective-permute-start.13 = (bf16[32,2048]{1,0:T(8,128)(2,1)S(1)}, bf16[32,2048]{1,0:T(8,128)(2,1)S(1)}, u32[]{:S(2)}, u32[]{:S(2)}) collective-permute-start(bf16[32,2048]{1,0:T(8,128)(2,1)S(1)} %get-tuple-element.14), channel_id=1, source_target_pairs={{0,8},{2,10},{4,12},{6,14},{8,16},{10,18},{12,20},{14,22},{16,24},... | collective-permute-start | bytes 393224 | tf_op jit(solution)/shard_map/ppermute | solution.py:30
  158.4 1.9 %collective-permute-start.14 = (bf16[32,2048]{1,0:T(8,128)(2,1)S(1)}, bf16[32,2048]{1,0:T(8,128)(2,1)S(1)}, u32[]{:S(2)}, u32[]{:S(2)}) collective-permute-start(bf16[32,2048]{1,0:T(8,128)(2,1)S(1)} %get-tuple-element.15), channel_id=1, source_target_pairs={{0,24},{2,26},{4,28},{6,30},{8,0},{10,2},{12,4},{14,6},{16,8},{18,... | collective-permute-start | bytes 393224 | tf_op jit(solution)/shard_map/ppermute | solution.py:30
  160.3 7.3 %collective-permute-start.12 = (bf16[32,2048]{1,0:T(8,128)(2,1)S(1)}, bf16[32,2048]{1,0:T(8,128)(2,1)S(1)}, u32[]{:S(2)}, u32[]{:S(2)}) collective-permute-start(bf16[32,2048]{1,0:T(8,128)(2,1)S(1)} %shard_map.90), channel_id=1, source_target_pairs={{0,16},{2,18},{4,20},{6,22},{8,24},{10,26},{12,28},{14,30},{16,0},... | collective-permute-start | bytes 393224 | tf_op jit(solution)/shard_map/ppermute | solution.py:30
  167.6 1.8 fusion
  169.4 0.0 collective-permute-done.13.above_ref
  169.4 13.5 %collective-permute-done.14.below_ref = bf16[32,2048]{1,0:T(8,128)(2,1)S(1)} collective-permute-done((bf16[32,2048]{1,0:T(8,128)(2,1)S(1)}, bf16[32,2048]{1,0:T(8,128)(2,1)S(1)}, u32[]{:S(2)}, u32[]{:S(2)}) %collective-permute-start.14) | collective-permute-done | bytes 131104 | tf_op jit(solution)/shard_map/ppermute | solution.py:30
  182.9 0.0 collective-permute-done.12.far_ref
  182.9 0.8 shard_map.92
  (4 shorter events, 0.1 us)
Async XLA Ops:
  3.5 48.7 %copy-start = (bf16[32,2048]{1,0:T(8,128)(2,1)S(1)}, bf16[32,2048]{1,0:T(8,128)(2,1)}, u32[]{:S(2)}) copy-start(bf16[32,2048]{1,0:T(8,128)(2,1)} %tokens_ref.1) | copy-start | bytes 393220
  50.3 66.6 %collective-permute-start.3 = (bf16[16,3,128,256]{3,2,1,0:T(8,128)(2,1)S(1)}, bf16[16,3,128,256]{3,2,1,0:T(8,128)(2,1)S(1)}, u32[]{:S(2)}, u32[]{:S(2)}) collective-permute-start(bf16[16,3,128,256]{3,2,1,0:T(8,128)(2,1)S(1)} %all_to_all.5.refs_1_.refs_2_), channel_id=1, source_target_pairs={{0,1},{1,0},{2,3},{3,2},{4,5},{5,4},{6,7},{7,6},{8,9},{9,8},{10,11... | collective-permute-start | bytes 9437192 | tf_op jit(solution)/shard_map/ppermute | solution.py:157
  52.2 23.7 %collective-permute-start.1 = (bf16[32,2048]{1,0:T(8,128)(2,1)S(1)}, bf16[32,2048]{1,0:T(8,128)(2,1)S(1)}, u32[]{:S(2)}, u32[]{:S(2)}) collective-permute-start(bf16[32,2048]{1,0:T(8,128)(2,1)S(1)} %copy-done), channel_id=1, source_target_pairs={{0,24},{2,26},{4,28},{6,30},{8,0},{10,2},{12,4},{14,6},{16,8},{18,... | collective-permute-start | bytes 393224 | tf_op jit(solution)/shard_map/ppermute | solution.py:30
  63.2 20.9 %collective-permute-start.2 = (bf16[32,2048]{1,0:T(8,128)(2,1)S(1)}, bf16[32,2048]{1,0:T(8,128)(2,1)S(1)}, u32[]{:S(2)}, u32[]{:S(2)}) collective-permute-start(bf16[32,2048]{1,0:T(8,128)(2,1)S(1)} %copy-done), channel_id=1, source_target_pairs={{0,8},{2,10},{4,12},{6,14},{8,16},{10,18},{12,20},{14,22},{16,24},... | collective-permute-start | bytes 393224 | tf_op jit(solution)/shard_map/ppermute | solution.py:30
  65.1 27.1 %collective-permute-start = (bf16[32,2048]{1,0:T(8,128)(2,1)S(1)}, bf16[32,2048]{1,0:T(8,128)(2,1)S(1)}, u32[]{:S(2)}, u32[]{:S(2)}) collective-permute-start(bf16[32,2048]{1,0:T(8,128)(2,1)S(1)} %copy-done), channel_id=1, source_target_pairs={{0,16},{2,18},{4,20},{6,22},{8,24},{10,26},{12,28},{14,30},{16,0},... | collective-permute-start | bytes 393224 | tf_op jit(solution)/shard_map/ppermute | solution.py:30
  92.2 16.5 %collective-permute-start.4 = (bf16[128,2048]{1,0:T(8,128)(2,1)S(1)}, bf16[128,2048]{1,0:T(8,128)(2,1)S(1)}, u32[]{:S(2)}, u32[]{:S(2)}) collective-permute-start(bf16[128,2048]{1,0:T(8,128)(2,1)S(1)} %shard_map.84.refs_0_), channel_id=1, source_target_pairs={{0,30},{2,0},{4,2},{6,4},{8,6},{10,8},{12,10},{14,12},{16,14},{18,... | collective-permute-start | bytes 1572872 | tf_op jit(solution)/shard_map/ppermute | solution.py:30
  94.2 22.7 %collective-permute-start.5 = (bf16[128,2048]{1,0:T(8,128)(2,1)S(1)}, bf16[128,2048]{1,0:T(8,128)(2,1)S(1)}, u32[]{:S(2)}, u32[]{:S(2)}) collective-permute-start(bf16[128,2048]{1,0:T(8,128)(2,1)S(1)} %shard_map.84.refs_0_), channel_id=1, source_target_pairs={{0,2},{2,4},{4,6},{6,8},{8,10},{10,12},{12,14},{14,16},{16,18},{18... | collective-permute-start | bytes 1572872 | tf_op jit(solution)/shard_map/ppermute | solution.py:30
  98.1 26.6 %collective-permute-start.8 = (bf16[64,2048]{1,0:T(8,128)(2,1)S(1)}, bf16[64,2048]{1,0:T(8,128)(2,1)S(1)}, u32[]{:S(2)}, u32[]{:S(2)}) collective-permute-start(bf16[64,2048]{1,0:T(8,128)(2,1)S(1)} %shard_map.87), channel_id=1, source_target_pairs={{0,28},{2,30},{4,0},{6,2},{8,4},{10,6},{12,8},{14,10},{16,12},{18,... | collective-permute-start | bytes 786440 | tf_op jit(solution)/shard_map/ppermute | solution.py:30
  105.8 18.9 %collective-permute-start.9 = (bf16[64,2048]{1,0:T(8,128)(2,1)S(1)}, bf16[64,2048]{1,0:T(8,128)(2,1)S(1)}, u32[]{:S(2)}, u32[]{:S(2)}) collective-permute-start(bf16[64,2048]{1,0:T(8,128)(2,1)S(1)} %shard_map.88), channel_id=1, source_target_pairs={{0,4},{2,6},{4,8},{6,10},{8,12},{10,14},{12,16},{14,18},{16,20},{1... | collective-permute-start | bytes 786440 | tf_op jit(solution)/shard_map/ppermute | solution.py:30
  118.9 28.8 %collective-permute-start.6 = (bf16[128,2048]{1,0:T(8,128)(2,1)S(1)}, bf16[128,2048]{1,0:T(8,128)(2,1)S(1)}, u32[]{:S(2)}, u32[]{:S(2)}) collective-permute-start(bf16[128,2048]{1,0:T(8,128)(2,1)S(1)} %get-tuple-element.10), channel_id=1, source_target_pairs={{0,2},{2,4},{4,6},{6,8},{8,10},{10,12},{12,14},{14,16},{16,18},{18... | collective-permute-start | bytes 1572872 | tf_op jit(solution)/shard_map/ppermute | solution.py:30
  121.2 26.5 %collective-permute-start.7 = (bf16[128,2048]{1,0:T(8,128)(2,1)S(1)}, bf16[128,2048]{1,0:T(8,128)(2,1)S(1)}, u32[]{:S(2)}, u32[]{:S(2)}) collective-permute-start(bf16[128,2048]{1,0:T(8,128)(2,1)S(1)} %get-tuple-element.11), channel_id=1, source_target_pairs={{0,30},{2,0},{4,2},{6,4},{8,6},{10,8},{12,10},{14,12},{16,14},{18,... | collective-permute-start | bytes 1572872 | tf_op jit(solution)/shard_map/ppermute | solution.py:30
  126.2 19.5 %collective-permute-start.10 = (bf16[64,2048]{1,0:T(8,128)(2,1)S(1)}, bf16[64,2048]{1,0:T(8,128)(2,1)S(1)}, u32[]{:S(2)}, u32[]{:S(2)}) collective-permute-start(bf16[64,2048]{1,0:T(8,128)(2,1)S(1)} %get-tuple-element.12), channel_id=1, source_target_pairs={{0,4},{2,6},{4,8},{6,10},{8,12},{10,14},{12,16},{14,18},{16,20},{1... | collective-permute-start | bytes 786440 | tf_op jit(solution)/shard_map/ppermute | solution.py:30
  133.0 14.7 %collective-permute-start.11 = (bf16[64,2048]{1,0:T(8,128)(2,1)S(1)}, bf16[64,2048]{1,0:T(8,128)(2,1)S(1)}, u32[]{:S(2)}, u32[]{:S(2)}) collective-permute-start(bf16[64,2048]{1,0:T(8,128)(2,1)S(1)} %get-tuple-element.13), channel_id=1, source_target_pairs={{0,28},{2,30},{4,0},{6,2},{8,4},{10,6},{12,8},{14,10},{16,12},{18,... | collective-permute-start | bytes 786440 | tf_op jit(solution)/shard_map/ppermute | solution.py:30
  147.8 21.6 %collective-permute-start.13 = (bf16[32,2048]{1,0:T(8,128)(2,1)S(1)}, bf16[32,2048]{1,0:T(8,128)(2,1)S(1)}, u32[]{:S(2)}, u32[]{:S(2)}) collective-permute-start(bf16[32,2048]{1,0:T(8,128)(2,1)S(1)} %get-tuple-element.14), channel_id=1, source_target_pairs={{0,8},{2,10},{4,12},{6,14},{8,16},{10,18},{12,20},{14,22},{16,24},... | collective-permute-start | bytes 393224 | tf_op jit(solution)/shard_map/ppermute | solution.py:30
  158.4 24.5 %collective-permute-start.14 = (bf16[32,2048]{1,0:T(8,128)(2,1)S(1)}, bf16[32,2048]{1,0:T(8,128)(2,1)S(1)}, u32[]{:S(2)}, u32[]{:S(2)}) collective-permute-start(bf16[32,2048]{1,0:T(8,128)(2,1)S(1)} %get-tuple-element.15), channel_id=1, source_target_pairs={{0,24},{2,26},{4,28},{6,30},{8,0},{10,2},{12,4},{14,6},{16,8},{18,... | collective-permute-start | bytes 393224 | tf_op jit(solution)/shard_map/ppermute | solution.py:30
  160.3 22.6 %collective-permute-start.12 = (bf16[32,2048]{1,0:T(8,128)(2,1)S(1)}, bf16[32,2048]{1,0:T(8,128)(2,1)S(1)}, u32[]{:S(2)}, u32[]{:S(2)}) collective-permute-start(bf16[32,2048]{1,0:T(8,128)(2,1)S(1)} %shard_map.90), channel_id=1, source_target_pairs={{0,16},{2,18},{4,20},{6,22},{8,24},{10,26},{12,28},{14,30},{16,0},... | collective-permute-start | bytes 393224 | tf_op jit(solution)/shard_map/ppermute | solution.py:30

commit v4 on v3

--- a/solution.py
+++ b/solution.py
@@ -81,6 +81,12 @@
         at += ref.shape[0]
 
 
+def pack_pairs_kernel(first_ref, *refs):
+    parts, out_refs = refs[: len(refs) // 2], refs[len(refs) // 2 :]
+    for ref, out_ref in zip(parts, out_refs):
+        pack_kernel(first_ref, ref, out_ref)
+
+
 def pack(*parts):
     count = sum(p.shape[0] for p in parts)
     return local(pack_kernel, (jax.ShapeDtypeStruct((count, parts[0].shape[1]), parts[0].dtype),), *parts)[0]
@@ -143,16 +149,18 @@
 
 
 def step(tokens, norm_gain, gate_master, up_master, down_master):
-    far = move(tokens, 8)
     copies = weight_copies(norm_gain, gate_master, up_master, down_master, lax.axis_size("fs"))
     packed = lax.all_to_all(copies, "fs", split_axis=0, concat_axis=0, tiled=True)
     above = move(tokens, -4)
     below = move(tokens, 4)
+    far = move(tokens, 8)
+    pair = jax.ShapeDtypeStruct((2 * tokens.shape[0], tokens.shape[1]), tokens.dtype)
+    pair_above, pair_below = local(pack_pairs_kernel, (pair, pair), tokens, above, below)
+    from_next2 = move(pair_above, -2)
+    from_prev2 = move(pair_below, 2)
     held = pack(tokens, far, above, below)
     from_next = move(held, -1)
     from_prev = move(held, 1)
-    from_next2 = move(pack(tokens, above), -2)
-    from_prev2 = move(pack(tokens, below), 2)
 
     partner = lax.ppermute(packed, "c", [(0, 1), (1, 0)])
     weights = (packed, partner)

time: 184 us -> 184 us (level)
    pallas_call x9 -> x8, Pallas kernels: 5.87 us -> 5.86 us  [local(): pl.pallas_call(kernel, out_shape=outs, in_specs=[VMEM] * len(args), out_s...]
where the time goes in v4:
time: 184 us
  starting transfers between devices  78 us (42%)
  waiting for transfers between devices  47.6 us (26%)
  blocking collectives  46.8 us (25%)
  Pallas kernels  8.74 us (5%)
    ppermute x14, starting transfers between devices, move(): lax.ppermute(array, 'z', [(i, (i + by) % planes) for i in range(planes)])  76.1 us
    ppermute x14, waiting for transfers between devices, move(): lax.ppermute(array, 'z', [(i, (i + by) % planes) for i in range(planes)])  47.6 us
    all_to_all x1, blocking collectives, step(): lax.all_to_all(copies, 'fs', split_axis=0, concat_axis=0, tiled=True)  46.8 us
    pallas_call x8, Pallas kernels, local(): pl.pallas_call(kernel, out_shape=outs, in_specs=[VMEM] * len(args), out_s...  5.86 us
  transfers between devices with their start and end apart: 15, of which 7 were waited for; matrix products, arithmetic and copies ran while one was open for 1% of the time, Pallas kernels for 3%

profile of v4, /device:TPU:64, one launch (start us, length us, event | category | flops | bytes accessed | tf_op | source)
XLA Modules:
  0.0 183.7 jit_solution(5653125651876330282)
XLA Ops:
  0.6 2.9 %prepare.1 = bf16[16,3,128,256]{3,2,1,0:T(8,128)(2,1)} custom-call(f32[1,128]{1,0:T(1,128)} %bitcast.7, f32[128,256]{1,0:T(8,128)} %gate_hbm.1, f32[128,256]{1,0:T(8,128)} %up_hbm.1, f32[128,256]{1,0:T(8,128)} %down_hbm.1), custom_call_target="tpu_custom_call" | custom-call | flops 1000000 | bytes 4000000 | tf_op jit(solution)/shard_map/prepare/pallas_call | solution.py:58
  3.5 0.0 copy-start
  3.5 46.8 %all_to_all.5.refs_1_.refs_2_ = bf16[16,3,128,256]{3,2,1,0:T(8,128)(2,1)S(1)} all-to-all(bf16[16,3,128,256]{3,2,1,0:T(8,128)(2,1)} %prepare.1), channel_id=1, replica_groups=mesh['fs'=16,'z'=16,'c'=2] {'fs'}, dimensions={0} | all-to-all | bytes 6291456 | tf_op jit(solution)/shard_map/all_to_all | solution.py:153
  50.3 1.9 %collective-permute-start.3 = (bf16[16,3,128,256]{3,2,1,0:T(8,128)(2,1)S(1)}, bf16[16,3,128,256]{3,2,1,0:T(8,128)(2,1)S(1)}, u32[]{:S(2)}, u32[]{:S(2)}) collective-permute-start(bf16[16,3,128,256]{3,2,1,0:T(8,128)(2,1)S(1)} %all_to_all.5.refs_1_.refs_2_), channel_id=1, source_target_pairs={{0,1},{1,0},{2,3},{3,2},{4,5},{5,4},{6,7},{7,6},{8,9},{9,8},{10,11... | collective-permute-start | bytes 9437192 | tf_op jit(solution)/shard_map/ppermute | solution.py:165
  52.3 0.0 copy-done
  52.3 10.9 %collective-permute-start.1 = (bf16[32,2048]{1,0:T(8,128)(2,1)S(1)}, bf16[32,2048]{1,0:T(8,128)(2,1)S(1)}, u32[]{:S(2)}, u32[]{:S(2)}) collective-permute-start(bf16[32,2048]{1,0:T(8,128)(2,1)S(1)} %copy-done), channel_id=1, source_target_pairs={{0,24},{2,26},{4,28},{6,30},{8,0},{10,2},{12,4},{14,6},{16,8},{18,... | collective-permute-start | bytes 393224 | tf_op jit(solution)/shard_map/ppermute | solution.py:30
  63.2 1.9 %collective-permute-start.2 = (bf16[32,2048]{1,0:T(8,128)(2,1)S(1)}, bf16[32,2048]{1,0:T(8,128)(2,1)S(1)}, u32[]{:S(2)}, u32[]{:S(2)}) collective-permute-start(bf16[32,2048]{1,0:T(8,128)(2,1)S(1)} %copy-done), channel_id=1, source_target_pairs={{0,8},{2,10},{4,12},{6,14},{8,16},{10,18},{12,20},{14,22},{16,24},... | collective-permute-start | bytes 393224 | tf_op jit(solution)/shard_map/ppermute | solution.py:30
  65.1 10.8 %collective-permute-start = (bf16[32,2048]{1,0:T(8,128)(2,1)S(1)}, bf16[32,2048]{1,0:T(8,128)(2,1)S(1)}, u32[]{:S(2)}, u32[]{:S(2)}) collective-permute-start(bf16[32,2048]{1,0:T(8,128)(2,1)S(1)} %copy-done), channel_id=1, source_target_pairs={{0,16},{2,18},{4,20},{6,22},{8,24},{10,26},{12,28},{14,30},{16,0},... | collective-permute-start | bytes 393224 | tf_op jit(solution)/shard_map/ppermute | solution.py:30
  76.0 0.0 collective-permute-done.1.refs_2_.refs_0_
  76.0 8.2 %collective-permute-done.2.refs_3_.refs_1_ = bf16[32,2048]{1,0:T(8,128)(2,1)S(1)} collective-permute-done((bf16[32,2048]{1,0:T(8,128)(2,1)S(1)}, bf16[32,2048]{1,0:T(8,128)(2,1)S(1)}, u32[]{:S(2)}, u32[]{:S(2)}) %collective-permute-start.2) | collective-permute-done | bytes 131104 | tf_op jit(solution)/shard_map/ppermute | solution.py:30
  84.1 8.1 %collective-permute-done.refs_1_ = bf16[32,2048]{1,0:T(8,128)(2,1)S(1)} collective-permute-done((bf16[32,2048]{1,0:T(8,128)(2,1)S(1)}, bf16[32,2048]{1,0:T(8,128)(2,1)S(1)}, u32[]{:S(2)}, u32[]{:S(2)}) %collective-permute-start) | collective-permute-done | bytes 131104 | tf_op jit(solution)/shard_map/ppermute | solution.py:30
  92.3 1.9 %collective-permute-start.4 = (bf16[128,2048]{1,0:T(8,128)(2,1)S(1)}, bf16[128,2048]{1,0:T(8,128)(2,1)S(1)}, u32[]{:S(2)}, u32[]{:S(2)}) collective-permute-start(bf16[128,2048]{1,0:T(8,128)(2,1)S(1)} %shard_map.84.refs_0_), channel_id=1, source_target_pairs={{0,30},{2,0},{4,2},{6,4},{8,6},{10,8},{12,10},{14,12},{16,14},{18,... | collective-permute-start | bytes 1572872 | tf_op jit(solution)/shard_map/ppermute | solution.py:30
  94.2 3.9 %collective-permute-start.5 = (bf16[128,2048]{1,0:T(8,128)(2,1)S(1)}, bf16[128,2048]{1,0:T(8,128)(2,1)S(1)}, u32[]{:S(2)}, u32[]{:S(2)}) collective-permute-start(bf16[128,2048]{1,0:T(8,128)(2,1)S(1)} %shard_map.84.refs_0_), channel_id=1, source_target_pairs={{0,2},{2,4},{4,6},{6,8},{8,10},{10,12},{12,14},{14,16},{16,18},{18... | collective-permute-start | bytes 1572872 | tf_op jit(solution)/shard_map/ppermute | solution.py:30
  98.2 7.6 %collective-permute-start.8 = (bf16[64,2048]{1,0:T(8,128)(2,1)S(1)}, bf16[64,2048]{1,0:T(8,128)(2,1)S(1)}, u32[]{:S(2)}, u32[]{:S(2)}) collective-permute-start(bf16[64,2048]{1,0:T(8,128)(2,1)S(1)} %get-tuple-element.14), channel_id=1, source_target_pairs={{0,28},{2,30},{4,0},{6,2},{8,4},{10,6},{12,8},{14,10},{16,12},{18,... | collective-permute-start | bytes 786440 | tf_op jit(solution)/shard_map/ppermute | solution.py:30
  105.8 1.9 %collective-permute-start.9 = (bf16[64,2048]{1,0:T(8,128)(2,1)S(1)}, bf16[64,2048]{1,0:T(8,128)(2,1)S(1)}, u32[]{:S(2)}, u32[]{:S(2)}) collective-permute-start(bf16[64,2048]{1,0:T(8,128)(2,1)S(1)} %get-tuple-element.15), channel_id=1, source_target_pairs={{0,4},{2,6},{4,8},{6,10},{8,12},{10,14},{12,16},{14,18},{16,20},{1... | collective-permute-start | bytes 786440 | tf_op jit(solution)/shard_map/ppermute | solution.py:30
  107.7 1.0 collective-permute-done.4.refs_0_
  108.7 8.2 %collective-permute-done.5.refs_1_ = bf16[128,2048]{1,0:T(8,128)(2,1)S(1)} collective-permute-done((bf16[128,2048]{1,0:T(8,128)(2,1)S(1)}, bf16[128,2048]{1,0:T(8,128)(2,1)S(1)}, u32[]{:S(2)}, u32[]{:S(2)}) %collective-permute-start.5) | collective-permute-done | bytes 524320 | tf_op jit(solution)/shard_map/ppermute | solution.py:30
  116.9 0.0 collective-permute-done.3.refs_2_.refs_3_
  116.9 1.9 %shard_map.86 = (bf16[128,2048]{1,0:T(8,128)(2,1)S(1)}, bf16[128,2048]{1,0:T(8,128)(2,1)S(1)}) custom-call(bf16[128,2048]{1,0:T(8,128)(2,1)S(1)} %collective-permute-done.4.refs_0_, bf16[128,2048]{1,0:T(8,128)(2,1)S(1)} %collective-permute-done.5.refs_1_, bf16[16,3,128,256]{3,2,1,0:T(8,128)(2,1)S(1)} %all_to_all.5.refs_1_.refs_2_, ...), custom_call_target="tpu_custom_call" | custom-call | flops 1610612736 | bytes 8388608 | tf_op jit(solution)/shard_map/pallas_call | solution.py:18
  118.9 2.4 %collective-permute-start.6 = (bf16[128,2048]{1,0:T(8,128)(2,1)S(1)}, bf16[128,2048]{1,0:T(8,128)(2,1)S(1)}, u32[]{:S(2)}, u32[]{:S(2)}) collective-permute-start(bf16[128,2048]{1,0:T(8,128)(2,1)S(1)} %get-tuple-element.12), channel_id=1, source_target_pairs={{0,2},{2,4},{4,6},{6,8},{8,10},{10,12},{12,14},{14,16},{16,18},{18... | collective-permute-start | bytes 1572872 | tf_op jit(solution)/shard_map/ppermute | solution.py:30
  121.2 3.5 %collective-permute-start.7 = (bf16[128,2048]{1,0:T(8,128)(2,1)S(1)}, bf16[128,2048]{1,0:T(8,128)(2,1)S(1)}, u32[]{:S(2)}, u32[]{:S(2)}) collective-permute-start(bf16[128,2048]{1,0:T(8,128)(2,1)S(1)} %get-tuple-element.13), channel_id=1, source_target_pairs={{0,30},{2,0},{4,2},{6,4},{8,6},{10,8},{12,10},{14,12},{16,14},{18,... | collective-permute-start | bytes 1572872 | tf_op jit(solution)/shard_map/ppermute | solution.py:30
  124.7 0.0 collective-permute-done.8.refs_0_
  124.7 0.0 collective-permute-done.9.refs_1_
  124.7 1.4 shard_map.88
  126.2 6.8 %collective-permute-start.10 = (bf16[64,2048]{1,0:T(8,128)(2,1)S(1)}, bf16[64,2048]{1,0:T(8,128)(2,1)S(1)}, u32[]{:S(2)}, u32[]{:S(2)}) collective-permute-start(bf16[64,2048]{1,0:T(8,128)(2,1)S(1)} %get-tuple-element.16), channel_id=1, source_target_pairs={{0,4},{2,6},{4,8},{6,10},{8,12},{10,14},{12,16},{14,18},{16,20},{1... | collective-permute-start | bytes 786440 | tf_op jit(solution)/shard_map/ppermute | solution.py:30
  133.1 4.6 %collective-permute-start.11 = (bf16[64,2048]{1,0:T(8,128)(2,1)S(1)}, bf16[64,2048]{1,0:T(8,128)(2,1)S(1)}, u32[]{:S(2)}, u32[]{:S(2)}) collective-permute-start(bf16[64,2048]{1,0:T(8,128)(2,1)S(1)} %get-tuple-element.17), channel_id=1, source_target_pairs={{0,28},{2,30},{4,0},{6,2},{8,4},{10,6},{12,8},{14,10},{16,12},{18,... | collective-permute-start | bytes 786440 | tf_op jit(solution)/shard_map/ppermute | solution.py:30
  137.7 1.5 shard_map.85.refs_0_.own_ref
  139.2 6.5 %collective-permute-done.10.refs_3_.next2_ref = bf16[64,2048]{1,0:T(8,128)(2,1)S(1)} collective-permute-done((bf16[64,2048]{1,0:T(8,128)(2,1)S(1)}, bf16[64,2048]{1,0:T(8,128)(2,1)S(1)}, u32[]{:S(2)}, u32[]{:S(2)}) %collective-permute-start.10) | collective-permute-done | bytes 262176 | tf_op jit(solution)/shard_map/ppermute | solution.py:30
  145.7 2.1 %collective-permute-done.11.refs_4_.prev2_ref = bf16[64,2048]{1,0:T(8,128)(2,1)S(1)} collective-permute-done((bf16[64,2048]{1,0:T(8,128)(2,1)S(1)}, bf16[64,2048]{1,0:T(8,128)(2,1)S(1)}, u32[]{:S(2)}, u32[]{:S(2)}) %collective-permute-start.11) | collective-permute-done | bytes 262176 | tf_op jit(solution)/shard_map/ppermute | solution.py:30
  147.8 0.0 collective-permute-done.6.refs_1_.next_ref
  147.8 0.0 collective-permute-done.7.refs_2_.prev_ref
  147.8 0.1 shard_map.90
  147.9 10.5 %collective-permute-start.13 = (bf16[32,2048]{1,0:T(8,128)(2,1)S(1)}, bf16[32,2048]{1,0:T(8,128)(2,1)S(1)}, u32[]{:S(2)}, u32[]{:S(2)}) collective-permute-start(bf16[32,2048]{1,0:T(8,128)(2,1)S(1)} %get-tuple-element.18), channel_id=1, source_target_pairs={{0,8},{2,10},{4,12},{6,14},{8,16},{10,18},{12,20},{14,22},{16,24},... | collective-permute-start | bytes 393224 | tf_op jit(solution)/shard_map/ppermute | solution.py:30
  158.4 1.9 %collective-permute-start.14 = (bf16[32,2048]{1,0:T(8,128)(2,1)S(1)}, bf16[32,2048]{1,0:T(8,128)(2,1)S(1)}, u32[]{:S(2)}, u32[]{:S(2)}) collective-permute-start(bf16[32,2048]{1,0:T(8,128)(2,1)S(1)} %get-tuple-element.19), channel_id=1, source_target_pairs={{0,24},{2,26},{4,28},{6,30},{8,0},{10,2},{12,4},{14,6},{16,8},{18,... | collective-permute-start | bytes 393224 | tf_op jit(solution)/shard_map/ppermute | solution.py:30
  160.4 7.3 %collective-permute-start.12 = (bf16[32,2048]{1,0:T(8,128)(2,1)S(1)}, bf16[32,2048]{1,0:T(8,128)(2,1)S(1)}, u32[]{:S(2)}, u32[]{:S(2)}) collective-permute-start(bf16[32,2048]{1,0:T(8,128)(2,1)S(1)} %shard_map.89), channel_id=1, source_target_pairs={{0,16},{2,18},{4,20},{6,22},{8,24},{10,26},{12,28},{14,30},{16,0},... | collective-permute-start | bytes 393224 | tf_op jit(solution)/shard_map/ppermute | solution.py:30
  167.6 1.8 fusion
  169.4 0.0 collective-permute-done.13.above_ref
  169.4 13.5 %collective-permute-done.14.below_ref = bf16[32,2048]{1,0:T(8,128)(2,1)S(1)} collective-permute-done((bf16[32,2048]{1,0:T(8,128)(2,1)S(1)}, bf16[32,2048]{1,0:T(8,128)(2,1)S(1)}, u32[]{:S(2)}, u32[]{:S(2)}) %collective-permute-start.14) | collective-permute-done | bytes 131104 | tf_op jit(solution)/shard_map/ppermute | solution.py:30
  182.9 0.0 collective-permute-done.12.far_ref
  182.9 0.8 shard_map.91
  (3 shorter events, 0.1 us)
Async XLA Ops:
  3.5 48.7 %copy-start = (bf16[32,2048]{1,0:T(8,128)(2,1)S(1)}, bf16[32,2048]{1,0:T(8,128)(2,1)}, u32[]{:S(2)}) copy-start(bf16[32,2048]{1,0:T(8,128)(2,1)} %tokens_ref.1) | copy-start | bytes 393220
  50.3 66.6 %collective-permute-start.3 = (bf16[16,3,128,256]{3,2,1,0:T(8,128)(2,1)S(1)}, bf16[16,3,128,256]{3,2,1,0:T(8,128)(2,1)S(1)}, u32[]{:S(2)}, u32[]{:S(2)}) collective-permute-start(bf16[16,3,128,256]{3,2,1,0:T(8,128)(2,1)S(1)} %all_to_all.5.refs_1_.refs_2_), channel_id=1, source_target_pairs={{0,1},{1,0},{2,3},{3,2},{4,5},{5,4},{6,7},{7,6},{8,9},{9,8},{10,11... | collective-permute-start | bytes 9437192 | tf_op jit(solution)/shard_map/ppermute | solution.py:165
  52.3 23.7 %collective-permute-start.1 = (bf16[32,2048]{1,0:T(8,128)(2,1)S(1)}, bf16[32,2048]{1,0:T(8,128)(2,1)S(1)}, u32[]{:S(2)}, u32[]{:S(2)}) collective-permute-start(bf16[32,2048]{1,0:T(8,128)(2,1)S(1)} %copy-done), channel_id=1, source_target_pairs={{0,24},{2,26},{4,28},{6,30},{8,0},{10,2},{12,4},{14,6},{16,8},{18,... | collective-permute-start | bytes 393224 | tf_op jit(solution)/shard_map/ppermute | solution.py:30
  63.2 20.9 %collective-permute-start.2 = (bf16[32,2048]{1,0:T(8,128)(2,1)S(1)}, bf16[32,2048]{1,0:T(8,128)(2,1)S(1)}, u32[]{:S(2)}, u32[]{:S(2)}) collective-permute-start(bf16[32,2048]{1,0:T(8,128)(2,1)S(1)} %copy-done), channel_id=1, source_target_pairs={{0,8},{2,10},{4,12},{6,14},{8,16},{10,18},{12,20},{14,22},{16,24},... | collective-permute-start | bytes 393224 | tf_op jit(solution)/shard_map/ppermute | solution.py:30
  65.1 27.1 %collective-permute-start = (bf16[32,2048]{1,0:T(8,128)(2,1)S(1)}, bf16[32,2048]{1,0:T(8,128)(2,1)S(1)}, u32[]{:S(2)}, u32[]{:S(2)}) collective-permute-start(bf16[32,2048]{1,0:T(8,128)(2,1)S(1)} %copy-done), channel_id=1, source_target_pairs={{0,16},{2,18},{4,20},{6,22},{8,24},{10,26},{12,28},{14,30},{16,0},... | collective-permute-start | bytes 393224 | tf_op jit(solution)/shard_map/ppermute | solution.py:30
  92.3 16.5 %collective-permute-start.4 = (bf16[128,2048]{1,0:T(8,128)(2,1)S(1)}, bf16[128,2048]{1,0:T(8,128)(2,1)S(1)}, u32[]{:S(2)}, u32[]{:S(2)}) collective-permute-start(bf16[128,2048]{1,0:T(8,128)(2,1)S(1)} %shard_map.84.refs_0_), channel_id=1, source_target_pairs={{0,30},{2,0},{4,2},{6,4},{8,6},{10,8},{12,10},{14,12},{16,14},{18,... | collective-permute-start | bytes 1572872 | tf_op jit(solution)/shard_map/ppermute | solution.py:30
  94.2 22.7 %collective-permute-start.5 = (bf16[128,2048]{1,0:T(8,128)(2,1)S(1)}, bf16[128,2048]{1,0:T(8,128)(2,1)S(1)}, u32[]{:S(2)}, u32[]{:S(2)}) collective-permute-start(bf16[128,2048]{1,0:T(8,128)(2,1)S(1)} %shard_map.84.refs_0_), channel_id=1, source_target_pairs={{0,2},{2,4},{4,6},{6,8},{8,10},{10,12},{12,14},{14,16},{16,18},{18... | collective-permute-start | bytes 1572872 | tf_op jit(solution)/shard_map/ppermute | solution.py:30
  98.2 26.6 %collective-permute-start.8 = (bf16[64,2048]{1,0:T(8,128)(2,1)S(1)}, bf16[64,2048]{1,0:T(8,128)(2,1)S(1)}, u32[]{:S(2)}, u32[]{:S(2)}) collective-permute-start(bf16[64,2048]{1,0:T(8,128)(2,1)S(1)} %get-tuple-element.14), channel_id=1, source_target_pairs={{0,28},{2,30},{4,0},{6,2},{8,4},{10,6},{12,8},{14,10},{16,12},{18,... | collective-permute-start | bytes 786440 | tf_op jit(solution)/shard_map/ppermute | solution.py:30
  105.8 18.9 %collective-permute-start.9 = (bf16[64,2048]{1,0:T(8,128)(2,1)S(1)}, bf16[64,2048]{1,0:T(8,128)(2,1)S(1)}, u32[]{:S(2)}, u32[]{:S(2)}) collective-permute-start(bf16[64,2048]{1,0:T(8,128)(2,1)S(1)} %get-tuple-element.15), channel_id=1, source_target_pairs={{0,4},{2,6},{4,8},{6,10},{8,12},{10,14},{12,16},{14,18},{16,20},{1... | collective-permute-start | bytes 786440 | tf_op jit(solution)/shard_map/ppermute | solution.py:30
  118.9 28.9 %collective-permute-start.6 = (bf16[128,2048]{1,0:T(8,128)(2,1)S(1)}, bf16[128,2048]{1,0:T(8,128)(2,1)S(1)}, u32[]{:S(2)}, u32[]{:S(2)}) collective-permute-start(bf16[128,2048]{1,0:T(8,128)(2,1)S(1)} %get-tuple-element.12), channel_id=1, source_target_pairs={{0,2},{2,4},{4,6},{6,8},{8,10},{10,12},{12,14},{14,16},{16,18},{18... | collective-permute-start | bytes 1572872 | tf_op jit(solution)/shard_map/ppermute | solution.py:30
  121.2 26.5 %collective-permute-start.7 = (bf16[128,2048]{1,0:T(8,128)(2,1)S(1)}, bf16[128,2048]{1,0:T(8,128)(2,1)S(1)}, u32[]{:S(2)}, u32[]{:S(2)}) collective-permute-start(bf16[128,2048]{1,0:T(8,128)(2,1)S(1)} %get-tuple-element.13), channel_id=1, source_target_pairs={{0,30},{2,0},{4,2},{6,4},{8,6},{10,8},{12,10},{14,12},{16,14},{18,... | collective-permute-start | bytes 1572872 | tf_op jit(solution)/shard_map/ppermute | solution.py:30
  126.2 19.5 %collective-permute-start.10 = (bf16[64,2048]{1,0:T(8,128)(2,1)S(1)}, bf16[64,2048]{1,0:T(8,128)(2,1)S(1)}, u32[]{:S(2)}, u32[]{:S(2)}) collective-permute-start(bf16[64,2048]{1,0:T(8,128)(2,1)S(1)} %get-tuple-element.16), channel_id=1, source_target_pairs={{0,4},{2,6},{4,8},{6,10},{8,12},{10,14},{12,16},{14,18},{16,20},{1... | collective-permute-start | bytes 786440 | tf_op jit(solution)/shard_map/ppermute | solution.py:30
  133.1 14.7 %collective-permute-start.11 = (bf16[64,2048]{1,0:T(8,128)(2,1)S(1)}, bf16[64,2048]{1,0:T(8,128)(2,1)S(1)}, u32[]{:S(2)}, u32[]{:S(2)}) collective-permute-start(bf16[64,2048]{1,0:T(8,128)(2,1)S(1)} %get-tuple-element.17), channel_id=1, source_target_pairs={{0,28},{2,30},{4,0},{6,2},{8,4},{10,6},{12,8},{14,10},{16,12},{18,... | collective-permute-start | bytes 786440 | tf_op jit(solution)/shard_map/ppermute | solution.py:30
  147.9 21.5 %collective-permute-start.13 = (bf16[32,2048]{1,0:T(8,128)(2,1)S(1)}, bf16[32,2048]{1,0:T(8,128)(2,1)S(1)}, u32[]{:S(2)}, u32[]{:S(2)}) collective-permute-start(bf16[32,2048]{1,0:T(8,128)(2,1)S(1)} %get-tuple-element.18), channel_id=1, source_target_pairs={{0,8},{2,10},{4,12},{6,14},{8,16},{10,18},{12,20},{14,22},{16,24},... | collective-permute-start | bytes 393224 | tf_op jit(solution)/shard_map/ppermute | solution.py:30
  158.4 24.5 %collective-permute-start.14 = (bf16[32,2048]{1,0:T(8,128)(2,1)S(1)}, bf16[32,2048]{1,0:T(8,128)(2,1)S(1)}, u32[]{:S(2)}, u32[]{:S(2)}) collective-permute-start(bf16[32,2048]{1,0:T(8,128)(2,1)S(1)} %get-tuple-element.19), channel_id=1, source_target_pairs={{0,24},{2,26},{4,28},{6,30},{8,0},{10,2},{12,4},{14,6},{16,8},{18,... | collective-permute-start | bytes 393224 | tf_op jit(solution)/shard_map/ppermute | solution.py:30
  160.4 22.5 %collective-permute-start.12 = (bf16[32,2048]{1,0:T(8,128)(2,1)S(1)}, bf16[32,2048]{1,0:T(8,128)(2,1)S(1)}, u32[]{:S(2)}, u32[]{:S(2)}) collective-permute-start(bf16[32,2048]{1,0:T(8,128)(2,1)S(1)} %shard_map.89), channel_id=1, source_target_pairs={{0,16},{2,18},{4,20},{6,22},{8,24},{10,26},{12,28},{14,30},{16,0},... | collective-permute-start | bytes 393224 | tf_op jit(solution)/shard_map/ppermute | solution.py:30

commit v5 on v3

--- a/solution.py
+++ b/solution.py
@@ -143,16 +143,18 @@
 
 
 def step(tokens, norm_gain, gate_master, up_master, down_master):
-    far = move(tokens, 8)
     copies = weight_copies(norm_gain, gate_master, up_master, down_master, lax.axis_size("fs"))
     packed = lax.all_to_all(copies, "fs", split_axis=0, concat_axis=0, tiled=True)
+    far = move(tokens, 8)
     above = move(tokens, -4)
     below = move(tokens, 4)
+    own_next2 = move(tokens, -2)
+    own_prev2 = move(tokens, 2)
     held = pack(tokens, far, above, below)
     from_next = move(held, -1)
     from_prev = move(held, 1)
-    from_next2 = move(pack(tokens, above), -2)
-    from_prev2 = move(pack(tokens, below), 2)
+    from_next2 = (own_next2, move(above, -2))
+    from_prev2 = (own_prev2, move(below, 2))
 
     partner = lax.ppermute(packed, "c", [(0, 1), (1, 0)])
     weights = (packed, partner)
@@ -160,7 +162,7 @@
     ones_next, ones_prev = partial_sums((from_next, from_prev), weights, 2, jnp.bfloat16)
     to_next = move(ones_next, 1)
     to_prev = move(ones_prev, -1)
-    twos_next, twos_prev = partial_sums((from_next2, from_prev2), weights, 2, jnp.bfloat16)
+    twos_next, twos_prev = partial_sums((*from_next2, *from_prev2), weights, 2, jnp.bfloat16)
     to_next2 = move(twos_next, 2)
     to_prev2 = move(twos_prev, -2)
     (own,) = partial_sums((held,), weights, 1, jnp.float32)

time: 184 us -> 195 us (1.060)
  the two profiles are of different devices: /device:TPU:64 before, /device:TPU:32 now
where the time goes in v5:
time: 195 us; the launch traced here: 194 us
  starting transfers between devices  89.8 us (46%)
  blocking collectives  46.8 us (24%)
  waiting for transfers between devices  46.6 us (24%)
  Pallas kernels  8.7 us (4%)
    ppermute x16, starting transfers between devices, move(): lax.ppermute(array, 'z', [(i, (i + by) % planes) for i in range(planes)])  87.9 us
    all_to_all x1, blocking collectives, step(): lax.all_to_all(copies, 'fs', split_axis=0, concat_axis=0, tiled=True)  46.8 us
    ppermute x16, waiting for transfers between devices, move(): lax.ppermute(array, 'z', [(i, (i + by) % planes) for i in range(planes)])  46.6 us
    pallas_call x7, Pallas kernels, local(): pl.pallas_call(kernel, out_shape=outs, in_specs=[VMEM] * len(args), out_s...  5.82 us
  transfers between devices with their start and end apart: 17, of which 11 were waited for; matrix products, arithmetic and copies ran while one was open for 1% of the time, Pallas kernels for 3%

profile of v5, /device:TPU:32, one launch (start us, length us, event | category | flops | bytes accessed | tf_op | source)
XLA Modules:
  0.0 194.5 jit_solution(3943631020708773013)
XLA Ops:
  0.6 2.9 %prepare.1 = bf16[16,3,128,256]{3,2,1,0:T(8,128)(2,1)} custom-call(f32[1,128]{1,0:T(1,128)} %bitcast.7, f32[128,256]{1,0:T(8,128)} %gate_hbm.1, f32[128,256]{1,0:T(8,128)} %up_hbm.1, f32[128,256]{1,0:T(8,128)} %down_hbm.1), custom_call_target="tpu_custom_call" | custom-call | flops 1000000 | bytes 4000000 | tf_op jit(solution)/shard_map/prepare/pallas_call | solution.py:58
  3.5 0.0 copy-start
  3.5 46.8 %all_to_all.5.refs_1_.refs_2_.refs_4_ = bf16[16,3,128,256]{3,2,1,0:T(8,128)(2,1)S(1)} all-to-all(bf16[16,3,128,256]{3,2,1,0:T(8,128)(2,1)} %prepare.1), channel_id=1, replica_groups=mesh['fs'=16,'z'=16,'c'=2] {'fs'}, dimensions={0} | all-to-all | bytes 6291456 | tf_op jit(solution)/shard_map/all_to_all | solution.py:147
  50.3 1.9 collective-permute-start.3
  52.2 0.0 copy-done
  52.3 11.8 %collective-permute-start.1 = (bf16[32,2048]{1,0:T(8,128)(2,1)S(1)}, bf16[32,2048]{1,0:T(8,128)(2,1)S(1)}, u32[]{:S(2)}, u32[]{:S(2)}) collective-permute-start(bf16[32,2048]{1,0:T(8,128)(2,1)S(1)} %copy-done), channel_id=1, source_target_pairs={{0,24},{2,26},{4,28},{6,30},{8,0},{10,2},{12,4},{14,6},{16,8},{18,... | collective-permute-start | bytes 393224 | tf_op jit(solution)/shard_map/ppermute | solution.py:30
  64.1 1.9 collective-permute-start.2
  66.0 10.8 %collective-permute-start = (bf16[32,2048]{1,0:T(8,128)(2,1)S(1)}, bf16[32,2048]{1,0:T(8,128)(2,1)S(1)}, u32[]{:S(2)}, u32[]{:S(2)}) collective-permute-start(bf16[32,2048]{1,0:T(8,128)(2,1)S(1)} %copy-done), channel_id=1, source_target_pairs={{0,16},{2,18},{4,20},{6,22},{8,24},{10,26},{12,28},{14,30},{16,0},... | collective-permute-start | bytes 393224 | tf_op jit(solution)/shard_map/ppermute | solution.py:30
  76.9 0.0 collective-permute-done.1.refs_2_
  76.9 5.4 %collective-permute-done.2.refs_3_ = bf16[32,2048]{1,0:T(8,128)(2,1)S(1)} collective-permute-done((bf16[32,2048]{1,0:T(8,128)(2,1)S(1)}, bf16[32,2048]{1,0:T(8,128)(2,1)S(1)}, u32[]{:S(2)}, u32[]{:S(2)}) %collective-permute-start.2) | collective-permute-done | bytes 131104 | tf_op jit(solution)/shard_map/ppermute | solution.py:30
  82.2 5.7 %collective-permute-done.refs_1_ = bf16[32,2048]{1,0:T(8,128)(2,1)S(1)} collective-permute-done((bf16[32,2048]{1,0:T(8,128)(2,1)S(1)}, bf16[32,2048]{1,0:T(8,128)(2,1)S(1)}, u32[]{:S(2)}, u32[]{:S(2)}) %collective-permute-start) | collective-permute-done | bytes 131104 | tf_op jit(solution)/shard_map/ppermute | solution.py:30
  88.0 12.3 %collective-permute-start.4 = (bf16[128,2048]{1,0:T(8,128)(2,1)S(1)}, bf16[128,2048]{1,0:T(8,128)(2,1)S(1)}, u32[]{:S(2)}, u32[]{:S(2)}) collective-permute-start(bf16[128,2048]{1,0:T(8,128)(2,1)S(1)} %shard_map.84.refs_0_), channel_id=1, source_target_pairs={{0,30},{2,0},{4,2},{6,4},{8,6},{10,8},{12,10},{14,12},{16,14},{18,... | collective-permute-start | bytes 1572872 | tf_op jit(solution)/shard_map/ppermute | solution.py:30
  100.3 1.9 collective-permute-start.5
  102.3 1.9 collective-permute-start.10
  104.2 6.9 %collective-permute-done.4.refs_0_ = bf16[128,2048]{1,0:T(8,128)(2,1)S(1)} collective-permute-done((bf16[128,2048]{1,0:T(8,128)(2,1)S(1)}, bf16[128,2048]{1,0:T(8,128)(2,1)S(1)}, u32[]{:S(2)}, u32[]{:S(2)}) %collective-permute-start.4) | collective-permute-done | bytes 524320 | tf_op jit(solution)/shard_map/ppermute | solution.py:30
  111.1 5.8 %collective-permute-done.5.refs_1_ = bf16[128,2048]{1,0:T(8,128)(2,1)S(1)} collective-permute-done((bf16[128,2048]{1,0:T(8,128)(2,1)S(1)}, bf16[128,2048]{1,0:T(8,128)(2,1)S(1)}, u32[]{:S(2)}, u32[]{:S(2)}) %collective-permute-start.5) | collective-permute-done | bytes 524320 | tf_op jit(solution)/shard_map/ppermute | solution.py:30
  116.9 0.0 collective-permute-done.3.refs_2_.refs_3_.refs_5_
  116.9 1.9 shard_map.86
  118.8 3.4 %collective-permute-start.6 = (bf16[128,2048]{1,0:T(8,128)(2,1)S(1)}, bf16[128,2048]{1,0:T(8,128)(2,1)S(1)}, u32[]{:S(2)}, u32[]{:S(2)}) collective-permute-start(bf16[128,2048]{1,0:T(8,128)(2,1)S(1)} %get-tuple-element.10), channel_id=1, source_target_pairs={{0,2},{2,4},{4,6},{6,8},{8,10},{10,12},{12,14},{14,16},{16,18},{18... | collective-permute-start | bytes 1572872 | tf_op jit(solution)/shard_map/ppermute | solution.py:30
  122.2 4.5 %collective-permute-start.7 = (bf16[128,2048]{1,0:T(8,128)(2,1)S(1)}, bf16[128,2048]{1,0:T(8,128)(2,1)S(1)}, u32[]{:S(2)}, u32[]{:S(2)}) collective-permute-start(bf16[128,2048]{1,0:T(8,128)(2,1)S(1)} %get-tuple-element.11), channel_id=1, source_target_pairs={{0,30},{2,0},{4,2},{6,4},{8,6},{10,8},{12,10},{14,12},{16,14},{18,... | collective-permute-start | bytes 1572872 | tf_op jit(solution)/shard_map/ppermute | solution.py:30
  126.7 4.6 %collective-permute-start.8 = (bf16[32,2048]{1,0:T(8,128)(2,1)S(1)}, bf16[32,2048]{1,0:T(8,128)(2,1)S(1)}, u32[]{:S(2)}, u32[]{:S(2)}) collective-permute-start(bf16[32,2048]{1,0:T(8,128)(2,1)S(1)} %copy-done), channel_id=1, source_target_pairs={{0,28},{2,30},{4,0},{6,2},{8,4},{10,6},{12,8},{14,10},{16,12},{18,... | collective-permute-start | bytes 393224 | tf_op jit(solution)/shard_map/ppermute | solution.py:30
  131.3 2.2 %collective-permute-start.11 = (bf16[32,2048]{1,0:T(8,128)(2,1)S(1)}, bf16[32,2048]{1,0:T(8,128)(2,1)S(1)}, u32[]{:S(2)}, u32[]{:S(2)}) collective-permute-start(bf16[32,2048]{1,0:T(8,128)(2,1)S(1)} %collective-permute-done.2.refs_3_), channel_id=1, source_target_pairs={{0,4},{2,6},{4,8},{6,10},{8,12},{10,14},{12,16},{14,18},{16,20},{1... | collective-permute-start | bytes 393224 | tf_op jit(solution)/shard_map/ppermute | solution.py:30
  133.5 0.0 collective-permute-done.10.refs_2_
  133.5 5.8 %collective-permute-start.9 = (bf16[32,2048]{1,0:T(8,128)(2,1)S(1)}, bf16[32,2048]{1,0:T(8,128)(2,1)S(1)}, u32[]{:S(2)}, u32[]{:S(2)}) collective-permute-start(bf16[32,2048]{1,0:T(8,128)(2,1)S(1)} %collective-permute-done.1.refs_2_), channel_id=1, source_target_pairs={{0,28},{2,30},{4,0},{6,2},{8,4},{10,6},{12,8},{14,10},{16,12},{18,... | collective-permute-start | bytes 393224 | tf_op jit(solution)/shard_map/ppermute | solution.py:30
  139.3 1.7 collective-permute-done.8.refs_0_
  141.0 0.7 collective-permute-done.11.refs_3_
  141.7 3.4 %collective-permute-done.9.refs_1_ = bf16[32,2048]{1,0:T(8,128)(2,1)S(1)} collective-permute-done((bf16[32,2048]{1,0:T(8,128)(2,1)S(1)}, bf16[32,2048]{1,0:T(8,128)(2,1)S(1)}, u32[]{:S(2)}, u32[]{:S(2)}) %collective-permute-start.9) | collective-permute-done | bytes 131104 | tf_op jit(solution)/shard_map/ppermute | solution.py:30
  145.1 1.4 shard_map.87
  146.6 3.2 %collective-permute-start.12 = (bf16[64,2048]{1,0:T(8,128)(2,1)S(1)}, bf16[64,2048]{1,0:T(8,128)(2,1)S(1)}, u32[]{:S(2)}, u32[]{:S(2)}) collective-permute-start(bf16[64,2048]{1,0:T(8,128)(2,1)S(1)} %get-tuple-element.12), channel_id=1, source_target_pairs={{0,4},{2,6},{4,8},{6,10},{8,12},{10,14},{12,16},{14,18},{16,20},{1... | collective-permute-start | bytes 786440 | tf_op jit(solution)/shard_map/ppermute | solution.py:30
  149.7 5.3 %collective-permute-start.13 = (bf16[64,2048]{1,0:T(8,128)(2,1)S(1)}, bf16[64,2048]{1,0:T(8,128)(2,1)S(1)}, u32[]{:S(2)}, u32[]{:S(2)}) collective-permute-start(bf16[64,2048]{1,0:T(8,128)(2,1)S(1)} %get-tuple-element.13), channel_id=1, source_target_pairs={{0,28},{2,30},{4,0},{6,2},{8,4},{10,6},{12,8},{14,10},{16,12},{18,... | collective-permute-start | bytes 786440 | tf_op jit(solution)/shard_map/ppermute | solution.py:30
  155.1 1.5 shard_map.85.refs_0_.own_ref
  156.5 1.2 collective-permute-done.12.refs_3_.next2_ref
  157.7 4.7 %collective-permute-done.13.refs_4_.prev2_ref = bf16[64,2048]{1,0:T(8,128)(2,1)S(1)} collective-permute-done((bf16[64,2048]{1,0:T(8,128)(2,1)S(1)}, bf16[64,2048]{1,0:T(8,128)(2,1)S(1)}, u32[]{:S(2)}, u32[]{:S(2)}) %collective-permute-start.13) | collective-permute-done | bytes 262176 | tf_op jit(solution)/shard_map/ppermute | solution.py:30
  162.4 0.0 collective-permute-done.6.refs_1_.next_ref
  162.4 0.0 collective-permute-done.7.refs_2_.prev_ref
  162.4 0.1 shard_map.89
  162.5 8.5 %collective-permute-start.15 = (bf16[32,2048]{1,0:T(8,128)(2,1)S(1)}, bf16[32,2048]{1,0:T(8,128)(2,1)S(1)}, u32[]{:S(2)}, u32[]{:S(2)}) collective-permute-start(bf16[32,2048]{1,0:T(8,128)(2,1)S(1)} %get-tuple-element.14), channel_id=1, source_target_pairs={{0,8},{2,10},{4,12},{6,14},{8,16},{10,18},{12,20},{14,22},{16,24},... | collective-permute-start | bytes 393224 | tf_op jit(solution)/shard_map/ppermute | solution.py:30
  171.0 1.9 collective-permute-start.16
  173.0 7.8 %collective-permute-start.14 = (bf16[32,2048]{1,0:T(8,128)(2,1)S(1)}, bf16[32,2048]{1,0:T(8,128)(2,1)S(1)}, u32[]{:S(2)}, u32[]{:S(2)}) collective-permute-start(bf16[32,2048]{1,0:T(8,128)(2,1)S(1)} %shard_map.88), channel_id=1, source_target_pairs={{0,16},{2,18},{4,20},{6,22},{8,24},{10,26},{12,28},{14,30},{16,0},... | collective-permute-start | bytes 393224 | tf_op jit(solution)/shard_map/ppermute | solution.py:30
  180.8 1.8 fusion
  182.5 0.0 collective-permute-done.15.above_ref
  182.5 2.6 %collective-permute-done.16.below_ref = bf16[32,2048]{1,0:T(8,128)(2,1)S(1)} collective-permute-done((bf16[32,2048]{1,0:T(8,128)(2,1)S(1)}, bf16[32,2048]{1,0:T(8,128)(2,1)S(1)}, u32[]{:S(2)}, u32[]{:S(2)}) %collective-permute-start.16) | collective-permute-done | bytes 131104 | tf_op jit(solution)/shard_map/ppermute | solution.py:30
  185.1 8.5 %collective-permute-done.14.far_ref = bf16[32,2048]{1,0:T(8,128)(2,1)S(1)} collective-permute-done((bf16[32,2048]{1,0:T(8,128)(2,1)S(1)}, bf16[32,2048]{1,0:T(8,128)(2,1)S(1)}, u32[]{:S(2)}, u32[]{:S(2)}) %collective-permute-start.14) | collective-permute-done | bytes 131104 | tf_op jit(solution)/shard_map/ppermute | solution.py:30
  193.7 0.8 shard_map.90
  (2 shorter events, 0.1 us)
Async XLA Ops:
  3.5 48.7 %copy-start = (bf16[32,2048]{1,0:T(8,128)(2,1)S(1)}, bf16[32,2048]{1,0:T(8,128)(2,1)}, u32[]{:S(2)}) copy-start(bf16[32,2048]{1,0:T(8,128)(2,1)} %tokens_ref.1) | copy-start | bytes 393220
  50.3 66.5 %collective-permute-start.3 = (bf16[16,3,128,256]{3,2,1,0:T(8,128)(2,1)S(1)}, bf16[16,3,128,256]{3,2,1,0:T(8,128)(2,1)S(1)}, u32[]{:S(2)}, u32[]{:S(2)}) collective-permute-start(bf16[16,3,128,256]{3,2,1,0:T(8,128)(2,1)S(1)} %all_to_all.5.refs_1_.refs_2_.refs_4_), channel_id=1, source_target_pairs={{0,1},{1,0},{2,3},{3,2},{4,5},{5,4},{6,7},{7,6},{8,9},{9,8},{10,11... | collective-permute-start | bytes 9437192 | tf_op jit(solution)/shard_map/ppermute | solution.py:159
  52.3 24.6 %collective-permute-start.1 = (bf16[32,2048]{1,0:T(8,128)(2,1)S(1)}, bf16[32,2048]{1,0:T(8,128)(2,1)S(1)}, u32[]{:S(2)}, u32[]{:S(2)}) collective-permute-start(bf16[32,2048]{1,0:T(8,128)(2,1)S(1)} %copy-done), channel_id=1, source_target_pairs={{0,24},{2,26},{4,28},{6,30},{8,0},{10,2},{12,4},{14,6},{16,8},{18,... | collective-permute-start | bytes 393224 | tf_op jit(solution)/shard_map/ppermute | solution.py:30
  64.1 18.1 %collective-permute-start.2 = (bf16[32,2048]{1,0:T(8,128)(2,1)S(1)}, bf16[32,2048]{1,0:T(8,128)(2,1)S(1)}, u32[]{:S(2)}, u32[]{:S(2)}) collective-permute-start(bf16[32,2048]{1,0:T(8,128)(2,1)S(1)} %copy-done), channel_id=1, source_target_pairs={{0,8},{2,10},{4,12},{6,14},{8,16},{10,18},{12,20},{14,22},{16,24},... | collective-permute-start | bytes 393224 | tf_op jit(solution)/shard_map/ppermute | solution.py:30
  66.0 21.9 %collective-permute-start = (bf16[32,2048]{1,0:T(8,128)(2,1)S(1)}, bf16[32,2048]{1,0:T(8,128)(2,1)S(1)}, u32[]{:S(2)}, u32[]{:S(2)}) collective-permute-start(bf16[32,2048]{1,0:T(8,128)(2,1)S(1)} %copy-done), channel_id=1, source_target_pairs={{0,16},{2,18},{4,20},{6,22},{8,24},{10,26},{12,28},{14,30},{16,0},... | collective-permute-start | bytes 393224 | tf_op jit(solution)/shard_map/ppermute | solution.py:30
  88.0 23.1 %collective-permute-start.4 = (bf16[128,2048]{1,0:T(8,128)(2,1)S(1)}, bf16[128,2048]{1,0:T(8,128)(2,1)S(1)}, u32[]{:S(2)}, u32[]{:S(2)}) collective-permute-start(bf16[128,2048]{1,0:T(8,128)(2,1)S(1)} %shard_map.84.refs_0_), channel_id=1, source_target_pairs={{0,30},{2,0},{4,2},{6,4},{8,6},{10,8},{12,10},{14,12},{16,14},{18,... | collective-permute-start | bytes 1572872 | tf_op jit(solution)/shard_map/ppermute | solution.py:30
  100.3 16.5 %collective-permute-start.5 = (bf16[128,2048]{1,0:T(8,128)(2,1)S(1)}, bf16[128,2048]{1,0:T(8,128)(2,1)S(1)}, u32[]{:S(2)}, u32[]{:S(2)}) collective-permute-start(bf16[128,2048]{1,0:T(8,128)(2,1)S(1)} %shard_map.84.refs_0_), channel_id=1, source_target_pairs={{0,2},{2,4},{4,6},{6,8},{8,10},{10,12},{12,14},{14,16},{16,18},{18... | collective-permute-start | bytes 1572872 | tf_op jit(solution)/shard_map/ppermute | solution.py:30
  102.3 31.2 %collective-permute-start.10 = (bf16[32,2048]{1,0:T(8,128)(2,1)S(1)}, bf16[32,2048]{1,0:T(8,128)(2,1)S(1)}, u32[]{:S(2)}, u32[]{:S(2)}) collective-permute-start(bf16[32,2048]{1,0:T(8,128)(2,1)S(1)} %copy-done), channel_id=1, source_target_pairs={{0,4},{2,6},{4,8},{6,10},{8,12},{10,14},{12,16},{14,18},{16,20},{1... | collective-permute-start | bytes 393224 | tf_op jit(solution)/shard_map/ppermute | solution.py:30
  118.8 43.6 %collective-permute-start.6 = (bf16[128,2048]{1,0:T(8,128)(2,1)S(1)}, bf16[128,2048]{1,0:T(8,128)(2,1)S(1)}, u32[]{:S(2)}, u32[]{:S(2)}) collective-permute-start(bf16[128,2048]{1,0:T(8,128)(2,1)S(1)} %get-tuple-element.10), channel_id=1, source_target_pairs={{0,2},{2,4},{4,6},{6,8},{8,10},{10,12},{12,14},{14,16},{16,18},{18... | collective-permute-start | bytes 1572872 | tf_op jit(solution)/shard_map/ppermute | solution.py:30
  122.2 40.2 %collective-permute-start.7 = (bf16[128,2048]{1,0:T(8,128)(2,1)S(1)}, bf16[128,2048]{1,0:T(8,128)(2,1)S(1)}, u32[]{:S(2)}, u32[]{:S(2)}) collective-permute-start(bf16[128,2048]{1,0:T(8,128)(2,1)S(1)} %get-tuple-element.11), channel_id=1, source_target_pairs={{0,30},{2,0},{4,2},{6,4},{8,6},{10,8},{12,10},{14,12},{16,14},{18,... | collective-permute-start | bytes 1572872 | tf_op jit(solution)/shard_map/ppermute | solution.py:30
  126.7 14.3 %collective-permute-start.8 = (bf16[32,2048]{1,0:T(8,128)(2,1)S(1)}, bf16[32,2048]{1,0:T(8,128)(2,1)S(1)}, u32[]{:S(2)}, u32[]{:S(2)}) collective-permute-start(bf16[32,2048]{1,0:T(8,128)(2,1)S(1)} %copy-done), channel_id=1, source_target_pairs={{0,28},{2,30},{4,0},{6,2},{8,4},{10,6},{12,8},{14,10},{16,12},{18,... | collective-permute-start | bytes 393224 | tf_op jit(solution)/shard_map/ppermute | solution.py:30
  131.3 10.4 %collective-permute-start.11 = (bf16[32,2048]{1,0:T(8,128)(2,1)S(1)}, bf16[32,2048]{1,0:T(8,128)(2,1)S(1)}, u32[]{:S(2)}, u32[]{:S(2)}) collective-permute-start(bf16[32,2048]{1,0:T(8,128)(2,1)S(1)} %collective-permute-done.2.refs_3_), channel_id=1, source_target_pairs={{0,4},{2,6},{4,8},{6,10},{8,12},{10,14},{12,16},{14,18},{16,20},{1... | collective-permute-start | bytes 393224 | tf_op jit(solution)/shard_map/ppermute | solution.py:30
  133.5 11.6 %collective-permute-start.9 = (bf16[32,2048]{1,0:T(8,128)(2,1)S(1)}, bf16[32,2048]{1,0:T(8,128)(2,1)S(1)}, u32[]{:S(2)}, u32[]{:S(2)}) collective-permute-start(bf16[32,2048]{1,0:T(8,128)(2,1)S(1)} %collective-permute-done.1.refs_2_), channel_id=1, source_target_pairs={{0,28},{2,30},{4,0},{6,2},{8,4},{10,6},{12,8},{14,10},{16,12},{18,... | collective-permute-start | bytes 393224 | tf_op jit(solution)/shard_map/ppermute | solution.py:30
  146.6 11.2 %collective-permute-start.12 = (bf16[64,2048]{1,0:T(8,128)(2,1)S(1)}, bf16[64,2048]{1,0:T(8,128)(2,1)S(1)}, u32[]{:S(2)}, u32[]{:S(2)}) collective-permute-start(bf16[64,2048]{1,0:T(8,128)(2,1)S(1)} %get-tuple-element.12), channel_id=1, source_target_pairs={{0,4},{2,6},{4,8},{6,10},{8,12},{10,14},{12,16},{14,18},{16,20},{1... | collective-permute-start | bytes 786440 | tf_op jit(solution)/shard_map/ppermute | solution.py:30
  149.7 12.6 %collective-permute-start.13 = (bf16[64,2048]{1,0:T(8,128)(2,1)S(1)}, bf16[64,2048]{1,0:T(8,128)(2,1)S(1)}, u32[]{:S(2)}, u32[]{:S(2)}) collective-permute-start(bf16[64,2048]{1,0:T(8,128)(2,1)S(1)} %get-tuple-element.13), channel_id=1, source_target_pairs={{0,28},{2,30},{4,0},{6,2},{8,4},{10,6},{12,8},{14,10},{16,12},{18,... | collective-permute-start | bytes 786440 | tf_op jit(solution)/shard_map/ppermute | solution.py:30
  162.5 20.0 %collective-permute-start.15 = (bf16[32,2048]{1,0:T(8,128)(2,1)S(1)}, bf16[32,2048]{1,0:T(8,128)(2,1)S(1)}, u32[]{:S(2)}, u32[]{:S(2)}) collective-permute-start(bf16[32,2048]{1,0:T(8,128)(2,1)S(1)} %get-tuple-element.14), channel_id=1, source_target_pairs={{0,8},{2,10},{4,12},{6,14},{8,16},{10,18},{12,20},{14,22},{16,24},... | collective-permute-start | bytes 393224 | tf_op jit(solution)/shard_map/ppermute | solution.py:30
  171.0 14.1 %collective-permute-start.16 = (bf16[32,2048]{1,0:T(8,128)(2,1)S(1)}, bf16[32,2048]{1,0:T(8,128)(2,1)S(1)}, u32[]{:S(2)}, u32[]{:S(2)}) collective-permute-start(bf16[32,2048]{1,0:T(8,128)(2,1)S(1)} %get-tuple-element.15), channel_id=1, source_target_pairs={{0,24},{2,26},{4,28},{6,30},{8,0},{10,2},{12,4},{14,6},{16,8},{18,... | collective-permute-start | bytes 393224 | tf_op jit(solution)/shard_map/ppermute | solution.py:30
  173.0 20.6 %collective-permute-start.14 = (bf16[32,2048]{1,0:T(8,128)(2,1)S(1)}, bf16[32,2048]{1,0:T(8,128)(2,1)S(1)}, u32[]{:S(2)}, u32[]{:S(2)}) collective-permute-start(bf16[32,2048]{1,0:T(8,128)(2,1)S(1)} %shard_map.88), channel_id=1, source_target_pairs={{0,16},{2,18},{4,20},{6,22},{8,24},{10,26},{12,28},{14,30},{16,0},... | collective-permute-start | bytes 393224 | tf_op jit(solution)/shard_map/ppermute | solution.py:30

commit v6 on v3

--- a/solution.py
+++ b/solution.py
@@ -7,8 +7,9 @@
 from jax.sharding import PartitionSpec as P
 
 
-TP = ("z", "c")
-ROWS = ("fs", "z", "c")
+Z = ("zh", "zl")
+TP = (*Z, "c")
+ROWS = ("fs", *TP)
 VMEM = pl.BlockSpec(memory_space=pltpu.VMEM)
 PARAMS = pltpu.CompilerParams(vmem_limit_bytes=32 * 1024 * 1024)
 
@@ -26,8 +27,8 @@
 
 
 def move(array, by):
-    planes = lax.axis_size("z")
-    return lax.ppermute(array, "z", [(i, (i + by) % planes) for i in range(planes)])
+    planes = lax.axis_size(Z)
+    return lax.ppermute(array, Z, [(i, (i + by) % planes) for i in range(planes)])
 
 
 def copies_kernel(gain_hbm, gate_hbm, up_hbm, down_hbm, out_hbm, gain_ref, wide_ref, shard_ref, in_sems, out_sems):
@@ -71,19 +72,6 @@
         cost_estimate=pl.CostEstimate(flops=1000000, bytes_accessed=4000000, transcendentals=0),
         name="prepare",
     )(norm_gain.reshape(1, -1), gate_master, up_master, down_master)
-
-
-def pack_kernel(*refs):
-    *parts, out_ref = refs
-    at = 0
-    for ref in parts:
-        out_ref[at : at + ref.shape[0]] = ref[...]
-        at += ref.shape[0]
-
-
-def pack(*parts):
-    count = sum(p.shape[0] for p in parts)
-    return local(pack_kernel, (jax.ShapeDtypeStruct((count, parts[0].shape[1]), parts[0].dtype),), *parts)[0]
 
 
 def sums_kernel(count, *refs):
@@ -134,25 +122,33 @@
         out_ref[...] = total.astype(out_ref.dtype)
 
 
-def mix_kernel(tokens_ref, own_ref, next_ref, prev_ref, next2_ref, prev2_ref, far_ref, above_ref, below_ref, out_ref):
-    rows = tokens_ref.shape[0]
-    total = own_ref[:rows]
-    for ref in (next_ref, prev_ref, next2_ref, prev2_ref, far_ref, above_ref, below_ref):
-        total = total + ref[:rows].astype(jnp.float32)
+def mix_kernel(tokens_ref, sums_ref, out_ref):
+    total = sums_ref[0].astype(jnp.float32)
+    for k in range(1, sums_ref.shape[0]):
+        total = total + sums_ref[k].astype(jnp.float32)
     out_ref[...] = (tokens_ref[...].astype(jnp.float32) + 0.5 * total).astype(out_ref.dtype)
 
 
+def fold_kernel(own_ref, next_ref, prev_ref, next2_ref, prev2_ref, out_ref):
+    half = out_ref.shape[0] // 2
+    for at, ref in ((0, next2_ref), (half, prev2_ref)):
+        total = own_ref[at : at + half]
+        for other in (next_ref, prev_ref):
+            total = total + other[at : at + half].astype(jnp.float32)
+        out_ref[at : at + half] = (total + ref[...].astype(jnp.float32)).astype(out_ref.dtype)
+
+
 def step(tokens, norm_gain, gate_master, up_master, down_master):
-    far = move(tokens, 8)
+    rows, width = tokens.shape
+    groups = lax.axis_size("zh")
     copies = weight_copies(norm_gain, gate_master, up_master, down_master, lax.axis_size("fs"))
     packed = lax.all_to_all(copies, "fs", split_axis=0, concat_axis=0, tiled=True)
-    above = move(tokens, -4)
-    below = move(tokens, 4)
-    held = pack(tokens, far, above, below)
+    held = lax.all_gather(tokens, "zh", axis=0, tiled=True)
+    half = groups // 2 * rows
     from_next = move(held, -1)
     from_prev = move(held, 1)
-    from_next2 = move(pack(tokens, above), -2)
-    from_prev2 = move(pack(tokens, below), 2)
+    from_next2 = move(held[:half], -2)
+    from_prev2 = move(held[half:], 2)
 
     partner = lax.ppermute(packed, "c", [(0, 1), (1, 0)])
     weights = (packed, partner)
@@ -165,19 +161,14 @@
     to_prev2 = move(twos_prev, -2)
     (own,) = partial_sums((held,), weights, 1, jnp.float32)
 
-    block = jax.ShapeDtypeStruct(tokens.shape, jnp.bfloat16)
-    (sum_far,) = local(lambda *refs: fold_kernel((((0, 1), (1, 1), (2, 1)),), *refs), (block,), own, to_next, to_prev)
-    back_far = move(sum_far, 8)
-    terms = (((0, 2), (1, 2), (2, 2), (3, 1)), ((0, 3), (1, 3), (2, 3), (4, 1)))
-    sum_above, sum_below = local(lambda *refs: fold_kernel(terms, *refs), (block, block), own, to_next, to_prev, to_next2, to_prev2)
-    back_above = move(sum_above, 4)
-    back_below = move(sum_below, -4)
-    (mixed,) = local(mix_kernel, (block,), tokens, own, to_next, to_prev, to_next2, to_prev2, back_far, back_above, back_below)
+    (sums,) = local(fold_kernel, (jax.ShapeDtypeStruct((groups * rows, width), jnp.bfloat16),), own, to_next, to_prev, to_next2, to_prev2)
+    sums = lax.all_to_all(sums.reshape(groups, rows, width), "zh", split_axis=0, concat_axis=0, tiled=True)
+    (mixed,) = local(mix_kernel, (jax.ShapeDtypeStruct((rows, width), jnp.bfloat16),), tokens, sums)
     return (mixed, *(packed[:, k].reshape(-1, packed.shape[-1]) for k in range(3)))
 
 
 def solution(mesh):
-    split = Mesh(mesh.devices.reshape(mesh.shape["fs"], 16, 2), ROWS)
+    split = Mesh(mesh.devices.reshape(mesh.shape["fs"], 4, 4, 2), ROWS)
     placed = (P(ROWS, None), P("fs"), P("fs", TP), P("fs", TP), P("fs", TP))
     return jax.shard_map(
         step,

time: 184 us -> 171 us (0.929)
  blocking collectives: 46.8 us -> 78.8 us
  starting transfers between devices: 78 us -> 49.1 us
  waiting for transfers between devices: 47.6 us -> 29.3 us
    ppermute x14 -> x8, starting transfers between devices: 76.1 us -> 34.3 us  [move(): lax.ppermute(array, Z, [(i, (i + by) % planes) for i in range(planes)])]
    ppermute x14 -> x8, waiting for transfers between devices: 47.6 us -> 13.6 us  [move(): lax.ppermute(array, Z, [(i, (i + by) % planes) for i in range(planes)])]
    all_gather x0 -> x1, blocking collectives: none -> 32 us  [step(): held = lax.all_gather(tokens, 'zh', axis=0, tiled=True)]
    all_to_all x0 -> x1, waiting for transfers between devices: none -> 15.8 us  [step(): lax.all_to_all(sums.reshape(groups, rows, width), 'zh', split_axis=0, con...]
    all_to_all x0 -> x1, starting transfers between devices: none -> 12.8 us  [step(): lax.all_to_all(sums.reshape(groups, rows, width), 'zh', split_axis=0, con...]
    pallas_call x9 -> x5, Pallas kernels: 5.87 us -> 6.84 us  [local(): pl.pallas_call(kernel, out_shape=outs, in_specs=[VMEM] * len(args), out_s...]
  transfers between devices with their start and end apart: 15 -> 10, of which waited for: 7 -> 5; matrix products, arithmetic and copies ran while one was open for 1% -> 1% of each run, Pallas kernels for 3% -> 3%
where the time goes in v6:
time: 171 us; the launch traced here: 170 us
  blocking collectives  78.8 us (46%)
  starting transfers between devices  49.1 us (29%)
  waiting for transfers between devices  29.3 us (17%)
  Pallas kernels  9.72 us (6%)
  local copies, waits for them, and re-layouts  2.57 us (2%)
    all_to_all x1, blocking collectives, step(): lax.all_to_all(copies, 'fs', split_axis=0, concat_axis=0, tiled=True)  46.8 us
    ppermute x8, starting transfers between devices, move(): lax.ppermute(array, Z, [(i, (i + by) % planes) for i in range(planes)])  34.3 us
    all_gather x1, blocking collectives, step(): held = lax.all_gather(tokens, 'zh', axis=0, tiled=True)  32 us
    all_to_all x1, waiting for transfers between devices, step(): lax.all_to_all(sums.reshape(groups, rows, width), 'zh', split_axis=0, con...  15.8 us
    ppermute x8, waiting for transfers between devices, move(): lax.ppermute(array, Z, [(i, (i + by) % planes) for i in range(planes)])  13.6 us
    all_to_all x1, starting transfers between devices, step(): lax.all_to_all(sums.reshape(groups, rows, width), 'zh', split_axis=0, con...  12.8 us
    pallas_call x5, Pallas kernels, local(): pl.pallas_call(kernel, out_shape=outs, in_specs=[VMEM] * len(args), out_s...  6.84 us
  transfers between devices with their start and end apart: 10, of which 5 were waited for; matrix products, arithmetic and copies ran while one was open for 1% of the time, Pallas kernels for 3%

profile of v6, /device:TPU:64, one launch (start us, length us, event | category | flops | bytes accessed | tf_op | source)
XLA Modules:
  0.0 170.3 jit_solution(7244806364767698296)
XLA Ops:
  0.6 2.9 %prepare.1 = bf16[16,3,128,256]{3,2,1,0:T(8,128)(2,1)} custom-call(f32[1,128]{1,0:T(1,128)} %bitcast.9, f32[128,256]{1,0:T(8,128)} %gate_hbm.1, f32[128,256]{1,0:T(8,128)} %up_hbm.1, f32[128,256]{1,0:T(8,128)} %down_hbm.1), custom_call_target="tpu_custom_call" | custom-call | flops 1000000 | bytes 4000000 | tf_op jit(solution)/shard_map/prepare/pallas_call | solution.py:59
  3.5 0.0 copy-start.1
  3.5 46.8 %all_to_all.10.refs_1_.refs_2_ = bf16[16,3,128,256]{3,2,1,0:T(8,128)(2,1)S(1)} all-to-all(bf16[16,3,128,256]{3,2,1,0:T(8,128)(2,1)} %prepare.1), channel_id=1, replica_groups=mesh['fs'=16,'zh'=4,'zl'=4,'c'=2] {'fs'}, dimensions={0} | all-to-all | bytes 6291456 | tf_op jit(solution)/shard_map/all_to_all | solution.py:145
  50.3 1.9 %collective-permute-start = (bf16[16,3,128,256]{3,2,1,0:T(8,128)(2,1)S(1)}, bf16[16,3,128,256]{3,2,1,0:T(8,128)(2,1)S(1)}, u32[]{:S(2)}, u32[]{:S(2)}) collective-permute-start(bf16[16,3,128,256]{3,2,1,0:T(8,128)(2,1)S(1)} %all_to_all.10.refs_1_.refs_2_), channel_id=1, source_target_pairs={{0,1},{1,0},{2,3},{3,2},{4,5},{5,4},{6,7},{7,6},{8,9},{9,8},{10,11... | collective-permute-start | bytes 9437192 | tf_op jit(solution)/shard_map/ppermute | solution.py:153
  52.3 0.0 copy-done.1
  52.3 32.0 %all_gather.3.refs_0_ = bf16[128,2048]{1,0:T(8,128)(2,1)S(1)} all-gather(bf16[32,2048]{1,0:T(8,128)(2,1)S(1)} %copy-done.1), channel_id=1, replica_groups=mesh['fs'=16,'zh'=4,'zl'=4,'c'=2] {'zh'}, dimensions={0}, use_global_device_ids=true | all-gather | bytes 655360 | tf_op jit(solution)/shard_map/all_gather | solution.py:146
  84.3 3.4 %collective-permute-start.1 = (bf16[128,2048]{1,0:T(8,128)(2,1)S(1)}, bf16[128,2048]{1,0:T(8,128)(2,1)S(1)}, u32[]{:S(2)}, u32[]{:S(2)}) collective-permute-start(bf16[128,2048]{1,0:T(8,128)(2,1)S(1)} %all_gather.3.refs_0_), channel_id=1, source_target_pairs={{0,30},{2,0},{4,2},{6,4},{8,6},{10,8},{12,10},{14,12},{16,14},{18,... | collective-permute-start | bytes 1572872 | tf_op jit(solution)/shard_map/ppermute | solution.py:31
  87.7 2.5 %collective-permute-start.2 = (bf16[128,2048]{1,0:T(8,128)(2,1)S(1)}, bf16[128,2048]{1,0:T(8,128)(2,1)S(1)}, u32[]{:S(2)}, u32[]{:S(2)}) collective-permute-start(bf16[128,2048]{1,0:T(8,128)(2,1)S(1)} %all_gather.3.refs_0_), channel_id=1, source_target_pairs={{0,2},{2,4},{4,6},{6,8},{8,10},{10,12},{12,14},{14,16},{16,18},{18... | collective-permute-start | bytes 1572872 | tf_op jit(solution)/shard_map/ppermute | solution.py:31
  90.3 4.1 %collective-permute-start.5 = (bf16[64,2048]{1,0:T(8,128)(2,1)S(1)}, bf16[64,2048]{1,0:T(8,128)(2,1)S(1)}, u32[]{:S(2)}, u32[]{:S(2)}) collective-permute-start(bf16[64,2048]{1,0:T(8,128)(2,1)S(1)} %get-tuple-element.16), channel_id=1, source_target_pairs={{0,28},{2,30},{4,0},{6,2},{8,4},{10,6},{12,8},{14,10},{16,12},{18,... | collective-permute-start | bytes 786440 | tf_op jit(solution)/shard_map/ppermute | solution.py:31
  94.4 3.9 %collective-permute-start.6 = (bf16[64,2048]{1,0:T(8,128)(2,1)S(1)}, bf16[64,2048]{1,0:T(8,128)(2,1)S(1)}, u32[]{:S(2)}, u32[]{:S(2)}) collective-permute-start(bf16[64,2048]{1,0:T(8,128)(2,1)S(1)} %get-tuple-element.15), channel_id=1, source_target_pairs={{0,4},{2,6},{4,8},{6,10},{8,12},{10,14},{12,16},{14,18},{16,20},{1... | collective-permute-start | bytes 786440 | tf_op jit(solution)/shard_map/ppermute | solution.py:31
  98.3 3.9 %collective-permute-done.1.refs_0_ = bf16[128,2048]{1,0:T(8,128)(2,1)S(1)} collective-permute-done((bf16[128,2048]{1,0:T(8,128)(2,1)S(1)}, bf16[128,2048]{1,0:T(8,128)(2,1)S(1)}, u32[]{:S(2)}, u32[]{:S(2)}) %collective-permute-start.1) | collective-permute-done | bytes 524320 | tf_op jit(solution)/shard_map/ppermute | solution.py:31
  102.1 1.1 collective-permute-done.2.refs_1_
  103.2 0.0 collective-permute-done.refs_2_.refs_3_
  103.3 1.9 %shard_map.85 = (bf16[128,2048]{1,0:T(8,128)(2,1)S(1)}, bf16[128,2048]{1,0:T(8,128)(2,1)S(1)}) custom-call(bf16[128,2048]{1,0:T(8,128)(2,1)S(1)} %collective-permute-done.1.refs_0_, bf16[128,2048]{1,0:T(8,128)(2,1)S(1)} %collective-permute-done.2.refs_1_, bf16[16,3,128,256]{3,2,1,0:T(8,128)(2,1)S(1)} %all_to_all.10.refs_1_.refs_2_, ...), custom_call_target="tpu_custom_call" | custom-call | flops 1610612736 | bytes 8388608 | tf_op jit(solution)/shard_map/pallas_call | solution.py:19
  105.2 8.0 %collective-permute-start.3 = (bf16[128,2048]{1,0:T(8,128)(2,1)S(1)}, bf16[128,2048]{1,0:T(8,128)(2,1)S(1)}, u32[]{:S(2)}, u32[]{:S(2)}) collective-permute-start(bf16[128,2048]{1,0:T(8,128)(2,1)S(1)} %get-tuple-element.8), channel_id=1, source_target_pairs={{0,2},{2,4},{4,6},{6,8},{8,10},{10,12},{12,14},{14,16},{16,18},{18... | collective-permute-start | bytes 1572872 | tf_op jit(solution)/shard_map/ppermute | solution.py:31
  113.2 1.9 %collective-permute-start.4 = (bf16[128,2048]{1,0:T(8,128)(2,1)S(1)}, bf16[128,2048]{1,0:T(8,128)(2,1)S(1)}, u32[]{:S(2)}, u32[]{:S(2)}) collective-permute-start(bf16[128,2048]{1,0:T(8,128)(2,1)S(1)} %get-tuple-element.9), channel_id=1, source_target_pairs={{0,30},{2,0},{4,2},{6,4},{8,6},{10,8},{12,10},{14,12},{16,14},{18,... | collective-permute-start | bytes 1572872 | tf_op jit(solution)/shard_map/ppermute | solution.py:31
  115.1 0.0 collective-permute-done.5.refs_0_
  115.2 0.0 collective-permute-done.6.refs_1_
  115.2 1.5 shard_map.86
  116.6 8.6 %collective-permute-start.7 = (bf16[64,2048]{1,0:T(8,128)(2,1)S(1)}, bf16[64,2048]{1,0:T(8,128)(2,1)S(1)}, u32[]{:S(2)}, u32[]{:S(2)}) collective-permute-start(bf16[64,2048]{1,0:T(8,128)(2,1)S(1)} %get-tuple-element.10), channel_id=1, source_target_pairs={{0,4},{2,6},{4,8},{6,10},{8,12},{10,14},{12,16},{14,18},{16,20},{1... | collective-permute-start | bytes 786440 | tf_op jit(solution)/shard_map/ppermute | solution.py:31
  125.2 1.9 %collective-permute-start.8 = (bf16[64,2048]{1,0:T(8,128)(2,1)S(1)}, bf16[64,2048]{1,0:T(8,128)(2,1)S(1)}, u32[]{:S(2)}, u32[]{:S(2)}) collective-permute-start(bf16[64,2048]{1,0:T(8,128)(2,1)S(1)} %get-tuple-element.11), channel_id=1, source_target_pairs={{0,28},{2,30},{4,0},{6,2},{8,4},{10,6},{12,8},{14,10},{16,12},{18,... | collective-permute-start | bytes 786440 | tf_op jit(solution)/shard_map/ppermute | solution.py:31
  127.1 1.5 shard_map.84.own_ref
  128.6 4.6 %collective-permute-done.7.next2_ref = bf16[64,2048]{1,0:T(8,128)(2,1)S(1)} collective-permute-done((bf16[64,2048]{1,0:T(8,128)(2,1)S(1)}, bf16[64,2048]{1,0:T(8,128)(2,1)S(1)}, u32[]{:S(2)}, u32[]{:S(2)}) %collective-permute-start.7) | collective-permute-done | bytes 262176 | tf_op jit(solution)/shard_map/ppermute | solution.py:31
  133.2 4.0 %collective-permute-done.8.prev2_ref = bf16[64,2048]{1,0:T(8,128)(2,1)S(1)} collective-permute-done((bf16[64,2048]{1,0:T(8,128)(2,1)S(1)}, bf16[64,2048]{1,0:T(8,128)(2,1)S(1)}, u32[]{:S(2)}, u32[]{:S(2)}) %collective-permute-start.8) | collective-permute-done | bytes 262176 | tf_op jit(solution)/shard_map/ppermute | solution.py:31
  137.2 0.0 collective-permute-done.3.next_ref
  137.2 0.0 collective-permute-done.4.prev_ref
  137.2 0.2 shard_map.87
  137.4 0.0 copy-start
  137.4 0.8 copy-done
  138.2 12.8 %all-to-all-start.1 = ((bf16[4,32,2048]{2,1,0:T(8,128)(2,1)}), bf16[4,32,2048]{2,1,0:T(8,128)(2,1)}, u32[]{:S(2)}, u32[]{:S(2)}) async-start(bf16[4,32,2048]{2,1,0:T(8,128)(2,1)} %bitcast.5), calls=%async_computation.1 | async-start | bytes 1048576 | tf_op jit(solution)/shard_map/all_to_all | solution.py:165
  151.1 1.7 %fusion = (bf16[16,1,128,256]{3,2,1,0:T(8,128)(2,1)}, bf16[16,1,128,256]{3,2,1,0:T(8,128)(2,1)}, bf16[16,1,128,256]{3,2,1,0:T(8,128)(2,1)}) fusion(bf16[16,3,128,256]{3,2,1,0:T(8,128)(2,1)S(1)} %all_to_all.10.refs_1_.refs_2_), kind=kLoop, calls=%fused_computation | loop fusion | bytes 6291456 | tf_op jit(solution)/shard_map/slice | solution.py:167
  152.8 15.8 %all-to-all-done.1.sums_ref = bf16[4,32,2048]{2,1,0:T(8,128)(2,1)} async-done(((bf16[4,32,2048]{2,1,0:T(8,128)(2,1)}), bf16[4,32,2048]{2,1,0:T(8,128)(2,1)}, u32[]{:S(2)}, u32[]{:S(2)}) %all-to-all-start.1) | async-done | bytes 524320 | tf_op jit(solution)/shard_map/all_to_all | solution.py:165
  168.5 1.8 %shard_map.88 = bf16[32,2048]{1,0:T(8,128)(2,1)} custom-call(bf16[32,2048]{1,0:T(8,128)(2,1)S(1)} %copy-done.1, bf16[4,32,2048]{2,1,0:T(8,128)(2,1)} %all-to-all-done.1.sums_ref), custom_call_target="tpu_custom_call" | custom-call | bytes 786432 | tf_op jit(solution)/shard_map/pallas_call | solution.py:19
  (1 shorter events, 0.0 us)
Async XLA Ops:
  3.5 48.7 %copy-start.1 = (bf16[32,2048]{1,0:T(8,128)(2,1)S(1)}, bf16[32,2048]{1,0:T(8,128)(2,1)}, u32[]{:S(2)}) copy-start(bf16[32,2048]{1,0:T(8,128)(2,1)} %tokens_ref.1) | copy-start | bytes 393220
  50.3 52.9 %collective-permute-start = (bf16[16,3,128,256]{3,2,1,0:T(8,128)(2,1)S(1)}, bf16[16,3,128,256]{3,2,1,0:T(8,128)(2,1)S(1)}, u32[]{:S(2)}, u32[]{:S(2)}) collective-permute-start(bf16[16,3,128,256]{3,2,1,0:T(8,128)(2,1)S(1)} %all_to_all.10.refs_1_.refs_2_), channel_id=1, source_target_pairs={{0,1},{1,0},{2,3},{3,2},{4,5},{5,4},{6,7},{7,6},{8,9},{9,8},{10,11... | collective-permute-start | bytes 9437192 | tf_op jit(solution)/shard_map/ppermute | solution.py:153
  84.3 17.9 %collective-permute-start.1 = (bf16[128,2048]{1,0:T(8,128)(2,1)S(1)}, bf16[128,2048]{1,0:T(8,128)(2,1)S(1)}, u32[]{:S(2)}, u32[]{:S(2)}) collective-permute-start(bf16[128,2048]{1,0:T(8,128)(2,1)S(1)} %all_gather.3.refs_0_), channel_id=1, source_target_pairs={{0,30},{2,0},{4,2},{6,4},{8,6},{10,8},{12,10},{14,12},{16,14},{18,... | collective-permute-start | bytes 1572872 | tf_op jit(solution)/shard_map/ppermute | solution.py:31
  87.7 15.5 %collective-permute-start.2 = (bf16[128,2048]{1,0:T(8,128)(2,1)S(1)}, bf16[128,2048]{1,0:T(8,128)(2,1)S(1)}, u32[]{:S(2)}, u32[]{:S(2)}) collective-permute-start(bf16[128,2048]{1,0:T(8,128)(2,1)S(1)} %all_gather.3.refs_0_), channel_id=1, source_target_pairs={{0,2},{2,4},{4,6},{6,8},{8,10},{10,12},{12,14},{14,16},{16,18},{18... | collective-permute-start | bytes 1572872 | tf_op jit(solution)/shard_map/ppermute | solution.py:31
  90.3 24.9 %collective-permute-start.5 = (bf16[64,2048]{1,0:T(8,128)(2,1)S(1)}, bf16[64,2048]{1,0:T(8,128)(2,1)S(1)}, u32[]{:S(2)}, u32[]{:S(2)}) collective-permute-start(bf16[64,2048]{1,0:T(8,128)(2,1)S(1)} %get-tuple-element.16), channel_id=1, source_target_pairs={{0,28},{2,30},{4,0},{6,2},{8,4},{10,6},{12,8},{14,10},{16,12},{18,... | collective-permute-start | bytes 786440 | tf_op jit(solution)/shard_map/ppermute | solution.py:31
  94.4 20.8 %collective-permute-start.6 = (bf16[64,2048]{1,0:T(8,128)(2,1)S(1)}, bf16[64,2048]{1,0:T(8,128)(2,1)S(1)}, u32[]{:S(2)}, u32[]{:S(2)}) collective-permute-start(bf16[64,2048]{1,0:T(8,128)(2,1)S(1)} %get-tuple-element.15), channel_id=1, source_target_pairs={{0,4},{2,6},{4,8},{6,10},{8,12},{10,14},{12,16},{14,18},{16,20},{1... | collective-permute-start | bytes 786440 | tf_op jit(solution)/shard_map/ppermute | solution.py:31
  105.2 32.0 %collective-permute-start.3 = (bf16[128,2048]{1,0:T(8,128)(2,1)S(1)}, bf16[128,2048]{1,0:T(8,128)(2,1)S(1)}, u32[]{:S(2)}, u32[]{:S(2)}) collective-permute-start(bf16[128,2048]{1,0:T(8,128)(2,1)S(1)} %get-tuple-element.8), channel_id=1, source_target_pairs={{0,2},{2,4},{4,6},{6,8},{8,10},{10,12},{12,14},{14,16},{16,18},{18... | collective-permute-start | bytes 1572872 | tf_op jit(solution)/shard_map/ppermute | solution.py:31
  113.2 24.0 %collective-permute-start.4 = (bf16[128,2048]{1,0:T(8,128)(2,1)S(1)}, bf16[128,2048]{1,0:T(8,128)(2,1)S(1)}, u32[]{:S(2)}, u32[]{:S(2)}) collective-permute-start(bf16[128,2048]{1,0:T(8,128)(2,1)S(1)} %get-tuple-element.9), channel_id=1, source_target_pairs={{0,30},{2,0},{4,2},{6,4},{8,6},{10,8},{12,10},{14,12},{16,14},{18,... | collective-permute-start | bytes 1572872 | tf_op jit(solution)/shard_map/ppermute | solution.py:31
  116.6 16.5 %collective-permute-start.7 = (bf16[64,2048]{1,0:T(8,128)(2,1)S(1)}, bf16[64,2048]{1,0:T(8,128)(2,1)S(1)}, u32[]{:S(2)}, u32[]{:S(2)}) collective-permute-start(bf16[64,2048]{1,0:T(8,128)(2,1)S(1)} %get-tuple-element.10), channel_id=1, source_target_pairs={{0,4},{2,6},{4,8},{6,10},{8,12},{10,14},{12,16},{14,18},{16,20},{1... | collective-permute-start | bytes 786440 | tf_op jit(solution)/shard_map/ppermute | solution.py:31
  125.2 12.0 %collective-permute-start.8 = (bf16[64,2048]{1,0:T(8,128)(2,1)S(1)}, bf16[64,2048]{1,0:T(8,128)(2,1)S(1)}, u32[]{:S(2)}, u32[]{:S(2)}) collective-permute-start(bf16[64,2048]{1,0:T(8,128)(2,1)S(1)} %get-tuple-element.11), channel_id=1, source_target_pairs={{0,28},{2,30},{4,0},{6,2},{8,4},{10,6},{12,8},{14,10},{16,12},{18,... | collective-permute-start | bytes 786440 | tf_op jit(solution)/shard_map/ppermute | solution.py:31
  137.4 0.8 copy-start
  138.2 30.3 %all-to-all-start.1 = ((bf16[4,32,2048]{2,1,0:T(8,128)(2,1)}), bf16[4,32,2048]{2,1,0:T(8,128)(2,1)}, u32[]{:S(2)}, u32[]{:S(2)}) async-start(bf16[4,32,2048]{2,1,0:T(8,128)(2,1)} %bitcast.5), calls=%async_computation.1 | async-start | bytes 1048576 | tf_op jit(solution)/shard_map/all_to_all | solution.py:165

commit v7 on v3

--- a/solution.py
+++ b/solution.py
@@ -7,8 +7,9 @@
 from jax.sharding import PartitionSpec as P
 
 
-TP = ("z", "c")
-ROWS = ("fs", "z", "c")
+Z = ("zh", "zl")
+TP = (*Z, "c")
+ROWS = ("fs", *TP)
 VMEM = pl.BlockSpec(memory_space=pltpu.VMEM)
 PARAMS = pltpu.CompilerParams(vmem_limit_bytes=32 * 1024 * 1024)
 
@@ -26,8 +27,8 @@
 
 
 def move(array, by):
-    planes = lax.axis_size("z")
-    return lax.ppermute(array, "z", [(i, (i + by) % planes) for i in range(planes)])
+    planes = lax.axis_size(Z)
+    return lax.ppermute(array, Z, [(i, (i + by) % planes) for i in range(planes)])
 
 
 def copies_kernel(gain_hbm, gate_hbm, up_hbm, down_hbm, out_hbm, gain_ref, wide_ref, shard_ref, in_sems, out_sems):
@@ -73,17 +74,19 @@
     )(norm_gain.reshape(1, -1), gate_master, up_master, down_master)
 
 
-def pack_kernel(*refs):
-    *parts, out_ref = refs
-    at = 0
-    for ref in parts:
-        out_ref[at : at + ref.shape[0]] = ref[...]
-        at += ref.shape[0]
+def order_kernel(from_ref, held_ref, above_ref, below_ref):
+    rows = from_ref.shape[0] // 4
+    here = lax.axis_index("zh")
 
+    def block(by):
+        return from_ref[pl.ds(pl.multiple_of((here + by) % 4 * rows, rows), rows)]
 
-def pack(*parts):
-    count = sum(p.shape[0] for p in parts)
-    return local(pack_kernel, (jax.ShapeDtypeStruct((count, parts[0].shape[1]), parts[0].dtype),), *parts)[0]
+    own, above, below = block(0), block(1), block(3)
+    for k, value in enumerate((own, block(2), above, below)):
+        held_ref[k * rows : (k + 1) * rows] = value
+    for ref, value in ((above_ref, above), (below_ref, below)):
+        ref[:rows] = own
+        ref[rows:] = value
 
 
 def sums_kernel(count, *refs):
@@ -143,22 +146,23 @@
 
 
 def step(tokens, norm_gain, gate_master, up_master, down_master):
-    far = move(tokens, 8)
     copies = weight_copies(norm_gain, gate_master, up_master, down_master, lax.axis_size("fs"))
     packed = lax.all_to_all(copies, "fs", split_axis=0, concat_axis=0, tiled=True)
-    above = move(tokens, -4)
-    below = move(tokens, 4)
-    held = pack(tokens, far, above, below)
+    spread = lax.all_gather(tokens, "zh", axis=0, tiled=True)
+    rows, width = tokens.shape
+    shapes = tuple(jax.ShapeDtypeStruct((k * rows, width), tokens.dtype) for k in (4, 2, 2))
+    held, pair_above, pair_below = local(order_kernel, shapes, spread)
     from_next = move(held, -1)
     from_prev = move(held, 1)
-    from_next2 = move(pack(tokens, above), -2)
-    from_prev2 = move(pack(tokens, below), 2)
+    from_next2 = move(pair_above, -2)
+    from_prev2 = move(pair_below, 2)
 
     partner = lax.ppermute(packed, "c", [(0, 1), (1, 0)])
     weights = (packed, partner)
 
-    ones_next, ones_prev = partial_sums((from_next, from_prev), weights, 2, jnp.bfloat16)
+    (ones_next,) = partial_sums((from_next,), weights, 1, jnp.bfloat16)
     to_next = move(ones_next, 1)
+    (ones_prev,) = partial_sums((from_prev,), weights, 1, jnp.bfloat16)
     to_prev = move(ones_prev, -1)
     twos_next, twos_prev = partial_sums((from_next2, from_prev2), weights, 2, jnp.bfloat16)
     to_next2 = move(twos_next, 2)
@@ -177,7 +181,7 @@
 
 
 def solution(mesh):
-    split = Mesh(mesh.devices.reshape(mesh.shape["fs"], 16, 2), ROWS)
+    split = Mesh(mesh.devices.reshape(mesh.shape["fs"], 4, 4, 2), ROWS)
     placed = (P(ROWS, None), P("fs"), P("fs", TP), P("fs", TP), P("fs", TP))
     return jax.shard_map(
         step,

time: 184 us -> 171 us (0.929)
  the two profiles are of different devices: /device:TPU:64 before, /device:TPU:96 now
where the time goes in v7:
time: 171 us; the launch traced here: 170 us
  blocking collectives  79 us (46%)
  starting transfers between devices  42.8 us (25%)
  waiting for transfers between devices  36.1 us (21%)
  Pallas kernels  9.73 us (6%)
  local copies, waits for them, and re-layouts  1.76 us (1%)
    all_to_all x1, blocking collectives, step(): lax.all_to_all(copies, 'fs', split_axis=0, concat_axis=0, tiled=True)  46.8 us
    ppermute x11, starting transfers between devices, move(): lax.ppermute(array, Z, [(i, (i + by) % planes) for i in range(planes)])  40.8 us
    ppermute x11, waiting for transfers between devices, move(): lax.ppermute(array, Z, [(i, (i + by) % planes) for i in range(planes)])  36.1 us
    all_gather x1, blocking collectives, step(): spread = lax.all_gather(tokens, 'zh', axis=0, tiled=True)  32.2 us
    pallas_call x8, Pallas kernels, local(): pl.pallas_call(kernel, out_shape=outs, in_specs=[VMEM] * len(args), out_s...  6.84 us
  transfers between devices with their start and end apart: 12, of which 7 were waited for; matrix products, arithmetic and copies ran while one was open for 1% of the time, Pallas kernels for 3%

profile of v7, /device:TPU:96, one launch (start us, length us, event | category | flops | bytes accessed | tf_op | source)
XLA Modules:
  0.0 170.2 jit_solution(16284898016763595383)
XLA Ops:
  0.6 2.9 %prepare.1 = bf16[16,3,128,256]{3,2,1,0:T(8,128)(2,1)} custom-call(f32[1,128]{1,0:T(1,128)} %bitcast.7, f32[128,256]{1,0:T(8,128)} %gate_hbm.1, f32[128,256]{1,0:T(8,128)} %up_hbm.1, f32[128,256]{1,0:T(8,128)} %down_hbm.1), custom_call_target="tpu_custom_call" | custom-call | flops 1000000 | bytes 4000000 | tf_op jit(solution)/shard_map/prepare/pallas_call | solution.py:59
  3.5 0.0 copy-start
  3.5 46.8 %all_to_all.5.refs_1_.refs_2_ = bf16[16,3,128,256]{3,2,1,0:T(8,128)(2,1)S(1)} all-to-all(bf16[16,3,128,256]{3,2,1,0:T(8,128)(2,1)} %prepare.1), channel_id=1, replica_groups=mesh['fs'=16,'zh'=4,'zl'=4,'c'=2] {'fs'}, dimensions={0} | all-to-all | bytes 6291456 | tf_op jit(solution)/shard_map/all_to_all | solution.py:150
  50.3 1.9 %collective-permute-start = (bf16[16,3,128,256]{3,2,1,0:T(8,128)(2,1)S(1)}, bf16[16,3,128,256]{3,2,1,0:T(8,128)(2,1)S(1)}, u32[]{:S(2)}, u32[]{:S(2)}) collective-permute-start(bf16[16,3,128,256]{3,2,1,0:T(8,128)(2,1)S(1)} %all_to_all.5.refs_1_.refs_2_), channel_id=1, source_target_pairs={{0,1},{1,0},{2,3},{3,2},{4,5},{5,4},{6,7},{7,6},{8,9},{9,8},{10,11... | collective-permute-start | bytes 9437192 | tf_op jit(solution)/shard_map/ppermute | solution.py:160
  52.3 0.0 copy-done
  52.3 32.2 %all_gather.3.from_ref = bf16[128,2048]{1,0:T(8,128)(2,1)S(1)} all-gather(bf16[32,2048]{1,0:T(8,128)(2,1)S(1)} %copy-done), channel_id=1, replica_groups=mesh['fs'=16,'zh'=4,'zl'=4,'c'=2] {'zh'}, dimensions={0}, use_global_device_ids=true | all-gather | bytes 655360 | tf_op jit(solution)/shard_map/all_gather | solution.py:151
  84.5 0.1 shard_map.84
  84.6 4.0 %collective-permute-start.3 = (bf16[128,2048]{1,0:T(8,128)(2,1)S(1)}, bf16[128,2048]{1,0:T(8,128)(2,1)S(1)}, u32[]{:S(2)}, u32[]{:S(2)}) collective-permute-start(bf16[128,2048]{1,0:T(8,128)(2,1)S(1)} %get-tuple-element.11.refs_0_), channel_id=1, source_target_pairs={{0,2},{2,4},{4,6},{6,8},{8,10},{10,12},{12,14},{14,16},{16,18},{18... | collective-permute-start | bytes 1572872 | tf_op jit(solution)/shard_map/ppermute | solution.py:31
  88.6 1.9 %collective-permute-start.1 = (bf16[128,2048]{1,0:T(8,128)(2,1)S(1)}, bf16[128,2048]{1,0:T(8,128)(2,1)S(1)}, u32[]{:S(2)}, u32[]{:S(2)}) collective-permute-start(bf16[128,2048]{1,0:T(8,128)(2,1)S(1)} %get-tuple-element.11.refs_0_), channel_id=1, source_target_pairs={{0,30},{2,0},{4,2},{6,4},{8,6},{10,8},{12,10},{14,12},{16,14},{18,... | collective-permute-start | bytes 1572872 | tf_op jit(solution)/shard_map/ppermute | solution.py:31
  90.5 2.6 %collective-permute-start.5 = (bf16[64,2048]{1,0:T(8,128)(2,1)S(1)}, bf16[64,2048]{1,0:T(8,128)(2,1)S(1)}, u32[]{:S(2)}, u32[]{:S(2)}) collective-permute-start(bf16[64,2048]{1,0:T(8,128)(2,1)S(1)} %get-tuple-element.12), channel_id=1, source_target_pairs={{0,28},{2,30},{4,0},{6,2},{8,4},{10,6},{12,8},{14,10},{16,12},{18,... | collective-permute-start | bytes 786440 | tf_op jit(solution)/shard_map/ppermute | solution.py:31
  93.2 5.3 %collective-permute-start.6 = (bf16[64,2048]{1,0:T(8,128)(2,1)S(1)}, bf16[64,2048]{1,0:T(8,128)(2,1)S(1)}, u32[]{:S(2)}, u32[]{:S(2)}) collective-permute-start(bf16[64,2048]{1,0:T(8,128)(2,1)S(1)} %get-tuple-element.13), channel_id=1, source_target_pairs={{0,4},{2,6},{4,8},{6,10},{8,12},{10,14},{12,16},{14,18},{16,20},{1... | collective-permute-start | bytes 786440 | tf_op jit(solution)/shard_map/ppermute | solution.py:31
  98.5 3.9 %collective-permute-done.3.refs_0_ = bf16[128,2048]{1,0:T(8,128)(2,1)S(1)} collective-permute-done((bf16[128,2048]{1,0:T(8,128)(2,1)S(1)}, bf16[128,2048]{1,0:T(8,128)(2,1)S(1)}, u32[]{:S(2)}, u32[]{:S(2)}) %collective-permute-start.3) | collective-permute-done | bytes 524320 | tf_op jit(solution)/shard_map/ppermute | solution.py:31
  102.5 0.0 collective-permute-done.refs_2_.refs_3_
  102.5 1.5 shard_map.87
  103.9 1.9 %collective-permute-start.4 = (bf16[128,2048]{1,0:T(8,128)(2,1)S(1)}, bf16[128,2048]{1,0:T(8,128)(2,1)S(1)}, u32[]{:S(2)}, u32[]{:S(2)}) collective-permute-start(bf16[128,2048]{1,0:T(8,128)(2,1)S(1)} %shard_map.87), channel_id=1, source_target_pairs={{0,30},{2,0},{4,2},{6,4},{8,6},{10,8},{12,10},{14,12},{16,14},{18,... | collective-permute-start | bytes 1572872 | tf_op jit(solution)/shard_map/ppermute | solution.py:31
  105.8 4.2 %collective-permute-done.1.refs_0_ = bf16[128,2048]{1,0:T(8,128)(2,1)S(1)} collective-permute-done((bf16[128,2048]{1,0:T(8,128)(2,1)S(1)}, bf16[128,2048]{1,0:T(8,128)(2,1)S(1)}, u32[]{:S(2)}, u32[]{:S(2)}) %collective-permute-start.1) | collective-permute-done | bytes 524320 | tf_op jit(solution)/shard_map/ppermute | solution.py:31
  110.1 1.5 shard_map.86
  111.5 1.9 %collective-permute-start.2 = (bf16[128,2048]{1,0:T(8,128)(2,1)S(1)}, bf16[128,2048]{1,0:T(8,128)(2,1)S(1)}, u32[]{:S(2)}, u32[]{:S(2)}) collective-permute-start(bf16[128,2048]{1,0:T(8,128)(2,1)S(1)} %shard_map.86), channel_id=1, source_target_pairs={{0,2},{2,4},{4,6},{6,8},{8,10},{10,12},{12,14},{14,16},{16,18},{18... | collective-permute-start | bytes 1572872 | tf_op jit(solution)/shard_map/ppermute | solution.py:31
  113.5 2.5 %collective-permute-done.5.refs_0_ = bf16[64,2048]{1,0:T(8,128)(2,1)S(1)} collective-permute-done((bf16[64,2048]{1,0:T(8,128)(2,1)S(1)}, bf16[64,2048]{1,0:T(8,128)(2,1)S(1)}, u32[]{:S(2)}, u32[]{:S(2)}) %collective-permute-start.5) | collective-permute-done | bytes 262176 | tf_op jit(solution)/shard_map/ppermute | solution.py:31
  116.0 0.0 collective-permute-done.6.refs_1_
  116.0 1.4 shard_map.88
  117.4 3.3 %collective-permute-start.7 = (bf16[64,2048]{1,0:T(8,128)(2,1)S(1)}, bf16[64,2048]{1,0:T(8,128)(2,1)S(1)}, u32[]{:S(2)}, u32[]{:S(2)}) collective-permute-start(bf16[64,2048]{1,0:T(8,128)(2,1)S(1)} %get-tuple-element.14), channel_id=1, source_target_pairs={{0,4},{2,6},{4,8},{6,10},{8,12},{10,14},{12,16},{14,18},{16,20},{1... | collective-permute-start | bytes 786440 | tf_op jit(solution)/shard_map/ppermute | solution.py:31
  120.7 3.5 %collective-permute-start.8 = (bf16[64,2048]{1,0:T(8,128)(2,1)S(1)}, bf16[64,2048]{1,0:T(8,128)(2,1)S(1)}, u32[]{:S(2)}, u32[]{:S(2)}) collective-permute-start(bf16[64,2048]{1,0:T(8,128)(2,1)S(1)} %get-tuple-element.15), channel_id=1, source_target_pairs={{0,28},{2,30},{4,0},{6,2},{8,4},{10,6},{12,8},{14,10},{16,12},{18,... | collective-permute-start | bytes 786440 | tf_op jit(solution)/shard_map/ppermute | solution.py:31
  124.2 1.5 shard_map.85.refs_0_.own_ref
  125.7 5.8 %collective-permute-done.7.refs_3_.next2_ref = bf16[64,2048]{1,0:T(8,128)(2,1)S(1)} collective-permute-done((bf16[64,2048]{1,0:T(8,128)(2,1)S(1)}, bf16[64,2048]{1,0:T(8,128)(2,1)S(1)}, u32[]{:S(2)}, u32[]{:S(2)}) %collective-permute-start.7) | collective-permute-done | bytes 262176 | tf_op jit(solution)/shard_map/ppermute | solution.py:31
  131.5 1.6 collective-permute-done.8.refs_4_.prev2_ref
  133.1 0.6 collective-permute-done.4.refs_2_.prev_ref
  133.7 0.0 collective-permute-done.2.refs_1_.next_ref
  133.7 0.1 shard_map.90
  133.8 3.1 %collective-permute-start.10 = (bf16[32,2048]{1,0:T(8,128)(2,1)S(1)}, bf16[32,2048]{1,0:T(8,128)(2,1)S(1)}, u32[]{:S(2)}, u32[]{:S(2)}) collective-permute-start(bf16[32,2048]{1,0:T(8,128)(2,1)S(1)} %get-tuple-element.16), channel_id=1, source_target_pairs={{0,8},{2,10},{4,12},{6,14},{8,16},{10,18},{12,20},{14,22},{16,24},... | collective-permute-start | bytes 393224 | tf_op jit(solution)/shard_map/ppermute | solution.py:31
  136.9 6.6 %collective-permute-start.11 = (bf16[32,2048]{1,0:T(8,128)(2,1)S(1)}, bf16[32,2048]{1,0:T(8,128)(2,1)S(1)}, u32[]{:S(2)}, u32[]{:S(2)}) collective-permute-start(bf16[32,2048]{1,0:T(8,128)(2,1)S(1)} %get-tuple-element.17), channel_id=1, source_target_pairs={{0,24},{2,26},{4,28},{6,30},{8,0},{10,2},{12,4},{14,6},{16,8},{18,... | collective-permute-start | bytes 393224 | tf_op jit(solution)/shard_map/ppermute | solution.py:31
  143.6 6.6 %collective-permute-start.9 = (bf16[32,2048]{1,0:T(8,128)(2,1)S(1)}, bf16[32,2048]{1,0:T(8,128)(2,1)S(1)}, u32[]{:S(2)}, u32[]{:S(2)}) collective-permute-start(bf16[32,2048]{1,0:T(8,128)(2,1)S(1)} %shard_map.89), channel_id=1, source_target_pairs={{0,16},{2,18},{4,20},{6,22},{8,24},{10,26},{12,28},{14,30},{16,0},... | collective-permute-start | bytes 393224 | tf_op jit(solution)/shard_map/ppermute | solution.py:31
  150.2 1.8 %fusion = (bf16[16,1,128,256]{3,2,1,0:T(8,128)(2,1)}, bf16[16,1,128,256]{3,2,1,0:T(8,128)(2,1)}, bf16[16,1,128,256]{3,2,1,0:T(8,128)(2,1)}) fusion(bf16[16,3,128,256]{3,2,1,0:T(8,128)(2,1)S(1)} %all_to_all.5.refs_1_.refs_2_), kind=kLoop, calls=%fused_computation | loop fusion | bytes 6291456 | tf_op jit(solution)/shard_map/slice | solution.py:180
  152.0 0.0 collective-permute-done.10.above_ref
  152.0 0.0 collective-permute-done.11.below_ref
  152.0 17.4 %collective-permute-done.9.far_ref = bf16[32,2048]{1,0:T(8,128)(2,1)S(1)} collective-permute-done((bf16[32,2048]{1,0:T(8,128)(2,1)S(1)}, bf16[32,2048]{1,0:T(8,128)(2,1)S(1)}, u32[]{:S(2)}, u32[]{:S(2)}) %collective-permute-start.9) | collective-permute-done | bytes 131104 | tf_op jit(solution)/shard_map/ppermute | solution.py:31
  169.3 0.8 shard_map.91
  (1 shorter events, 0.0 us)
Async XLA Ops:
  3.5 48.7 %copy-start = (bf16[32,2048]{1,0:T(8,128)(2,1)S(1)}, bf16[32,2048]{1,0:T(8,128)(2,1)}, u32[]{:S(2)}) copy-start(bf16[32,2048]{1,0:T(8,128)(2,1)} %tokens_ref.1) | copy-start | bytes 393220
  50.3 52.1 %collective-permute-start = (bf16[16,3,128,256]{3,2,1,0:T(8,128)(2,1)S(1)}, bf16[16,3,128,256]{3,2,1,0:T(8,128)(2,1)S(1)}, u32[]{:S(2)}, u32[]{:S(2)}) collective-permute-start(bf16[16,3,128,256]{3,2,1,0:T(8,128)(2,1)S(1)} %all_to_all.5.refs_1_.refs_2_), channel_id=1, source_target_pairs={{0,1},{1,0},{2,3},{3,2},{4,5},{5,4},{6,7},{7,6},{8,9},{9,8},{10,11... | collective-permute-start | bytes 9437192 | tf_op jit(solution)/shard_map/ppermute | solution.py:160
  84.6 17.9 %collective-permute-start.3 = (bf16[128,2048]{1,0:T(8,128)(2,1)S(1)}, bf16[128,2048]{1,0:T(8,128)(2,1)S(1)}, u32[]{:S(2)}, u32[]{:S(2)}) collective-permute-start(bf16[128,2048]{1,0:T(8,128)(2,1)S(1)} %get-tuple-element.11.refs_0_), channel_id=1, source_target_pairs={{0,2},{2,4},{4,6},{6,8},{8,10},{10,12},{12,14},{14,16},{16,18},{18... | collective-permute-start | bytes 1572872 | tf_op jit(solution)/shard_map/ppermute | solution.py:31
  88.6 21.5 %collective-permute-start.1 = (bf16[128,2048]{1,0:T(8,128)(2,1)S(1)}, bf16[128,2048]{1,0:T(8,128)(2,1)S(1)}, u32[]{:S(2)}, u32[]{:S(2)}) collective-permute-start(bf16[128,2048]{1,0:T(8,128)(2,1)S(1)} %get-tuple-element.11.refs_0_), channel_id=1, source_target_pairs={{0,30},{2,0},{4,2},{6,4},{8,6},{10,8},{12,10},{14,12},{16,14},{18,... | collective-permute-start | bytes 1572872 | tf_op jit(solution)/shard_map/ppermute | solution.py:31
  90.5 25.4 %collective-permute-start.5 = (bf16[64,2048]{1,0:T(8,128)(2,1)S(1)}, bf16[64,2048]{1,0:T(8,128)(2,1)S(1)}, u32[]{:S(2)}, u32[]{:S(2)}) collective-permute-start(bf16[64,2048]{1,0:T(8,128)(2,1)S(1)} %get-tuple-element.12), channel_id=1, source_target_pairs={{0,28},{2,30},{4,0},{6,2},{8,4},{10,6},{12,8},{14,10},{16,12},{18,... | collective-permute-start | bytes 786440 | tf_op jit(solution)/shard_map/ppermute | solution.py:31
  93.2 22.8 %collective-permute-start.6 = (bf16[64,2048]{1,0:T(8,128)(2,1)S(1)}, bf16[64,2048]{1,0:T(8,128)(2,1)S(1)}, u32[]{:S(2)}, u32[]{:S(2)}) collective-permute-start(bf16[64,2048]{1,0:T(8,128)(2,1)S(1)} %get-tuple-element.13), channel_id=1, source_target_pairs={{0,4},{2,6},{4,8},{6,10},{8,12},{10,14},{12,16},{14,18},{16,20},{1... | collective-permute-start | bytes 786440 | tf_op jit(solution)/shard_map/ppermute | solution.py:31
  103.9 29.7 %collective-permute-start.4 = (bf16[128,2048]{1,0:T(8,128)(2,1)S(1)}, bf16[128,2048]{1,0:T(8,128)(2,1)S(1)}, u32[]{:S(2)}, u32[]{:S(2)}) collective-permute-start(bf16[128,2048]{1,0:T(8,128)(2,1)S(1)} %shard_map.87), channel_id=1, source_target_pairs={{0,30},{2,0},{4,2},{6,4},{8,6},{10,8},{12,10},{14,12},{16,14},{18,... | collective-permute-start | bytes 1572872 | tf_op jit(solution)/shard_map/ppermute | solution.py:31
  111.5 22.1 %collective-permute-start.2 = (bf16[128,2048]{1,0:T(8,128)(2,1)S(1)}, bf16[128,2048]{1,0:T(8,128)(2,1)S(1)}, u32[]{:S(2)}, u32[]{:S(2)}) collective-permute-start(bf16[128,2048]{1,0:T(8,128)(2,1)S(1)} %shard_map.86), channel_id=1, source_target_pairs={{0,2},{2,4},{4,6},{6,8},{8,10},{10,12},{12,14},{14,16},{16,18},{18... | collective-permute-start | bytes 1572872 | tf_op jit(solution)/shard_map/ppermute | solution.py:31
  117.4 14.0 %collective-permute-start.7 = (bf16[64,2048]{1,0:T(8,128)(2,1)S(1)}, bf16[64,2048]{1,0:T(8,128)(2,1)S(1)}, u32[]{:S(2)}, u32[]{:S(2)}) collective-permute-start(bf16[64,2048]{1,0:T(8,128)(2,1)S(1)} %get-tuple-element.14), channel_id=1, source_target_pairs={{0,4},{2,6},{4,8},{6,10},{8,12},{10,14},{12,16},{14,18},{16,20},{1... | collective-permute-start | bytes 786440 | tf_op jit(solution)/shard_map/ppermute | solution.py:31
  120.7 12.3 %collective-permute-start.8 = (bf16[64,2048]{1,0:T(8,128)(2,1)S(1)}, bf16[64,2048]{1,0:T(8,128)(2,1)S(1)}, u32[]{:S(2)}, u32[]{:S(2)}) collective-permute-start(bf16[64,2048]{1,0:T(8,128)(2,1)S(1)} %get-tuple-element.15), channel_id=1, source_target_pairs={{0,28},{2,30},{4,0},{6,2},{8,4},{10,6},{12,8},{14,10},{16,12},{18,... | collective-permute-start | bytes 786440 | tf_op jit(solution)/shard_map/ppermute | solution.py:31
  133.8 18.2 %collective-permute-start.10 = (bf16[32,2048]{1,0:T(8,128)(2,1)S(1)}, bf16[32,2048]{1,0:T(8,128)(2,1)S(1)}, u32[]{:S(2)}, u32[]{:S(2)}) collective-permute-start(bf16[32,2048]{1,0:T(8,128)(2,1)S(1)} %get-tuple-element.16), channel_id=1, source_target_pairs={{0,8},{2,10},{4,12},{6,14},{8,16},{10,18},{12,20},{14,22},{16,24},... | collective-permute-start | bytes 393224 | tf_op jit(solution)/shard_map/ppermute | solution.py:31
  136.9 15.0 %collective-permute-start.11 = (bf16[32,2048]{1,0:T(8,128)(2,1)S(1)}, bf16[32,2048]{1,0:T(8,128)(2,1)S(1)}, u32[]{:S(2)}, u32[]{:S(2)}) collective-permute-start(bf16[32,2048]{1,0:T(8,128)(2,1)S(1)} %get-tuple-element.17), channel_id=1, source_target_pairs={{0,24},{2,26},{4,28},{6,30},{8,0},{10,2},{12,4},{14,6},{16,8},{18,... | collective-permute-start | bytes 393224 | tf_op jit(solution)/shard_map/ppermute | solution.py:31
  143.6 25.8 %collective-permute-start.9 = (bf16[32,2048]{1,0:T(8,128)(2,1)S(1)}, bf16[32,2048]{1,0:T(8,128)(2,1)S(1)}, u32[]{:S(2)}, u32[]{:S(2)}) collective-permute-start(bf16[32,2048]{1,0:T(8,128)(2,1)S(1)} %shard_map.89), channel_id=1, source_target_pairs={{0,16},{2,18},{4,20},{6,22},{8,24},{10,26},{12,28},{14,30},{16,0},... | collective-permute-start | bytes 393224 | tf_op jit(solution)/shard_map/ppermute | solution.py:31

commit v8 on v7

--- a/solution.py
+++ b/solution.py
@@ -126,21 +126,34 @@
     )
 
 
-def fold_kernel(terms, *refs):
-    inputs, outputs = refs[: len(refs) - len(terms)], refs[len(refs) - len(terms) :]
-    for out_ref, pairs in zip(outputs, terms):
-        rows = out_ref.shape[0]
-        total = None
-        for which, k in pairs:
-            value = inputs[which][k * rows : (k + 1) * rows].astype(jnp.float32)
-            total = value if total is None else total + value
-        out_ref[...] = total.astype(out_ref.dtype)
-
-
-def mix_kernel(tokens_ref, own_ref, next_ref, prev_ref, next2_ref, prev2_ref, far_ref, above_ref, below_ref, out_ref):
+def fold_far_kernel(own_ref, next_ref, prev_ref, up_ref, down_ref):
+    half = up_ref.shape[0]
+    rows = 2 * half
+    for ref, at in ((up_ref, rows), (down_ref, rows + half)):
+        total = own_ref[at : at + half]
+        for other in (next_ref, prev_ref):
+            total = total + other[at : at + half].astype(jnp.float32)
+        ref[...] = total.astype(ref.dtype)
+
+
+def fold_near_kernel(own_ref, next_ref, prev_ref, next2_ref, prev2_ref, up_ref, down_ref, above_ref, below_ref):
+    rows = above_ref.shape[0]
+    half = rows // 2
+    for out_ref, block, second_ref, half_ref, at in ((above_ref, 2, next2_ref, up_ref, 0), (below_ref, 3, prev2_ref, down_ref, half)):
+        for part in (0, half):
+            lower = block * rows + part
+            total = own_ref[lower : lower + half] + second_ref[rows + part : rows + part + half].astype(jnp.float32)
+            for other in (next_ref, prev_ref):
+                total = total + other[lower : lower + half].astype(jnp.float32)
+            if part == at:
+                total = total + half_ref[...].astype(jnp.float32)
+            out_ref[part : part + half] = total.astype(out_ref.dtype)
+
+
+def mix_kernel(tokens_ref, own_ref, next_ref, prev_ref, next2_ref, prev2_ref, above_ref, below_ref, out_ref):
     rows = tokens_ref.shape[0]
     total = own_ref[:rows]
-    for ref in (next_ref, prev_ref, next2_ref, prev2_ref, far_ref, above_ref, below_ref):
+    for ref in (next_ref, prev_ref, next2_ref, prev2_ref, above_ref, below_ref):
         total = total + ref[:rows].astype(jnp.float32)
     out_ref[...] = (tokens_ref[...].astype(jnp.float32) + 0.5 * total).astype(out_ref.dtype)
 
@@ -169,14 +182,16 @@
     to_prev2 = move(twos_prev, -2)
     (own,) = partial_sums((held,), weights, 1, jnp.float32)
 
-    block = jax.ShapeDtypeStruct(tokens.shape, jnp.bfloat16)
-    (sum_far,) = local(lambda *refs: fold_kernel((((0, 1), (1, 1), (2, 1)),), *refs), (block,), own, to_next, to_prev)
-    back_far = move(sum_far, 8)
-    terms = (((0, 2), (1, 2), (2, 2), (3, 1)), ((0, 3), (1, 3), (2, 3), (4, 1)))
-    sum_above, sum_below = local(lambda *refs: fold_kernel(terms, *refs), (block, block), own, to_next, to_prev, to_next2, to_prev2)
+    block = jax.ShapeDtypeStruct((rows, width), jnp.bfloat16)
+    part = jax.ShapeDtypeStruct((rows // 2, width), jnp.bfloat16)
+    far_up, far_down = local(fold_far_kernel, (part, part), own, to_next, to_prev)
+    back_up = move(far_up, 4)
+    back_down = move(far_down, -4)
+    received = (own, to_next, to_prev, to_next2, to_prev2)
+    sum_above, sum_below = local(fold_near_kernel, (block, block), *received, back_up, back_down)
     back_above = move(sum_above, 4)
     back_below = move(sum_below, -4)
-    (mixed,) = local(mix_kernel, (block,), tokens, own, to_next, to_prev, to_next2, to_prev2, back_far, back_above, back_below)
+    (mixed,) = local(mix_kernel, (block,), tokens, *received, back_above, back_below)
     return (mixed, *(packed[:, k].reshape(-1, packed.shape[-1]) for k in range(3)))
 
 

time: 171 us -> 172 us (level)
  the two profiles are of different devices: /device:TPU:96 before, /device:TPU:6 now
where the time goes in v8:
time: 172 us; the launch traced here: 170 us
  blocking collectives  78 us (45%)
  starting transfers between devices  50.4 us (29%)
  waiting for transfers between devices  29.2 us (17%)
  Pallas kernels  9.72 us (6%)
  local copies, waits for them, and re-layouts  1.76 us (1%)
    ppermute x12, starting transfers between devices, move(): lax.ppermute(array, Z, [(i, (i + by) % planes) for i in range(planes)])  48.5 us
    all_to_all x1, blocking collectives, step(): lax.all_to_all(copies, 'fs', split_axis=0, concat_axis=0, tiled=True)  44.6 us
    all_gather x1, blocking collectives, step(): spread = lax.all_gather(tokens, 'zh', axis=0, tiled=True)  33.4 us
    ppermute x12, waiting for transfers between devices, move(): lax.ppermute(array, Z, [(i, (i + by) % planes) for i in range(planes)])  29.2 us
    pallas_call x8, Pallas kernels, local(): pl.pallas_call(kernel, out_shape=outs, in_specs=[VMEM] * len(args), out_s...  6.85 us
  transfers between devices with their start and end apart: 13, of which 6 were waited for; matrix products, arithmetic and copies ran while one was open for 1% of the time, Pallas kernels for 3%

profile of v8, /device:TPU:6, one launch (start us, length us, event | category | flops | bytes accessed | tf_op | source)
XLA Modules:
  0.0 169.9 jit_solution(4615870605024437416)
XLA Ops:
  0.6 2.9 %prepare.1 = bf16[16,3,128,256]{3,2,1,0:T(8,128)(2,1)} custom-call(f32[1,128]{1,0:T(1,128)} %bitcast.7, f32[128,256]{1,0:T(8,128)} %gate_hbm.1, f32[128,256]{1,0:T(8,128)} %up_hbm.1, f32[128,256]{1,0:T(8,128)} %down_hbm.1), custom_call_target="tpu_custom_call" | custom-call | flops 1000000 | bytes 4000000 | tf_op jit(solution)/shard_map/prepare/pallas_call | solution.py:59
  3.5 0.0 copy-start
  3.5 44.6 %all_to_all.5.refs_1_.refs_2_ = bf16[16,3,128,256]{3,2,1,0:T(8,128)(2,1)S(1)} all-to-all(bf16[16,3,128,256]{3,2,1,0:T(8,128)(2,1)} %prepare.1), channel_id=1, replica_groups=mesh['fs'=16,'zh'=4,'zl'=4,'c'=2] {'fs'}, dimensions={0} | all-to-all | bytes 6291456 | tf_op jit(solution)/shard_map/all_to_all | solution.py:163
  48.1 1.9 %collective-permute-start = (bf16[16,3,128,256]{3,2,1,0:T(8,128)(2,1)S(1)}, bf16[16,3,128,256]{3,2,1,0:T(8,128)(2,1)S(1)}, u32[]{:S(2)}, u32[]{:S(2)}) collective-permute-start(bf16[16,3,128,256]{3,2,1,0:T(8,128)(2,1)S(1)} %all_to_all.5.refs_1_.refs_2_), channel_id=1, source_target_pairs={{0,1},{1,0},{2,3},{3,2},{4,5},{5,4},{6,7},{7,6},{8,9},{9,8},{10,11... | collective-permute-start | bytes 9437192 | tf_op jit(solution)/shard_map/ppermute | solution.py:173
  50.0 0.0 copy-done
  50.0 33.4 %all_gather.3.from_ref = bf16[128,2048]{1,0:T(8,128)(2,1)S(1)} all-gather(bf16[32,2048]{1,0:T(8,128)(2,1)S(1)} %copy-done), channel_id=1, replica_groups=mesh['fs'=16,'zh'=4,'zl'=4,'c'=2] {'zh'}, dimensions={0}, use_global_device_ids=true | all-gather | bytes 655360 | tf_op jit(solution)/shard_map/all_gather | solution.py:164
  83.4 0.1 shard_map.84
  83.5 5.1 %collective-permute-start.1 = (bf16[128,2048]{1,0:T(8,128)(2,1)S(1)}, bf16[128,2048]{1,0:T(8,128)(2,1)S(1)}, u32[]{:S(2)}, u32[]{:S(2)}) collective-permute-start(bf16[128,2048]{1,0:T(8,128)(2,1)S(1)} %get-tuple-element.13.refs_0_), channel_id=1, source_target_pairs={{0,30},{2,0},{4,2},{6,4},{8,6},{10,8},{12,10},{14,12},{16,14},{18,... | collective-permute-start | bytes 1572872 | tf_op jit(solution)/shard_map/ppermute | solution.py:31
  88.7 1.9 %collective-permute-start.3 = (bf16[128,2048]{1,0:T(8,128)(2,1)S(1)}, bf16[128,2048]{1,0:T(8,128)(2,1)S(1)}, u32[]{:S(2)}, u32[]{:S(2)}) collective-permute-start(bf16[128,2048]{1,0:T(8,128)(2,1)S(1)} %get-tuple-element.13.refs_0_), channel_id=1, source_target_pairs={{0,2},{2,4},{4,6},{6,8},{8,10},{10,12},{12,14},{14,16},{16,18},{18... | collective-permute-start | bytes 1572872 | tf_op jit(solution)/shard_map/ppermute | solution.py:31
  90.6 3.5 %collective-permute-start.5 = (bf16[64,2048]{1,0:T(8,128)(2,1)S(1)}, bf16[64,2048]{1,0:T(8,128)(2,1)S(1)}, u32[]{:S(2)}, u32[]{:S(2)}) collective-permute-start(bf16[64,2048]{1,0:T(8,128)(2,1)S(1)} %get-tuple-element.14), channel_id=1, source_target_pairs={{0,28},{2,30},{4,0},{6,2},{8,4},{10,6},{12,8},{14,10},{16,12},{18,... | collective-permute-start | bytes 786440 | tf_op jit(solution)/shard_map/ppermute | solution.py:31
  94.1 3.2 %collective-permute-start.6 = (bf16[64,2048]{1,0:T(8,128)(2,1)S(1)}, bf16[64,2048]{1,0:T(8,128)(2,1)S(1)}, u32[]{:S(2)}, u32[]{:S(2)}) collective-permute-start(bf16[64,2048]{1,0:T(8,128)(2,1)S(1)} %get-tuple-element.15), channel_id=1, source_target_pairs={{0,4},{2,6},{4,8},{6,10},{8,12},{10,14},{12,16},{14,18},{16,20},{1... | collective-permute-start | bytes 786440 | tf_op jit(solution)/shard_map/ppermute | solution.py:31
  97.3 8.7 %collective-permute-done.1.refs_0_ = bf16[128,2048]{1,0:T(8,128)(2,1)S(1)} collective-permute-done((bf16[128,2048]{1,0:T(8,128)(2,1)S(1)}, bf16[128,2048]{1,0:T(8,128)(2,1)S(1)}, u32[]{:S(2)}, u32[]{:S(2)}) %collective-permute-start.1) | collective-permute-done | bytes 524320 | tf_op jit(solution)/shard_map/ppermute | solution.py:31
  106.1 0.0 collective-permute-done.refs_2_.refs_3_
  106.1 1.5 shard_map.86
  107.5 1.9 %collective-permute-start.2 = (bf16[128,2048]{1,0:T(8,128)(2,1)S(1)}, bf16[128,2048]{1,0:T(8,128)(2,1)S(1)}, u32[]{:S(2)}, u32[]{:S(2)}) collective-permute-start(bf16[128,2048]{1,0:T(8,128)(2,1)S(1)} %shard_map.86), channel_id=1, source_target_pairs={{0,2},{2,4},{4,6},{6,8},{8,10},{10,12},{12,14},{14,16},{16,18},{18... | collective-permute-start | bytes 1572872 | tf_op jit(solution)/shard_map/ppermute | solution.py:31
  109.5 0.4 collective-permute-done.3.refs_0_
  109.9 1.5 shard_map.87
  111.4 5.3 %collective-permute-start.4 = (bf16[128,2048]{1,0:T(8,128)(2,1)S(1)}, bf16[128,2048]{1,0:T(8,128)(2,1)S(1)}, u32[]{:S(2)}, u32[]{:S(2)}) collective-permute-start(bf16[128,2048]{1,0:T(8,128)(2,1)S(1)} %shard_map.87), channel_id=1, source_target_pairs={{0,30},{2,0},{4,2},{6,4},{8,6},{10,8},{12,10},{14,12},{16,14},{18,... | collective-permute-start | bytes 1572872 | tf_op jit(solution)/shard_map/ppermute | solution.py:31
  116.7 0.0 collective-permute-done.5.refs_0_
  116.7 0.0 collective-permute-done.6.refs_1_
  116.7 1.4 shard_map.88
  118.2 1.9 %collective-permute-start.7 = (bf16[64,2048]{1,0:T(8,128)(2,1)S(1)}, bf16[64,2048]{1,0:T(8,128)(2,1)S(1)}, u32[]{:S(2)}, u32[]{:S(2)}) collective-permute-start(bf16[64,2048]{1,0:T(8,128)(2,1)S(1)} %get-tuple-element.16), channel_id=1, source_target_pairs={{0,4},{2,6},{4,8},{6,10},{8,12},{10,14},{12,16},{14,18},{16,20},{1... | collective-permute-start | bytes 786440 | tf_op jit(solution)/shard_map/ppermute | solution.py:31
  120.1 6.0 %collective-permute-start.8 = (bf16[64,2048]{1,0:T(8,128)(2,1)S(1)}, bf16[64,2048]{1,0:T(8,128)(2,1)S(1)}, u32[]{:S(2)}, u32[]{:S(2)}) collective-permute-start(bf16[64,2048]{1,0:T(8,128)(2,1)S(1)} %get-tuple-element.17), channel_id=1, source_target_pairs={{0,28},{2,30},{4,0},{6,2},{8,4},{10,6},{12,8},{14,10},{16,12},{18,... | collective-permute-start | bytes 786440 | tf_op jit(solution)/shard_map/ppermute | solution.py:31
  126.1 1.5 shard_map.85.own_ref
  127.6 6.6 %collective-permute-done.2.next_ref = bf16[128,2048]{1,0:T(8,128)(2,1)S(1)} collective-permute-done((bf16[128,2048]{1,0:T(8,128)(2,1)S(1)}, bf16[128,2048]{1,0:T(8,128)(2,1)S(1)}, u32[]{:S(2)}, u32[]{:S(2)}) %collective-permute-start.2) | collective-permute-done | bytes 524320 | tf_op jit(solution)/shard_map/ppermute | solution.py:31
  134.2 0.0 collective-permute-done.4.prev_ref
  134.2 4.7 %collective-permute-start.9 = (bf16[16,2048]{1,0:T(8,128)(2,1)S(1)}, bf16[16,2048]{1,0:T(8,128)(2,1)S(1)}, u32[]{:S(2)}, u32[]{:S(2)}) collective-permute-start(bf16[16,2048]{1,0:T(8,128)(2,1)S(1)} %get-tuple-element.18), channel_id=1, source_target_pairs={{0,8},{2,10},{4,12},{6,14},{8,16},{10,18},{12,20},{14,22},{16,24},... | collective-permute-start | bytes 196616 | tf_op jit(solution)/shard_map/ppermute | solution.py:31
  138.9 5.1 %collective-permute-start.10 = (bf16[16,2048]{1,0:T(8,128)(2,1)S(1)}, bf16[16,2048]{1,0:T(8,128)(2,1)S(1)}, u32[]{:S(2)}, u32[]{:S(2)}) collective-permute-start(bf16[16,2048]{1,0:T(8,128)(2,1)S(1)} %get-tuple-element.19), channel_id=1, source_target_pairs={{0,24},{2,26},{4,28},{6,30},{8,0},{10,2},{12,4},{14,6},{16,8},{18,... | collective-permute-start | bytes 196616 | tf_op jit(solution)/shard_map/ppermute | solution.py:31
  144.0 0.0 collective-permute-done.7.next2_ref
  144.0 0.0 collective-permute-done.8.prev2_ref
  144.0 3.8 %collective-permute-done.9.up_ref = bf16[16,2048]{1,0:T(8,128)(2,1)S(1)} collective-permute-done((bf16[16,2048]{1,0:T(8,128)(2,1)S(1)}, bf16[16,2048]{1,0:T(8,128)(2,1)S(1)}, u32[]{:S(2)}, u32[]{:S(2)}) %collective-permute-start.9) | collective-permute-done | bytes 65568 | tf_op jit(solution)/shard_map/ppermute | solution.py:31
  147.8 4.1 %collective-permute-done.10.down_ref = bf16[16,2048]{1,0:T(8,128)(2,1)S(1)} collective-permute-done((bf16[16,2048]{1,0:T(8,128)(2,1)S(1)}, bf16[16,2048]{1,0:T(8,128)(2,1)S(1)}, u32[]{:S(2)}, u32[]{:S(2)}) %collective-permute-start.10) | collective-permute-done | bytes 65568 | tf_op jit(solution)/shard_map/ppermute | solution.py:31
  151.9 0.1 shard_map.90
  152.0 6.3 %collective-permute-start.11 = (bf16[32,2048]{1,0:T(8,128)(2,1)S(1)}, bf16[32,2048]{1,0:T(8,128)(2,1)S(1)}, u32[]{:S(2)}, u32[]{:S(2)}) collective-permute-start(bf16[32,2048]{1,0:T(8,128)(2,1)S(1)} %get-tuple-element.20), channel_id=1, source_target_pairs={{0,8},{2,10},{4,12},{6,14},{8,16},{10,18},{12,20},{14,22},{16,24},... | collective-permute-start | bytes 393224 | tf_op jit(solution)/shard_map/ppermute | solution.py:31
  158.3 3.5 %collective-permute-start.12 = (bf16[32,2048]{1,0:T(8,128)(2,1)S(1)}, bf16[32,2048]{1,0:T(8,128)(2,1)S(1)}, u32[]{:S(2)}, u32[]{:S(2)}) collective-permute-start(bf16[32,2048]{1,0:T(8,128)(2,1)S(1)} %get-tuple-element.21), channel_id=1, source_target_pairs={{0,24},{2,26},{4,28},{6,30},{8,0},{10,2},{12,4},{14,6},{16,8},{18,... | collective-permute-start | bytes 393224 | tf_op jit(solution)/shard_map/ppermute | solution.py:31
  161.8 1.8 %fusion = (bf16[16,1,128,256]{3,2,1,0:T(8,128)(2,1)}, bf16[16,1,128,256]{3,2,1,0:T(8,128)(2,1)}, bf16[16,1,128,256]{3,2,1,0:T(8,128)(2,1)}) fusion(bf16[16,3,128,256]{3,2,1,0:T(8,128)(2,1)S(1)} %all_to_all.5.refs_1_.refs_2_), kind=kLoop, calls=%fused_computation | loop fusion | bytes 6291456 | tf_op jit(solution)/shard_map/slice | solution.py:195
  163.5 0.0 collective-permute-done.11.above_ref
  163.5 5.5 %collective-permute-done.12.below_ref = bf16[32,2048]{1,0:T(8,128)(2,1)S(1)} collective-permute-done((bf16[32,2048]{1,0:T(8,128)(2,1)S(1)}, bf16[32,2048]{1,0:T(8,128)(2,1)S(1)}, u32[]{:S(2)}, u32[]{:S(2)}) %collective-permute-start.12) | collective-permute-done | bytes 131104 | tf_op jit(solution)/shard_map/ppermute | solution.py:31
  169.1 0.8 shard_map.91
  (1 shorter events, 0.0 us)
Async XLA Ops:
  3.5 46.5 %copy-start = (bf16[32,2048]{1,0:T(8,128)(2,1)S(1)}, bf16[32,2048]{1,0:T(8,128)(2,1)}, u32[]{:S(2)}) copy-start(bf16[32,2048]{1,0:T(8,128)(2,1)} %tokens_ref.1) | copy-start | bytes 393220
  48.1 58.0 %collective-permute-start = (bf16[16,3,128,256]{3,2,1,0:T(8,128)(2,1)S(1)}, bf16[16,3,128,256]{3,2,1,0:T(8,128)(2,1)S(1)}, u32[]{:S(2)}, u32[]{:S(2)}) collective-permute-start(bf16[16,3,128,256]{3,2,1,0:T(8,128)(2,1)S(1)} %all_to_all.5.refs_1_.refs_2_), channel_id=1, source_target_pairs={{0,1},{1,0},{2,3},{3,2},{4,5},{5,4},{6,7},{7,6},{8,9},{9,8},{10,11... | collective-permute-start | bytes 9437192 | tf_op jit(solution)/shard_map/ppermute | solution.py:173
  83.5 22.6 %collective-permute-start.1 = (bf16[128,2048]{1,0:T(8,128)(2,1)S(1)}, bf16[128,2048]{1,0:T(8,128)(2,1)S(1)}, u32[]{:S(2)}, u32[]{:S(2)}) collective-permute-start(bf16[128,2048]{1,0:T(8,128)(2,1)S(1)} %get-tuple-element.13.refs_0_), channel_id=1, source_target_pairs={{0,30},{2,0},{4,2},{6,4},{8,6},{10,8},{12,10},{14,12},{16,14},{18,... | collective-permute-start | bytes 1572872 | tf_op jit(solution)/shard_map/ppermute | solution.py:31
  88.7 21.2 %collective-permute-start.3 = (bf16[128,2048]{1,0:T(8,128)(2,1)S(1)}, bf16[128,2048]{1,0:T(8,128)(2,1)S(1)}, u32[]{:S(2)}, u32[]{:S(2)}) collective-permute-start(bf16[128,2048]{1,0:T(8,128)(2,1)S(1)} %get-tuple-element.13.refs_0_), channel_id=1, source_target_pairs={{0,2},{2,4},{4,6},{6,8},{8,10},{10,12},{12,14},{14,16},{16,18},{18... | collective-permute-start | bytes 1572872 | tf_op jit(solution)/shard_map/ppermute | solution.py:31
  90.6 26.1 %collective-permute-start.5 = (bf16[64,2048]{1,0:T(8,128)(2,1)S(1)}, bf16[64,2048]{1,0:T(8,128)(2,1)S(1)}, u32[]{:S(2)}, u32[]{:S(2)}) collective-permute-start(bf16[64,2048]{1,0:T(8,128)(2,1)S(1)} %get-tuple-element.14), channel_id=1, source_target_pairs={{0,28},{2,30},{4,0},{6,2},{8,4},{10,6},{12,8},{14,10},{16,12},{18,... | collective-permute-start | bytes 786440 | tf_op jit(solution)/shard_map/ppermute | solution.py:31
  94.1 22.6 %collective-permute-start.6 = (bf16[64,2048]{1,0:T(8,128)(2,1)S(1)}, bf16[64,2048]{1,0:T(8,128)(2,1)S(1)}, u32[]{:S(2)}, u32[]{:S(2)}) collective-permute-start(bf16[64,2048]{1,0:T(8,128)(2,1)S(1)} %get-tuple-element.15), channel_id=1, source_target_pairs={{0,4},{2,6},{4,8},{6,10},{8,12},{10,14},{12,16},{14,18},{16,20},{1... | collective-permute-start | bytes 786440 | tf_op jit(solution)/shard_map/ppermute | solution.py:31
  107.5 26.6 %collective-permute-start.2 = (bf16[128,2048]{1,0:T(8,128)(2,1)S(1)}, bf16[128,2048]{1,0:T(8,128)(2,1)S(1)}, u32[]{:S(2)}, u32[]{:S(2)}) collective-permute-start(bf16[128,2048]{1,0:T(8,128)(2,1)S(1)} %shard_map.86), channel_id=1, source_target_pairs={{0,2},{2,4},{4,6},{6,8},{8,10},{10,12},{12,14},{14,16},{16,18},{18... | collective-permute-start | bytes 1572872 | tf_op jit(solution)/shard_map/ppermute | solution.py:31
  111.4 22.8 %collective-permute-start.4 = (bf16[128,2048]{1,0:T(8,128)(2,1)S(1)}, bf16[128,2048]{1,0:T(8,128)(2,1)S(1)}, u32[]{:S(2)}, u32[]{:S(2)}) collective-permute-start(bf16[128,2048]{1,0:T(8,128)(2,1)S(1)} %shard_map.87), channel_id=1, source_target_pairs={{0,30},{2,0},{4,2},{6,4},{8,6},{10,8},{12,10},{14,12},{16,14},{18,... | collective-permute-start | bytes 1572872 | tf_op jit(solution)/shard_map/ppermute | solution.py:31
  118.2 25.8 %collective-permute-start.7 = (bf16[64,2048]{1,0:T(8,128)(2,1)S(1)}, bf16[64,2048]{1,0:T(8,128)(2,1)S(1)}, u32[]{:S(2)}, u32[]{:S(2)}) collective-permute-start(bf16[64,2048]{1,0:T(8,128)(2,1)S(1)} %get-tuple-element.16), channel_id=1, source_target_pairs={{0,4},{2,6},{4,8},{6,10},{8,12},{10,14},{12,16},{14,18},{16,20},{1... | collective-permute-start | bytes 786440 | tf_op jit(solution)/shard_map/ppermute | solution.py:31
  120.1 23.9 %collective-permute-start.8 = (bf16[64,2048]{1,0:T(8,128)(2,1)S(1)}, bf16[64,2048]{1,0:T(8,128)(2,1)S(1)}, u32[]{:S(2)}, u32[]{:S(2)}) collective-permute-start(bf16[64,2048]{1,0:T(8,128)(2,1)S(1)} %get-tuple-element.17), channel_id=1, source_target_pairs={{0,28},{2,30},{4,0},{6,2},{8,4},{10,6},{12,8},{14,10},{16,12},{18,... | collective-permute-start | bytes 786440 | tf_op jit(solution)/shard_map/ppermute | solution.py:31
  134.2 13.6 %collective-permute-start.9 = (bf16[16,2048]{1,0:T(8,128)(2,1)S(1)}, bf16[16,2048]{1,0:T(8,128)(2,1)S(1)}, u32[]{:S(2)}, u32[]{:S(2)}) collective-permute-start(bf16[16,2048]{1,0:T(8,128)(2,1)S(1)} %get-tuple-element.18), channel_id=1, source_target_pairs={{0,8},{2,10},{4,12},{6,14},{8,16},{10,18},{12,20},{14,22},{16,24},... | collective-permute-start | bytes 196616 | tf_op jit(solution)/shard_map/ppermute | solution.py:31
  138.9 13.0 %collective-permute-start.10 = (bf16[16,2048]{1,0:T(8,128)(2,1)S(1)}, bf16[16,2048]{1,0:T(8,128)(2,1)S(1)}, u32[]{:S(2)}, u32[]{:S(2)}) collective-permute-start(bf16[16,2048]{1,0:T(8,128)(2,1)S(1)} %get-tuple-element.19), channel_id=1, source_target_pairs={{0,24},{2,26},{4,28},{6,30},{8,0},{10,2},{12,4},{14,6},{16,8},{18,... | collective-permute-start | bytes 196616 | tf_op jit(solution)/shard_map/ppermute | solution.py:31
  152.0 11.5 %collective-permute-start.11 = (bf16[32,2048]{1,0:T(8,128)(2,1)S(1)}, bf16[32,2048]{1,0:T(8,128)(2,1)S(1)}, u32[]{:S(2)}, u32[]{:S(2)}) collective-permute-start(bf16[32,2048]{1,0:T(8,128)(2,1)S(1)} %get-tuple-element.20), channel_id=1, source_target_pairs={{0,8},{2,10},{4,12},{6,14},{8,16},{10,18},{12,20},{14,22},{16,24},... | collective-permute-start | bytes 393224 | tf_op jit(solution)/shard_map/ppermute | solution.py:31
  158.3 10.8 %collective-permute-start.12 = (bf16[32,2048]{1,0:T(8,128)(2,1)S(1)}, bf16[32,2048]{1,0:T(8,128)(2,1)S(1)}, u32[]{:S(2)}, u32[]{:S(2)}) collective-permute-start(bf16[32,2048]{1,0:T(8,128)(2,1)S(1)} %get-tuple-element.21), channel_id=1, source_target_pairs={{0,24},{2,26},{4,28},{6,30},{8,0},{10,2},{12,4},{14,6},{16,8},{18,... | collective-permute-start | bytes 393224 | tf_op jit(solution)/shard_map/ppermute | solution.py:31

commit v9 on v7

--- a/solution.py
+++ b/solution.py
@@ -29,6 +29,12 @@
 def move(array, by):
     planes = lax.axis_size(Z)
     return lax.ppermute(array, Z, [(i, (i + by) % planes) for i in range(planes)])
+
+
+def move_by_core(array, by):
+    planes = lax.axis_size(Z)
+    pairs = [(2 * i + c, 2 * ((i + way * by) % planes) + c) for c, way in ((0, 1), (1, -1)) for i in range(planes)]
+    return lax.ppermute(array, TP, pairs)
 
 
 def copies_kernel(gain_hbm, gate_hbm, up_hbm, down_hbm, out_hbm, gain_ref, wide_ref, shard_ref, in_sems, out_sems):
@@ -74,24 +80,25 @@
     )(norm_gain.reshape(1, -1), gate_master, up_master, down_master)
 
 
-def order_kernel(from_ref, held_ref, above_ref, below_ref):
+def order_kernel(from_ref, held_ref):
     rows = from_ref.shape[0] // 4
     here = lax.axis_index("zh")
-
-    def block(by):
-        return from_ref[pl.ds(pl.multiple_of((here + by) % 4 * rows, rows), rows)]
-
-    own, above, below = block(0), block(1), block(3)
-    for k, value in enumerate((own, block(2), above, below)):
-        held_ref[k * rows : (k + 1) * rows] = value
-    for ref, value in ((above_ref, above), (below_ref, below)):
-        ref[:rows] = own
-        ref[rows:] = value
-
-
-def sums_kernel(count, *refs):
+    for k, by in enumerate((0, 2, 1, 3)):
+        held_ref[k * rows : (k + 1) * rows] = from_ref[pl.ds(pl.multiple_of((here + by) % 4 * rows, rows), rows)]
+
+
+def plane_twos(ref):
+    rows = ref.shape[0] // 4
+    core = lax.axis_index("c")
+    return [ref[pl.ds(pl.multiple_of(jnp.where(core == 0, up, down) * rows, rows), rows)] for up, down in ((0, 2), (2, 1), (3, 0), (1, 3))]
+
+
+def sums_kernel(count, twos, *refs):
     rows_refs, (own_ref, partner_ref), out_refs = refs[:count], refs[count : count + 2], refs[count + 2 :]
-    rows = jnp.concatenate([ref[...] for ref in rows_refs], axis=0)
+    blocks = [ref[...] for ref in rows_refs[: count - twos]]
+    for ref in rows_refs[count - twos :]:
+        blocks += plane_twos(ref)
+    rows = jnp.concatenate(blocks, axis=0)
     width = rows.shape[1]
     wide = rows.astype(jnp.float32)
     row_scale = lax.rsqrt(jnp.mean(wide * wide, axis=1, keepdims=True) + 1e-06)
@@ -113,12 +120,12 @@
         at += ref.shape[0]
 
 
-def partial_sums(parts, weights, outs, dtype):
+def partial_sums(parts, twos, weights, counts, dtype):
     units = 2 * weights[0].shape[-1]
-    count, width = sum(p.shape[0] for p in parts), parts[0].shape[1]
+    count, width = sum(counts), parts[0].shape[1]
     return local(
-        lambda *refs: sums_kernel(len(parts), *refs),
-        tuple(jax.ShapeDtypeStruct((count // outs, width), dtype) for _ in range(outs)),
+        lambda *refs: sums_kernel(len(parts), twos, *refs),
+        tuple(jax.ShapeDtypeStruct((k, width), dtype) for k in counts),
         *parts,
         *weights,
         flops=6 * count * width * units,
@@ -126,21 +133,29 @@
     )
 
 
-def fold_kernel(terms, *refs):
-    inputs, outputs = refs[: len(refs) - len(terms)], refs[len(refs) - len(terms) :]
-    for out_ref, pairs in zip(outputs, terms):
-        rows = out_ref.shape[0]
-        total = None
-        for which, k in pairs:
-            value = inputs[which][k * rows : (k + 1) * rows].astype(jnp.float32)
-            total = value if total is None else total + value
-        out_ref[...] = total.astype(out_ref.dtype)
-
-
-def mix_kernel(tokens_ref, own_ref, next_ref, prev_ref, next2_ref, prev2_ref, far_ref, above_ref, below_ref, out_ref):
+def fold_far_kernel(own_ref, next_ref, prev_ref, far_ref):
+    rows = far_ref.shape[0]
+    total = own_ref[rows : 2 * rows]
+    for other in (next_ref, prev_ref):
+        total = total + other[rows : 2 * rows].astype(jnp.float32)
+    far_ref[...] = total.astype(far_ref.dtype)
+
+
+def fold_near_kernel(own_ref, next_ref, prev_ref, next2_ref, prev2_ref, far_ref, above_ref, below_ref):
+    rows = above_ref.shape[0]
+    core = lax.axis_index("c")
+    far = far_ref[...].astype(jnp.float32)
+    for out_ref, block, second_ref, way in ((above_ref, 2, next2_ref, 0), (below_ref, 3, prev2_ref, 1)):
+        total = own_ref[block * rows : (block + 1) * rows] + second_ref[rows:].astype(jnp.float32)
+        for other in (next_ref, prev_ref):
+            total = total + other[block * rows : (block + 1) * rows].astype(jnp.float32)
+        out_ref[...] = (total + jnp.where(core == way, far, 0.0)).astype(out_ref.dtype)
+
+
+def mix_kernel(tokens_ref, own_ref, next_ref, prev_ref, next2_ref, prev2_ref, above_ref, below_ref, out_ref):
     rows = tokens_ref.shape[0]
     total = own_ref[:rows]
-    for ref in (next_ref, prev_ref, next2_ref, prev2_ref, far_ref, above_ref, below_ref):
+    for ref in (next_ref, prev_ref, next2_ref, prev2_ref, above_ref, below_ref):
         total = total + ref[:rows].astype(jnp.float32)
     out_ref[...] = (tokens_ref[...].astype(jnp.float32) + 0.5 * total).astype(out_ref.dtype)
 
@@ -150,33 +165,30 @@
     packed = lax.all_to_all(copies, "fs", split_axis=0, concat_axis=0, tiled=True)
     spread = lax.all_gather(tokens, "zh", axis=0, tiled=True)
     rows, width = tokens.shape
-    shapes = tuple(jax.ShapeDtypeStruct((k * rows, width), tokens.dtype) for k in (4, 2, 2))
-    held, pair_above, pair_below = local(order_kernel, shapes, spread)
+    (held,) = local(order_kernel, (jax.ShapeDtypeStruct((4 * rows, width), tokens.dtype),), spread)
     from_next = move(held, -1)
     from_prev = move(held, 1)
-    from_next2 = move(pair_above, -2)
-    from_prev2 = move(pair_below, 2)
+    from_twos = move_by_core(held, -2)
 
     partner = lax.ppermute(packed, "c", [(0, 1), (1, 0)])
     weights = (packed, partner)
 
-    (ones_next,) = partial_sums((from_next,), weights, 1, jnp.bfloat16)
-    to_next = move(ones_next, 1)
-    (ones_prev,) = partial_sums((from_prev,), weights, 1, jnp.bfloat16)
-    to_prev = move(ones_prev, -1)
-    twos_next, twos_prev = partial_sums((from_next2, from_prev2), weights, 2, jnp.bfloat16)
-    to_next2 = move(twos_next, 2)
-    to_prev2 = move(twos_prev, -2)
-    (own,) = partial_sums((held,), weights, 1, jnp.float32)
-
-    block = jax.ShapeDtypeStruct(tokens.shape, jnp.bfloat16)
-    (sum_far,) = local(lambda *refs: fold_kernel((((0, 1), (1, 1), (2, 1)),), *refs), (block,), own, to_next, to_prev)
-    back_far = move(sum_far, 8)
-    terms = (((0, 2), (1, 2), (2, 2), (3, 1)), ((0, 3), (1, 3), (2, 3), (4, 1)))
-    sum_above, sum_below = local(lambda *refs: fold_kernel(terms, *refs), (block, block), own, to_next, to_prev, to_next2, to_prev2)
+    counts = (4 * rows, 4 * rows, 2 * rows, 2 * rows)
+    for_next, for_prev, for_next2, for_prev2 = partial_sums((from_next, from_prev, from_twos), 1, weights, counts, jnp.bfloat16)
+    to_next = move(for_next, 1)
+    to_prev = move(for_prev, -1)
+    to_next2 = move(for_next2, 2)
+    to_prev2 = move(for_prev2, -2)
+    (own,) = partial_sums((held,), 0, weights, (4 * rows,), jnp.float32)
+
+    block = jax.ShapeDtypeStruct((rows, width), jnp.bfloat16)
+    (sum_far,) = local(fold_far_kernel, (block,), own, to_next, to_prev)
+    back_far = move_by_core(sum_far, 4)
+    received = (own, to_next, to_prev, to_next2, to_prev2)
+    sum_above, sum_below = local(fold_near_kernel, (block, block), *received, back_far)
     back_above = move(sum_above, 4)
     back_below = move(sum_below, -4)
-    (mixed,) = local(mix_kernel, (block,), tokens, own, to_next, to_prev, to_next2, to_prev2, back_far, back_above, back_below)
+    (mixed,) = local(mix_kernel, (block,), tokens, *received, back_above, back_below)
     return (mixed, *(packed[:, k].reshape(-1, packed.shape[-1]) for k in range(3)))
 
 

time: 171 us -> 178 us (1.041)
  the two profiles are of different devices: /device:TPU:96 before, /device:TPU:1 now
where the time goes in v9:
time: 178 us; the launch traced here: 177 us
  blocking collectives  74.9 us (42%)
  waiting for transfers between devices  52 us (29%)
  starting transfers between devices  40 us (22%)
  Pallas kernels  8.07 us (5%)
    all_to_all x1, blocking collectives, step(): lax.all_to_all(copies, 'fs', split_axis=0, concat_axis=0, tiled=True)  44.4 us
    ppermute x8, waiting for transfers between devices, move(): lax.ppermute(array, Z, [(i, (i + by) % planes) for i in range(planes)])  33.8 us
    all_gather x1, blocking collectives, step(): spread = lax.all_gather(tokens, 'zh', axis=0, tiled=True)  30.5 us
    ppermute x8, starting transfers between devices, move(): lax.ppermute(array, Z, [(i, (i + by) % planes) for i in range(planes)])  30.1 us
    ppermute x2, waiting for transfers between devices, move_by_core(): return lax.ppermute(array, TP, pairs)  18.1 us
    ppermute x1, starting transfers between devices, step(): partner = lax.ppermute(packed, 'c', [(0, 1), (1, 0)])  6.01 us
    pallas_call x6, Pallas kernels, local(): pl.pallas_call(kernel, out_shape=outs, in_specs=[VMEM] * len(args), out_s...  5.21 us
    ppermute x2, starting transfers between devices, move_by_core(): return lax.ppermute(array, TP, pairs)  3.84 us
  transfers between devices with their start and end apart: 11, of which 9 were waited for; matrix products, arithmetic and copies ran while one was open for 1% of the time, Pallas kernels for 1%

profile of v9, /device:TPU:1, one launch (start us, length us, event | category | flops | bytes accessed | tf_op | source)
XLA Modules:
  0.0 177.4 jit_solution(6693312054168728113)
XLA Ops:
  0.6 2.9 %prepare.1 = bf16[16,3,128,256]{3,2,1,0:T(8,128)(2,1)} custom-call(f32[1,128]{1,0:T(1,128)} %bitcast.7, f32[128,256]{1,0:T(8,128)} %gate_hbm.1, f32[128,256]{1,0:T(8,128)} %up_hbm.1, f32[128,256]{1,0:T(8,128)} %down_hbm.1), custom_call_target="tpu_custom_call" | custom-call | flops 1000000 | bytes 4000000 | tf_op jit(solution)/shard_map/prepare/pallas_call | solution.py:65
  3.5 0.0 copy-start
  3.5 44.4 %all_to_all.5.refs_1_.refs_3_ = bf16[16,3,128,256]{3,2,1,0:T(8,128)(2,1)S(1)} all-to-all(bf16[16,3,128,256]{3,2,1,0:T(8,128)(2,1)} %prepare.1), channel_id=1, replica_groups=mesh['fs'=16,'zh'=4,'zl'=4,'c'=2] {'fs'}, dimensions={0} | all-to-all | bytes 6291456 | tf_op jit(solution)/shard_map/all_to_all | solution.py:165
  48.0 6.0 %collective-permute-start = (bf16[16,3,128,256]{3,2,1,0:T(8,128)(2,1)S(1)}, bf16[16,3,128,256]{3,2,1,0:T(8,128)(2,1)S(1)}, u32[]{:S(2)}, u32[]{:S(2)}) collective-permute-start(bf16[16,3,128,256]{3,2,1,0:T(8,128)(2,1)S(1)} %all_to_all.5.refs_1_.refs_3_), channel_id=1, source_target_pairs={{0,1},{1,0},{2,3},{3,2},{4,5},{5,4},{6,7},{7,6},{8,9},{9,8},{10,11... | collective-permute-start | bytes 9437192 | tf_op jit(solution)/shard_map/ppermute | solution.py:173
  54.0 0.0 copy-done
  54.0 30.5 %all_gather.3.from_ref = bf16[128,2048]{1,0:T(8,128)(2,1)S(1)} all-gather(bf16[32,2048]{1,0:T(8,128)(2,1)S(1)} %copy-done), channel_id=1, replica_groups=mesh['fs'=16,'zh'=4,'zl'=4,'c'=2] {'zh'}, dimensions={0}, use_global_device_ids=true | all-gather | bytes 655360 | tf_op jit(solution)/shard_map/all_gather | solution.py:166
  84.5 5.1 %collective-permute-start.1 = (bf16[128,2048]{1,0:T(8,128)(2,1)S(1)}, bf16[128,2048]{1,0:T(8,128)(2,1)S(1)}, u32[]{:S(2)}, u32[]{:S(2)}) collective-permute-start(bf16[128,2048]{1,0:T(8,128)(2,1)S(1)} %shard_map.84.refs_0_), channel_id=1, source_target_pairs={{0,30},{2,0},{4,2},{6,4},{8,6},{10,8},{12,10},{14,12},{16,14},{18,... | collective-permute-start | bytes 1572872 | tf_op jit(solution)/shard_map/ppermute | solution.py:31
  89.6 1.9 %collective-permute-start.2 = (bf16[128,2048]{1,0:T(8,128)(2,1)S(1)}, bf16[128,2048]{1,0:T(8,128)(2,1)S(1)}, u32[]{:S(2)}, u32[]{:S(2)}) collective-permute-start(bf16[128,2048]{1,0:T(8,128)(2,1)S(1)} %shard_map.84.refs_0_), channel_id=1, source_target_pairs={{0,2},{2,4},{4,6},{6,8},{8,10},{10,12},{12,14},{14,16},{16,18},{18... | collective-permute-start | bytes 1572872 | tf_op jit(solution)/shard_map/ppermute | solution.py:31
  91.5 1.9 %collective-permute-start.3 = (bf16[128,2048]{1,0:T(8,128)(2,1)S(1)}, bf16[128,2048]{1,0:T(8,128)(2,1)S(1)}, u32[]{:S(2)}, u32[]{:S(2)}) collective-permute-start(bf16[128,2048]{1,0:T(8,128)(2,1)S(1)} %shard_map.84.refs_0_), channel_id=1, source_target_pairs={{0,28},{2,30},{4,0},{6,2},{8,4},{10,6},{12,8},{14,10},{16,12},{18,... | collective-permute-start | bytes 1572872 | tf_op jit(solution)/shard_map/ppermute | solution.py:37
  93.5 5.0 %collective-permute-done.1.refs_0_ = bf16[128,2048]{1,0:T(8,128)(2,1)S(1)} collective-permute-done((bf16[128,2048]{1,0:T(8,128)(2,1)S(1)}, bf16[128,2048]{1,0:T(8,128)(2,1)S(1)}, u32[]{:S(2)}, u32[]{:S(2)}) %collective-permute-start.1) | collective-permute-done | bytes 524320 | tf_op jit(solution)/shard_map/ppermute | solution.py:31
  98.4 5.3 %collective-permute-done.2.refs_1_ = bf16[128,2048]{1,0:T(8,128)(2,1)S(1)} collective-permute-done((bf16[128,2048]{1,0:T(8,128)(2,1)S(1)}, bf16[128,2048]{1,0:T(8,128)(2,1)S(1)}, u32[]{:S(2)}, u32[]{:S(2)}) %collective-permute-start.2) | collective-permute-done | bytes 524320 | tf_op jit(solution)/shard_map/ppermute | solution.py:31
  103.7 12.4 %collective-permute-done.3.refs_2_ = bf16[128,2048]{1,0:T(8,128)(2,1)S(1)} collective-permute-done((bf16[128,2048]{1,0:T(8,128)(2,1)S(1)}, bf16[128,2048]{1,0:T(8,128)(2,1)S(1)}, u32[]{:S(2)}, u32[]{:S(2)}) %collective-permute-start.3) | collective-permute-done | bytes 524320 | tf_op jit(solution)/shard_map/ppermute | solution.py:37
  116.1 0.0 collective-permute-done.refs_2_.refs_4_
  116.1 2.7 %shard_map.86 = (bf16[128,2048]{1,0:T(8,128)(2,1)S(1)}, bf16[128,2048]{1,0:T(8,128)(2,1)S(1)}, bf16[64,2048]{1,0:T(8,128)(2,1)S(1)}, bf16[64,2048]{1,0:T(8,128)(2,1)S(1)}) custom-call(bf16[128,2048]{1,0:T(8,128)(2,1)S(1)} %collective-permute-done.1.refs_0_, bf16[128,2048]{1,0:T(8,128)(2,1)S(1)} %collective-permute-done.2.refs_1_, ...), custom_call_target="tpu_custom_call" | custom-call | flops 2415919104 | bytes 9437184 | tf_op jit(solution)/shard_map/pallas_call | solution.py:19
  118.9 4.6 %collective-permute-start.4 = (bf16[128,2048]{1,0:T(8,128)(2,1)S(1)}, bf16[128,2048]{1,0:T(8,128)(2,1)S(1)}, u32[]{:S(2)}, u32[]{:S(2)}) collective-permute-start(bf16[128,2048]{1,0:T(8,128)(2,1)S(1)} %get-tuple-element.10), channel_id=1, source_target_pairs={{0,2},{2,4},{4,6},{6,8},{8,10},{10,12},{12,14},{14,16},{16,18},{18... | collective-permute-start | bytes 1572872 | tf_op jit(solution)/shard_map/ppermute | solution.py:31
  123.4 1.9 %collective-permute-start.5 = (bf16[128,2048]{1,0:T(8,128)(2,1)S(1)}, bf16[128,2048]{1,0:T(8,128)(2,1)S(1)}, u32[]{:S(2)}, u32[]{:S(2)}) collective-permute-start(bf16[128,2048]{1,0:T(8,128)(2,1)S(1)} %get-tuple-element.11), channel_id=1, source_target_pairs={{0,30},{2,0},{4,2},{6,4},{8,6},{10,8},{12,10},{14,12},{16,14},{18,... | collective-permute-start | bytes 1572872 | tf_op jit(solution)/shard_map/ppermute | solution.py:31
  125.4 3.1 %collective-permute-start.6 = (bf16[64,2048]{1,0:T(8,128)(2,1)S(1)}, bf16[64,2048]{1,0:T(8,128)(2,1)S(1)}, u32[]{:S(2)}, u32[]{:S(2)}) collective-permute-start(bf16[64,2048]{1,0:T(8,128)(2,1)S(1)} %get-tuple-element.12), channel_id=1, source_target_pairs={{0,4},{2,6},{4,8},{6,10},{8,12},{10,14},{12,16},{14,18},{16,20},{1... | collective-permute-start | bytes 786440 | tf_op jit(solution)/shard_map/ppermute | solution.py:31
  128.5 4.3 %collective-permute-start.7 = (bf16[64,2048]{1,0:T(8,128)(2,1)S(1)}, bf16[64,2048]{1,0:T(8,128)(2,1)S(1)}, u32[]{:S(2)}, u32[]{:S(2)}) collective-permute-start(bf16[64,2048]{1,0:T(8,128)(2,1)S(1)} %get-tuple-element.13), channel_id=1, source_target_pairs={{0,28},{2,30},{4,0},{6,2},{8,4},{10,6},{12,8},{14,10},{16,12},{18,... | collective-permute-start | bytes 786440 | tf_op jit(solution)/shard_map/ppermute | solution.py:31
  132.8 1.5 shard_map.85.own_ref
  134.2 5.0 %collective-permute-done.4.next_ref = bf16[128,2048]{1,0:T(8,128)(2,1)S(1)} collective-permute-done((bf16[128,2048]{1,0:T(8,128)(2,1)S(1)}, bf16[128,2048]{1,0:T(8,128)(2,1)S(1)}, u32[]{:S(2)}, u32[]{:S(2)}) %collective-permute-start.4) | collective-permute-done | bytes 524320 | tf_op jit(solution)/shard_map/ppermute | solution.py:31
  139.2 3.4 %collective-permute-done.5.prev_ref = bf16[128,2048]{1,0:T(8,128)(2,1)S(1)} collective-permute-done((bf16[128,2048]{1,0:T(8,128)(2,1)S(1)}, bf16[128,2048]{1,0:T(8,128)(2,1)S(1)}, u32[]{:S(2)}, u32[]{:S(2)}) %collective-permute-start.5) | collective-permute-done | bytes 524320 | tf_op jit(solution)/shard_map/ppermute | solution.py:31
  142.6 1.9 %collective-permute-start.8 = (bf16[32,2048]{1,0:T(8,128)(2,1)S(1)}, bf16[32,2048]{1,0:T(8,128)(2,1)S(1)}, u32[]{:S(2)}, u32[]{:S(2)}) collective-permute-start(bf16[32,2048]{1,0:T(8,128)(2,1)S(1)} %shard_map.87), channel_id=1, source_target_pairs={{0,8},{2,10},{4,12},{6,14},{8,16},{10,18},{12,20},{14,22},{16,24},... | collective-permute-start | bytes 393224 | tf_op jit(solution)/shard_map/ppermute | solution.py:37
  144.5 0.0 collective-permute-done.6.next2_ref
  144.5 5.4 %collective-permute-done.7.prev2_ref = bf16[64,2048]{1,0:T(8,128)(2,1)S(1)} collective-permute-done((bf16[64,2048]{1,0:T(8,128)(2,1)S(1)}, bf16[64,2048]{1,0:T(8,128)(2,1)S(1)}, u32[]{:S(2)}, u32[]{:S(2)}) %collective-permute-start.7) | collective-permute-done | bytes 262176 | tf_op jit(solution)/shard_map/ppermute | solution.py:31
  149.9 5.7 %collective-permute-done.8.far_ref = bf16[32,2048]{1,0:T(8,128)(2,1)S(1)} collective-permute-done((bf16[32,2048]{1,0:T(8,128)(2,1)S(1)}, bf16[32,2048]{1,0:T(8,128)(2,1)S(1)}, u32[]{:S(2)}, u32[]{:S(2)}) %collective-permute-start.8) | collective-permute-done | bytes 131104 | tf_op jit(solution)/shard_map/ppermute | solution.py:37
  155.7 0.2 shard_map.88
  155.8 3.4 %collective-permute-start.10 = (bf16[32,2048]{1,0:T(8,128)(2,1)S(1)}, bf16[32,2048]{1,0:T(8,128)(2,1)S(1)}, u32[]{:S(2)}, u32[]{:S(2)}) collective-permute-start(bf16[32,2048]{1,0:T(8,128)(2,1)S(1)} %get-tuple-element.15), channel_id=1, source_target_pairs={{0,24},{2,26},{4,28},{6,30},{8,0},{10,2},{12,4},{14,6},{16,8},{18,... | collective-permute-start | bytes 393224 | tf_op jit(solution)/shard_map/ppermute | solution.py:31
  159.3 5.7 %collective-permute-start.9 = (bf16[32,2048]{1,0:T(8,128)(2,1)S(1)}, bf16[32,2048]{1,0:T(8,128)(2,1)S(1)}, u32[]{:S(2)}, u32[]{:S(2)}) collective-permute-start(bf16[32,2048]{1,0:T(8,128)(2,1)S(1)} %get-tuple-element.14), channel_id=1, source_target_pairs={{0,8},{2,10},{4,12},{6,14},{8,16},{10,18},{12,20},{14,22},{16,24},... | collective-permute-start | bytes 393224 | tf_op jit(solution)/shard_map/ppermute | solution.py:31
  165.0 1.8 fusion
  166.8 2.3 %collective-permute-done.10.below_ref = bf16[32,2048]{1,0:T(8,128)(2,1)S(1)} collective-permute-done((bf16[32,2048]{1,0:T(8,128)(2,1)S(1)}, bf16[32,2048]{1,0:T(8,128)(2,1)S(1)}, u32[]{:S(2)}, u32[]{:S(2)}) %collective-permute-start.10) | collective-permute-done | bytes 131104 | tf_op jit(solution)/shard_map/ppermute | solution.py:31
  169.1 7.6 %collective-permute-done.9.above_ref = bf16[32,2048]{1,0:T(8,128)(2,1)S(1)} collective-permute-done((bf16[32,2048]{1,0:T(8,128)(2,1)S(1)}, bf16[32,2048]{1,0:T(8,128)(2,1)S(1)}, u32[]{:S(2)}, u32[]{:S(2)}) %collective-permute-start.9) | collective-permute-done | bytes 131104 | tf_op jit(solution)/shard_map/ppermute | solution.py:31
  176.6 0.8 shard_map.89
  (2 shorter events, 0.1 us)
Async XLA Ops:
  3.5 50.5 %copy-start = (bf16[32,2048]{1,0:T(8,128)(2,1)S(1)}, bf16[32,2048]{1,0:T(8,128)(2,1)}, u32[]{:S(2)}) copy-start(bf16[32,2048]{1,0:T(8,128)(2,1)} %tokens_ref.1) | copy-start | bytes 393220
  48.0 68.2 %collective-permute-start = (bf16[16,3,128,256]{3,2,1,0:T(8,128)(2,1)S(1)}, bf16[16,3,128,256]{3,2,1,0:T(8,128)(2,1)S(1)}, u32[]{:S(2)}, u32[]{:S(2)}) collective-permute-start(bf16[16,3,128,256]{3,2,1,0:T(8,128)(2,1)S(1)} %all_to_all.5.refs_1_.refs_3_), channel_id=1, source_target_pairs={{0,1},{1,0},{2,3},{3,2},{4,5},{5,4},{6,7},{7,6},{8,9},{9,8},{10,11... | collective-permute-start | bytes 9437192 | tf_op jit(solution)/shard_map/ppermute | solution.py:173
  84.5 13.9 %collective-permute-start.1 = (bf16[128,2048]{1,0:T(8,128)(2,1)S(1)}, bf16[128,2048]{1,0:T(8,128)(2,1)S(1)}, u32[]{:S(2)}, u32[]{:S(2)}) collective-permute-start(bf16[128,2048]{1,0:T(8,128)(2,1)S(1)} %shard_map.84.refs_0_), channel_id=1, source_target_pairs={{0,30},{2,0},{4,2},{6,4},{8,6},{10,8},{12,10},{14,12},{16,14},{18,... | collective-permute-start | bytes 1572872 | tf_op jit(solution)/shard_map/ppermute | solution.py:31
  89.6 14.1 %collective-permute-start.2 = (bf16[128,2048]{1,0:T(8,128)(2,1)S(1)}, bf16[128,2048]{1,0:T(8,128)(2,1)S(1)}, u32[]{:S(2)}, u32[]{:S(2)}) collective-permute-start(bf16[128,2048]{1,0:T(8,128)(2,1)S(1)} %shard_map.84.refs_0_), channel_id=1, source_target_pairs={{0,2},{2,4},{4,6},{6,8},{8,10},{10,12},{12,14},{14,16},{16,18},{18... | collective-permute-start | bytes 1572872 | tf_op jit(solution)/shard_map/ppermute | solution.py:31
  91.5 24.6 %collective-permute-start.3 = (bf16[128,2048]{1,0:T(8,128)(2,1)S(1)}, bf16[128,2048]{1,0:T(8,128)(2,1)S(1)}, u32[]{:S(2)}, u32[]{:S(2)}) collective-permute-start(bf16[128,2048]{1,0:T(8,128)(2,1)S(1)} %shard_map.84.refs_0_), channel_id=1, source_target_pairs={{0,28},{2,30},{4,0},{6,2},{8,4},{10,6},{12,8},{14,10},{16,12},{18,... | collective-permute-start | bytes 1572872 | tf_op jit(solution)/shard_map/ppermute | solution.py:37
  118.9 20.3 %collective-permute-start.4 = (bf16[128,2048]{1,0:T(8,128)(2,1)S(1)}, bf16[128,2048]{1,0:T(8,128)(2,1)S(1)}, u32[]{:S(2)}, u32[]{:S(2)}) collective-permute-start(bf16[128,2048]{1,0:T(8,128)(2,1)S(1)} %get-tuple-element.10), channel_id=1, source_target_pairs={{0,2},{2,4},{4,6},{6,8},{8,10},{10,12},{12,14},{14,16},{16,18},{18... | collective-permute-start | bytes 1572872 | tf_op jit(solution)/shard_map/ppermute | solution.py:31
  123.4 19.1 %collective-permute-start.5 = (bf16[128,2048]{1,0:T(8,128)(2,1)S(1)}, bf16[128,2048]{1,0:T(8,128)(2,1)S(1)}, u32[]{:S(2)}, u32[]{:S(2)}) collective-permute-start(bf16[128,2048]{1,0:T(8,128)(2,1)S(1)} %get-tuple-element.11), channel_id=1, source_target_pairs={{0,30},{2,0},{4,2},{6,4},{8,6},{10,8},{12,10},{14,12},{16,14},{18,... | collective-permute-start | bytes 1572872 | tf_op jit(solution)/shard_map/ppermute | solution.py:31
  125.4 19.2 %collective-permute-start.6 = (bf16[64,2048]{1,0:T(8,128)(2,1)S(1)}, bf16[64,2048]{1,0:T(8,128)(2,1)S(1)}, u32[]{:S(2)}, u32[]{:S(2)}) collective-permute-start(bf16[64,2048]{1,0:T(8,128)(2,1)S(1)} %get-tuple-element.12), channel_id=1, source_target_pairs={{0,4},{2,6},{4,8},{6,10},{8,12},{10,14},{12,16},{14,18},{16,20},{1... | collective-permute-start | bytes 786440 | tf_op jit(solution)/shard_map/ppermute | solution.py:31
  128.5 21.5 %collective-permute-start.7 = (bf16[64,2048]{1,0:T(8,128)(2,1)S(1)}, bf16[64,2048]{1,0:T(8,128)(2,1)S(1)}, u32[]{:S(2)}, u32[]{:S(2)}) collective-permute-start(bf16[64,2048]{1,0:T(8,128)(2,1)S(1)} %get-tuple-element.13), channel_id=1, source_target_pairs={{0,28},{2,30},{4,0},{6,2},{8,4},{10,6},{12,8},{14,10},{16,12},{18,... | collective-permute-start | bytes 786440 | tf_op jit(solution)/shard_map/ppermute | solution.py:31
  142.6 13.1 %collective-permute-start.8 = (bf16[32,2048]{1,0:T(8,128)(2,1)S(1)}, bf16[32,2048]{1,0:T(8,128)(2,1)S(1)}, u32[]{:S(2)}, u32[]{:S(2)}) collective-permute-start(bf16[32,2048]{1,0:T(8,128)(2,1)S(1)} %shard_map.87), channel_id=1, source_target_pairs={{0,8},{2,10},{4,12},{6,14},{8,16},{10,18},{12,20},{14,22},{16,24},... | collective-permute-start | bytes 393224 | tf_op jit(solution)/shard_map/ppermute | solution.py:37
  155.8 13.2 %collective-permute-start.10 = (bf16[32,2048]{1,0:T(8,128)(2,1)S(1)}, bf16[32,2048]{1,0:T(8,128)(2,1)S(1)}, u32[]{:S(2)}, u32[]{:S(2)}) collective-permute-start(bf16[32,2048]{1,0:T(8,128)(2,1)S(1)} %get-tuple-element.15), channel_id=1, source_target_pairs={{0,24},{2,26},{4,28},{6,30},{8,0},{10,2},{12,4},{14,6},{16,8},{18,... | collective-permute-start | bytes 393224 | tf_op jit(solution)/shard_map/ppermute | solution.py:31
  159.3 17.4 %collective-permute-start.9 = (bf16[32,2048]{1,0:T(8,128)(2,1)S(1)}, bf16[32,2048]{1,0:T(8,128)(2,1)S(1)}, u32[]{:S(2)}, u32[]{:S(2)}) collective-permute-start(bf16[32,2048]{1,0:T(8,128)(2,1)S(1)} %get-tuple-element.14), channel_id=1, source_target_pairs={{0,8},{2,10},{4,12},{6,14},{8,16},{10,18},{12,20},{14,22},{16,24},... | collective-permute-start | bytes 393224 | tf_op jit(solution)/shard_map/ppermute | solution.py:31

commit v10 on v9

--- a/solution.py
+++ b/solution.py
@@ -141,15 +141,17 @@
     far_ref[...] = total.astype(far_ref.dtype)
 
 
-def fold_near_kernel(own_ref, next_ref, prev_ref, next2_ref, prev2_ref, far_ref, above_ref, below_ref):
-    rows = above_ref.shape[0]
-    core = lax.axis_index("c")
-    far = far_ref[...].astype(jnp.float32)
-    for out_ref, block, second_ref, way in ((above_ref, 2, next2_ref, 0), (below_ref, 3, prev2_ref, 1)):
-        total = own_ref[block * rows : (block + 1) * rows] + second_ref[rows:].astype(jnp.float32)
-        for other in (next_ref, prev_ref):
-            total = total + other[block * rows : (block + 1) * rows].astype(jnp.float32)
-        out_ref[...] = (total + jnp.where(core == way, far, 0.0)).astype(out_ref.dtype)
+def fold_near_kernel(way, own_ref, next_ref, prev_ref, next2_ref, prev2_ref, *refs):
+    *far_refs, out_ref = refs
+    rows = out_ref.shape[0]
+    up = lax.axis_index("c") == way
+    lower = pl.multiple_of(jnp.where(up, 2, 3) * rows, rows)
+    total = own_ref[pl.ds(lower, rows)] + jnp.where(up, next2_ref[rows:].astype(jnp.float32), prev2_ref[rows:].astype(jnp.float32))
+    for other in (next_ref, prev_ref):
+        total = total + other[pl.ds(lower, rows)].astype(jnp.float32)
+    for ref in far_refs:
+        total = total + ref[...].astype(jnp.float32)
+    out_ref[...] = total.astype(out_ref.dtype)
 
 
 def mix_kernel(tokens_ref, own_ref, next_ref, prev_ref, next2_ref, prev2_ref, above_ref, below_ref, out_ref):
@@ -173,10 +175,10 @@
     partner = lax.ppermute(packed, "c", [(0, 1), (1, 0)])
     weights = (packed, partner)
 
-    counts = (4 * rows, 4 * rows, 2 * rows, 2 * rows)
-    for_next, for_prev, for_next2, for_prev2 = partial_sums((from_next, from_prev, from_twos), 1, weights, counts, jnp.bfloat16)
+    for_next, for_prev = partial_sums((from_next, from_prev), 0, weights, (4 * rows, 4 * rows), jnp.bfloat16)
     to_next = move(for_next, 1)
     to_prev = move(for_prev, -1)
+    for_next2, for_prev2 = partial_sums((from_twos,), 1, weights, (2 * rows, 2 * rows), jnp.bfloat16)
     to_next2 = move(for_next2, 2)
     to_prev2 = move(for_prev2, -2)
     (own,) = partial_sums((held,), 0, weights, (4 * rows,), jnp.float32)
@@ -185,10 +187,11 @@
     (sum_far,) = local(fold_far_kernel, (block,), own, to_next, to_prev)
     back_far = move_by_core(sum_far, 4)
     received = (own, to_next, to_prev, to_next2, to_prev2)
-    sum_above, sum_below = local(fold_near_kernel, (block, block), *received, back_far)
-    back_above = move(sum_above, 4)
-    back_below = move(sum_below, -4)
-    (mixed,) = local(mix_kernel, (block,), tokens, *received, back_above, back_below)
+    (sum_plain,) = local(lambda *refs: fold_near_kernel(1, *refs), (block,), *received)
+    back_plain = move_by_core(sum_plain, -4)
+    (sum_joint,) = local(lambda *refs: fold_near_kernel(0, *refs), (block,), *received, back_far)
+    back_joint = move_by_core(sum_joint, 4)
+    (mixed,) = local(mix_kernel, (block,), tokens, *received, back_plain, back_joint)
     return (mixed, *(packed[:, k].reshape(-1, packed.shape[-1]) for k in range(3)))
 
 

time: 178 us -> 169 us (0.949)
  the two profiles are of different devices: /device:TPU:1 before, /device:TPU:64 now
where the time goes in v10:
time: 169 us
  blocking collectives  78.8 us (47%)
  starting transfers between devices  44.6 us (26%)
  waiting for transfers between devices  34.3 us (20%)
  Pallas kernels  8.73 us (5%)
  local copies, waits for them, and re-layouts  1.76 us (1%)
    all_to_all x1, blocking collectives, step(): lax.all_to_all(copies, 'fs', split_axis=0, concat_axis=0, tiled=True)  46.8 us
    all_gather x1, blocking collectives, step(): spread = lax.all_gather(tokens, 'zh', axis=0, tiled=True)  32 us
    ppermute x6, starting transfers between devices, move(): lax.ppermute(array, Z, [(i, (i + by) % planes) for i in range(planes)])  23.2 us
    ppermute x6, waiting for transfers between devices, move(): lax.ppermute(array, Z, [(i, (i + by) % planes) for i in range(planes)])  22.7 us
    ppermute x4, starting transfers between devices, move_by_core(): return lax.ppermute(array, TP, pairs)  19.5 us
    ppermute x4, waiting for transfers between devices, move_by_core(): return lax.ppermute(array, TP, pairs)  11.6 us
    pallas_call x8, Pallas kernels, local(): pl.pallas_call(kernel, out_shape=outs, in_specs=[VMEM] * len(args), out_s...  5.87 us
  transfers between devices with their start and end apart: 11, of which 6 were waited for; matrix products, arithmetic and copies ran while one was open for 1% of the time, Pallas kernels for 3%

profile of v10, /device:TPU:64, one launch (start us, length us, event | category | flops | bytes accessed | tf_op | source)
XLA Modules:
  0.0 169.0 jit_solution(7747956324651828761)
XLA Ops:
  0.6 2.9 %prepare.1 = bf16[16,3,128,256]{3,2,1,0:T(8,128)(2,1)} custom-call(f32[1,128]{1,0:T(1,128)} %bitcast.7, f32[128,256]{1,0:T(8,128)} %gate_hbm.1, f32[128,256]{1,0:T(8,128)} %up_hbm.1, f32[128,256]{1,0:T(8,128)} %down_hbm.1), custom_call_target="tpu_custom_call" | custom-call | flops 1000000 | bytes 4000000 | tf_op jit(solution)/shard_map/prepare/pallas_call | solution.py:65
  3.5 0.0 copy-start
  3.5 46.8 %all_to_all.5.refs_1_.refs_2_ = bf16[16,3,128,256]{3,2,1,0:T(8,128)(2,1)S(1)} all-to-all(bf16[16,3,128,256]{3,2,1,0:T(8,128)(2,1)} %prepare.1), channel_id=1, replica_groups=mesh['fs'=16,'zh'=4,'zl'=4,'c'=2] {'fs'}, dimensions={0} | all-to-all | bytes 6291456 | tf_op jit(solution)/shard_map/all_to_all | solution.py:167
  50.3 1.9 %collective-permute-start = (bf16[16,3,128,256]{3,2,1,0:T(8,128)(2,1)S(1)}, bf16[16,3,128,256]{3,2,1,0:T(8,128)(2,1)S(1)}, u32[]{:S(2)}, u32[]{:S(2)}) collective-permute-start(bf16[16,3,128,256]{3,2,1,0:T(8,128)(2,1)S(1)} %all_to_all.5.refs_1_.refs_2_), channel_id=1, source_target_pairs={{0,1},{1,0},{2,3},{3,2},{4,5},{5,4},{6,7},{7,6},{8,9},{9,8},{10,11... | collective-permute-start | bytes 9437192 | tf_op jit(solution)/shard_map/ppermute | solution.py:175
  52.2 0.0 copy-done
  52.2 32.0 %all_gather.3.from_ref = bf16[128,2048]{1,0:T(8,128)(2,1)S(1)} all-gather(bf16[32,2048]{1,0:T(8,128)(2,1)S(1)} %copy-done), channel_id=1, replica_groups=mesh['fs'=16,'zh'=4,'zl'=4,'c'=2] {'zh'}, dimensions={0}, use_global_device_ids=true | all-gather | bytes 655360 | tf_op jit(solution)/shard_map/all_gather | solution.py:168
  84.3 3.4 %collective-permute-start.1 = (bf16[128,2048]{1,0:T(8,128)(2,1)S(1)}, bf16[128,2048]{1,0:T(8,128)(2,1)S(1)}, u32[]{:S(2)}, u32[]{:S(2)}) collective-permute-start(bf16[128,2048]{1,0:T(8,128)(2,1)S(1)} %shard_map.84.refs_0_), channel_id=1, source_target_pairs={{0,30},{2,0},{4,2},{6,4},{8,6},{10,8},{12,10},{14,12},{16,14},{18,... | collective-permute-start | bytes 1572872 | tf_op jit(solution)/shard_map/ppermute | solution.py:31
  87.7 2.5 %collective-permute-start.2 = (bf16[128,2048]{1,0:T(8,128)(2,1)S(1)}, bf16[128,2048]{1,0:T(8,128)(2,1)S(1)}, u32[]{:S(2)}, u32[]{:S(2)}) collective-permute-start(bf16[128,2048]{1,0:T(8,128)(2,1)S(1)} %shard_map.84.refs_0_), channel_id=1, source_target_pairs={{0,2},{2,4},{4,6},{6,8},{8,10},{10,12},{12,14},{14,16},{16,18},{18... | collective-permute-start | bytes 1572872 | tf_op jit(solution)/shard_map/ppermute | solution.py:31
  90.3 4.1 %collective-permute-start.5 = (bf16[128,2048]{1,0:T(8,128)(2,1)S(1)}, bf16[128,2048]{1,0:T(8,128)(2,1)S(1)}, u32[]{:S(2)}, u32[]{:S(2)}) collective-permute-start(bf16[128,2048]{1,0:T(8,128)(2,1)S(1)} %shard_map.84.refs_0_), channel_id=1, source_target_pairs={{0,28},{2,30},{4,0},{6,2},{8,4},{10,6},{12,8},{14,10},{16,12},{18,... | collective-permute-start | bytes 1572872 | tf_op jit(solution)/shard_map/ppermute | solution.py:37
  94.3 2.2 %collective-permute-done.1.refs_0_ = bf16[128,2048]{1,0:T(8,128)(2,1)S(1)} collective-permute-done((bf16[128,2048]{1,0:T(8,128)(2,1)S(1)}, bf16[128,2048]{1,0:T(8,128)(2,1)S(1)}, u32[]{:S(2)}, u32[]{:S(2)}) %collective-permute-start.1) | collective-permute-done | bytes 524320 | tf_op jit(solution)/shard_map/ppermute | solution.py:31
  96.6 11.6 %collective-permute-done.2.refs_1_ = bf16[128,2048]{1,0:T(8,128)(2,1)S(1)} collective-permute-done((bf16[128,2048]{1,0:T(8,128)(2,1)S(1)}, bf16[128,2048]{1,0:T(8,128)(2,1)S(1)}, u32[]{:S(2)}, u32[]{:S(2)}) %collective-permute-start.2) | collective-permute-done | bytes 524320 | tf_op jit(solution)/shard_map/ppermute | solution.py:31
  108.1 0.0 collective-permute-done.refs_2_.refs_3_
  108.1 1.9 %shard_map.86 = (bf16[128,2048]{1,0:T(8,128)(2,1)S(1)}, bf16[128,2048]{1,0:T(8,128)(2,1)S(1)}) custom-call(bf16[128,2048]{1,0:T(8,128)(2,1)S(1)} %collective-permute-done.1.refs_0_, bf16[128,2048]{1,0:T(8,128)(2,1)S(1)} %collective-permute-done.2.refs_1_, bf16[16,3,128,256]{3,2,1,0:T(8,128)(2,1)S(1)} %all_to_all.5.refs_1_.refs_2_, ...), custom_call_target="tpu_custom_call" | custom-call | flops 1610612736 | bytes 8388608 | tf_op jit(solution)/shard_map/pallas_call | solution.py:19
  110.0 5.0 %collective-permute-start.3 = (bf16[128,2048]{1,0:T(8,128)(2,1)S(1)}, bf16[128,2048]{1,0:T(8,128)(2,1)S(1)}, u32[]{:S(2)}, u32[]{:S(2)}) collective-permute-start(bf16[128,2048]{1,0:T(8,128)(2,1)S(1)} %get-tuple-element.8), channel_id=1, source_target_pairs={{0,2},{2,4},{4,6},{6,8},{8,10},{10,12},{12,14},{14,16},{16,18},{18... | collective-permute-start | bytes 1572872 | tf_op jit(solution)/shard_map/ppermute | solution.py:31
  115.0 1.9 %collective-permute-start.4 = (bf16[128,2048]{1,0:T(8,128)(2,1)S(1)}, bf16[128,2048]{1,0:T(8,128)(2,1)S(1)}, u32[]{:S(2)}, u32[]{:S(2)}) collective-permute-start(bf16[128,2048]{1,0:T(8,128)(2,1)S(1)} %get-tuple-element.9), channel_id=1, source_target_pairs={{0,30},{2,0},{4,2},{6,4},{8,6},{10,8},{12,10},{14,12},{16,14},{18,... | collective-permute-start | bytes 1572872 | tf_op jit(solution)/shard_map/ppermute | solution.py:31
  116.9 0.0 collective-permute-done.5.refs_0_
  116.9 1.5 shard_map.87
  118.4 8.4 %collective-permute-start.6 = (bf16[64,2048]{1,0:T(8,128)(2,1)S(1)}, bf16[64,2048]{1,0:T(8,128)(2,1)S(1)}, u32[]{:S(2)}, u32[]{:S(2)}) collective-permute-start(bf16[64,2048]{1,0:T(8,128)(2,1)S(1)} %get-tuple-element.10), channel_id=1, source_target_pairs={{0,4},{2,6},{4,8},{6,10},{8,12},{10,14},{12,16},{14,18},{16,20},{1... | collective-permute-start | bytes 786440 | tf_op jit(solution)/shard_map/ppermute | solution.py:31
  126.8 1.9 %collective-permute-start.7 = (bf16[64,2048]{1,0:T(8,128)(2,1)S(1)}, bf16[64,2048]{1,0:T(8,128)(2,1)S(1)}, u32[]{:S(2)}, u32[]{:S(2)}) collective-permute-start(bf16[64,2048]{1,0:T(8,128)(2,1)S(1)} %get-tuple-element.11), channel_id=1, source_target_pairs={{0,28},{2,30},{4,0},{6,2},{8,4},{10,6},{12,8},{14,10},{16,12},{18,... | collective-permute-start | bytes 786440 | tf_op jit(solution)/shard_map/ppermute | solution.py:31
  128.8 1.5 shard_map.85.refs_0_.own_ref
  130.2 0.0 collective-permute-done.3.refs_1_.next_ref
  130.2 8.9 %collective-permute-done.4.refs_2_.prev_ref = bf16[128,2048]{1,0:T(8,128)(2,1)S(1)} collective-permute-done((bf16[128,2048]{1,0:T(8,128)(2,1)S(1)}, bf16[128,2048]{1,0:T(8,128)(2,1)S(1)}, u32[]{:S(2)}, u32[]{:S(2)}) %collective-permute-start.4) | collective-permute-done | bytes 524320 | tf_op jit(solution)/shard_map/ppermute | solution.py:31
  139.2 3.8 %collective-permute-start.9 = (bf16[32,2048]{1,0:T(8,128)(2,1)S(1)}, bf16[32,2048]{1,0:T(8,128)(2,1)S(1)}, u32[]{:S(2)}, u32[]{:S(2)}) collective-permute-start(bf16[32,2048]{1,0:T(8,128)(2,1)S(1)} %shard_map.89), channel_id=1, source_target_pairs={{0,8},{2,10},{4,12},{6,14},{8,16},{10,18},{12,20},{14,22},{16,24},... | collective-permute-start | bytes 393224 | tf_op jit(solution)/shard_map/ppermute | solution.py:37
  143.0 0.0 collective-permute-done.6.refs_3_.next2_ref
  143.0 0.0 collective-permute-done.7.refs_4_.prev2_ref
  143.0 0.1 shard_map.88
  143.1 9.8 %collective-permute-start.8 = (bf16[32,2048]{1,0:T(8,128)(2,1)S(1)}, bf16[32,2048]{1,0:T(8,128)(2,1)S(1)}, u32[]{:S(2)}, u32[]{:S(2)}) collective-permute-start(bf16[32,2048]{1,0:T(8,128)(2,1)S(1)} %shard_map.88), channel_id=1, source_target_pairs={{0,24},{2,26},{4,28},{6,30},{8,0},{10,2},{12,4},{14,6},{16,8},{18,... | collective-permute-start | bytes 393224 | tf_op jit(solution)/shard_map/ppermute | solution.py:37
  152.8 2.6 %collective-permute-done.9.refs_5_ = bf16[32,2048]{1,0:T(8,128)(2,1)S(1)} collective-permute-done((bf16[32,2048]{1,0:T(8,128)(2,1)S(1)}, bf16[32,2048]{1,0:T(8,128)(2,1)S(1)}, u32[]{:S(2)}, u32[]{:S(2)}) %collective-permute-start.9) | collective-permute-done | bytes 131104 | tf_op jit(solution)/shard_map/ppermute | solution.py:37
  155.4 0.1 shard_map.90
  155.5 1.9 %collective-permute-start.10 = (bf16[32,2048]{1,0:T(8,128)(2,1)S(1)}, bf16[32,2048]{1,0:T(8,128)(2,1)S(1)}, u32[]{:S(2)}, u32[]{:S(2)}) collective-permute-start(bf16[32,2048]{1,0:T(8,128)(2,1)S(1)} %shard_map.90), channel_id=1, source_target_pairs={{0,8},{2,10},{4,12},{6,14},{8,16},{10,18},{12,20},{14,22},{16,24},... | collective-permute-start | bytes 393224 | tf_op jit(solution)/shard_map/ppermute | solution.py:37
  157.5 1.8 %fusion = (bf16[16,1,128,256]{3,2,1,0:T(8,128)(2,1)}, bf16[16,1,128,256]{3,2,1,0:T(8,128)(2,1)}, bf16[16,1,128,256]{3,2,1,0:T(8,128)(2,1)}) fusion(bf16[16,3,128,256]{3,2,1,0:T(8,128)(2,1)S(1)} %all_to_all.5.refs_1_.refs_2_), kind=kLoop, calls=%fused_computation | loop fusion | bytes 6291456 | tf_op jit(solution)/shard_map/slice | solution.py:195
  159.2 2.6 %collective-permute-done.8.above_ref = bf16[32,2048]{1,0:T(8,128)(2,1)S(1)} collective-permute-done((bf16[32,2048]{1,0:T(8,128)(2,1)S(1)}, bf16[32,2048]{1,0:T(8,128)(2,1)S(1)}, u32[]{:S(2)}, u32[]{:S(2)}) %collective-permute-start.8) | collective-permute-done | bytes 131104 | tf_op jit(solution)/shard_map/ppermute | solution.py:37
  161.8 6.4 %collective-permute-done.10.below_ref = bf16[32,2048]{1,0:T(8,128)(2,1)S(1)} collective-permute-done((bf16[32,2048]{1,0:T(8,128)(2,1)S(1)}, bf16[32,2048]{1,0:T(8,128)(2,1)S(1)}, u32[]{:S(2)}, u32[]{:S(2)}) %collective-permute-start.10) | collective-permute-done | bytes 131104 | tf_op jit(solution)/shard_map/ppermute | solution.py:37
  168.2 0.8 shard_map.91
  (2 shorter events, 0.1 us)
Async XLA Ops:
  3.5 48.7 %copy-start = (bf16[32,2048]{1,0:T(8,128)(2,1)S(1)}, bf16[32,2048]{1,0:T(8,128)(2,1)}, u32[]{:S(2)}) copy-start(bf16[32,2048]{1,0:T(8,128)(2,1)} %tokens_ref.1) | copy-start | bytes 393220
  50.3 57.8 %collective-permute-start = (bf16[16,3,128,256]{3,2,1,0:T(8,128)(2,1)S(1)}, bf16[16,3,128,256]{3,2,1,0:T(8,128)(2,1)S(1)}, u32[]{:S(2)}, u32[]{:S(2)}) collective-permute-start(bf16[16,3,128,256]{3,2,1,0:T(8,128)(2,1)S(1)} %all_to_all.5.refs_1_.refs_2_), channel_id=1, source_target_pairs={{0,1},{1,0},{2,3},{3,2},{4,5},{5,4},{6,7},{7,6},{8,9},{9,8},{10,11... | collective-permute-start | bytes 9437192 | tf_op jit(solution)/shard_map/ppermute | solution.py:175
  84.3 12.3 %collective-permute-start.1 = (bf16[128,2048]{1,0:T(8,128)(2,1)S(1)}, bf16[128,2048]{1,0:T(8,128)(2,1)S(1)}, u32[]{:S(2)}, u32[]{:S(2)}) collective-permute-start(bf16[128,2048]{1,0:T(8,128)(2,1)S(1)} %shard_map.84.refs_0_), channel_id=1, source_target_pairs={{0,30},{2,0},{4,2},{6,4},{8,6},{10,8},{12,10},{14,12},{16,14},{18,... | collective-permute-start | bytes 1572872 | tf_op jit(solution)/shard_map/ppermute | solution.py:31
  87.7 20.4 %collective-permute-start.2 = (bf16[128,2048]{1,0:T(8,128)(2,1)S(1)}, bf16[128,2048]{1,0:T(8,128)(2,1)S(1)}, u32[]{:S(2)}, u32[]{:S(2)}) collective-permute-start(bf16[128,2048]{1,0:T(8,128)(2,1)S(1)} %shard_map.84.refs_0_), channel_id=1, source_target_pairs={{0,2},{2,4},{4,6},{6,8},{8,10},{10,12},{12,14},{14,16},{16,18},{18... | collective-permute-start | bytes 1572872 | tf_op jit(solution)/shard_map/ppermute | solution.py:31
  90.3 26.7 %collective-permute-start.5 = (bf16[128,2048]{1,0:T(8,128)(2,1)S(1)}, bf16[128,2048]{1,0:T(8,128)(2,1)S(1)}, u32[]{:S(2)}, u32[]{:S(2)}) collective-permute-start(bf16[128,2048]{1,0:T(8,128)(2,1)S(1)} %shard_map.84.refs_0_), channel_id=1, source_target_pairs={{0,28},{2,30},{4,0},{6,2},{8,4},{10,6},{12,8},{14,10},{16,12},{18,... | collective-permute-start | bytes 1572872 | tf_op jit(solution)/shard_map/ppermute | solution.py:37
  110.0 20.2 %collective-permute-start.3 = (bf16[128,2048]{1,0:T(8,128)(2,1)S(1)}, bf16[128,2048]{1,0:T(8,128)(2,1)S(1)}, u32[]{:S(2)}, u32[]{:S(2)}) collective-permute-start(bf16[128,2048]{1,0:T(8,128)(2,1)S(1)} %get-tuple-element.8), channel_id=1, source_target_pairs={{0,2},{2,4},{4,6},{6,8},{8,10},{10,12},{12,14},{14,16},{16,18},{18... | collective-permute-start | bytes 1572872 | tf_op jit(solution)/shard_map/ppermute | solution.py:31
  115.0 24.1 %collective-permute-start.4 = (bf16[128,2048]{1,0:T(8,128)(2,1)S(1)}, bf16[128,2048]{1,0:T(8,128)(2,1)S(1)}, u32[]{:S(2)}, u32[]{:S(2)}) collective-permute-start(bf16[128,2048]{1,0:T(8,128)(2,1)S(1)} %get-tuple-element.9), channel_id=1, source_target_pairs={{0,30},{2,0},{4,2},{6,4},{8,6},{10,8},{12,10},{14,12},{16,14},{18,... | collective-permute-start | bytes 1572872 | tf_op jit(solution)/shard_map/ppermute | solution.py:31
  118.4 24.6 %collective-permute-start.6 = (bf16[64,2048]{1,0:T(8,128)(2,1)S(1)}, bf16[64,2048]{1,0:T(8,128)(2,1)S(1)}, u32[]{:S(2)}, u32[]{:S(2)}) collective-permute-start(bf16[64,2048]{1,0:T(8,128)(2,1)S(1)} %get-tuple-element.10), channel_id=1, source_target_pairs={{0,4},{2,6},{4,8},{6,10},{8,12},{10,14},{12,16},{14,18},{16,20},{1... | collective-permute-start | bytes 786440 | tf_op jit(solution)/shard_map/ppermute | solution.py:31
  126.8 16.2 %collective-permute-start.7 = (bf16[64,2048]{1,0:T(8,128)(2,1)S(1)}, bf16[64,2048]{1,0:T(8,128)(2,1)S(1)}, u32[]{:S(2)}, u32[]{:S(2)}) collective-permute-start(bf16[64,2048]{1,0:T(8,128)(2,1)S(1)} %get-tuple-element.11), channel_id=1, source_target_pairs={{0,28},{2,30},{4,0},{6,2},{8,4},{10,6},{12,8},{14,10},{16,12},{18,... | collective-permute-start | bytes 786440 | tf_op jit(solution)/shard_map/ppermute | solution.py:31
  139.2 16.2 %collective-permute-start.9 = (bf16[32,2048]{1,0:T(8,128)(2,1)S(1)}, bf16[32,2048]{1,0:T(8,128)(2,1)S(1)}, u32[]{:S(2)}, u32[]{:S(2)}) collective-permute-start(bf16[32,2048]{1,0:T(8,128)(2,1)S(1)} %shard_map.89), channel_id=1, source_target_pairs={{0,8},{2,10},{4,12},{6,14},{8,16},{10,18},{12,20},{14,22},{16,24},... | collective-permute-start | bytes 393224 | tf_op jit(solution)/shard_map/ppermute | solution.py:37
  143.1 18.7 %collective-permute-start.8 = (bf16[32,2048]{1,0:T(8,128)(2,1)S(1)}, bf16[32,2048]{1,0:T(8,128)(2,1)S(1)}, u32[]{:S(2)}, u32[]{:S(2)}) collective-permute-start(bf16[32,2048]{1,0:T(8,128)(2,1)S(1)} %shard_map.88), channel_id=1, source_target_pairs={{0,24},{2,26},{4,28},{6,30},{8,0},{10,2},{12,4},{14,6},{16,8},{18,... | collective-permute-start | bytes 393224 | tf_op jit(solution)/shard_map/ppermute | solution.py:37
  155.5 12.7 %collective-permute-start.10 = (bf16[32,2048]{1,0:T(8,128)(2,1)S(1)}, bf16[32,2048]{1,0:T(8,128)(2,1)S(1)}, u32[]{:S(2)}, u32[]{:S(2)}) collective-permute-start(bf16[32,2048]{1,0:T(8,128)(2,1)S(1)} %shard_map.90), channel_id=1, source_target_pairs={{0,8},{2,10},{4,12},{6,14},{8,16},{10,18},{12,20},{14,22},{16,24},... | collective-permute-start | bytes 393224 | tf_op jit(solution)/shard_map/ppermute | solution.py:37

commit v11 on v10

--- a/solution.py
+++ b/solution.py
@@ -80,54 +80,53 @@
     )(norm_gain.reshape(1, -1), gate_master, up_master, down_master)
 
 
-def order_kernel(from_ref, held_ref):
-    rows = from_ref.shape[0] // 4
-    here = lax.axis_index("zh")
-    for k, by in enumerate((0, 2, 1, 3)):
-        held_ref[k * rows : (k + 1) * rows] = from_ref[pl.ds(pl.multiple_of((here + by) % 4 * rows, rows), rows)]
-
-
-def plane_twos(ref):
+def blocks_of(ref, by, order):
     rows = ref.shape[0] // 4
-    core = lax.axis_index("c")
-    return [ref[pl.ds(pl.multiple_of(jnp.where(core == 0, up, down) * rows, rows), rows)] for up, down in ((0, 2), (2, 1), (3, 0), (1, 3))]
-
-
-def sums_kernel(count, twos, *refs):
-    rows_refs, (own_ref, partner_ref), out_refs = refs[:count], refs[count : count + 2], refs[count + 2 :]
-    blocks = [ref[...] for ref in rows_refs[: count - twos]]
-    for ref in rows_refs[count - twos :]:
-        blocks += plane_twos(ref)
-    rows = jnp.concatenate(blocks, axis=0)
+    plane = lax.rem(lax.axis_index("zh") * 4 + lax.axis_index("zl") + by + 16, 16)
+    first = lax.div(plane, 4)
+    return [ref[pl.ds(pl.multiple_of(lax.rem(first + j, 4) * rows, rows), rows)] for j in order]
+
+
+def blocks_of_twos(ref):
+    up = lax.axis_index("c") == 0
+    return blocks_of(ref, jnp.where(up, 2, -2), [jnp.where(up, a, b) for a, b in ((0, 1), (1, 2), (3, 0), (2, 3))])
+
+
+def share(rows, weights_ref):
     width = rows.shape[1]
+    gate, up, down = (weights_ref[:, k].reshape(width, -1) for k in range(3))
     wide = rows.astype(jnp.float32)
     row_scale = lax.rsqrt(jnp.mean(wide * wide, axis=1, keepdims=True) + 1e-06)
-    hidden = []
-    for ref in (own_ref, partner_ref):
-        gate = ref[:, 0].reshape(width, -1)
-        up = ref[:, 1].reshape(width, -1)
-        gate_proj = row_scale * jnp.dot(rows, gate, preferred_element_type=jnp.float32)
-        up_proj = row_scale * jnp.dot(rows, up, preferred_element_type=jnp.float32)
-        hidden.append((gate_proj / (1.0 + jnp.exp(-gate_proj)) * up_proj).astype(jnp.bfloat16))
-    total = None
-    for ref, part in zip((own_ref, partner_ref), hidden):
-        down = ref[:, 2].reshape(width, -1)
-        share = lax.dot_general(part, down, (((1,), (1,)), ((), ())), preferred_element_type=jnp.float32)
-        total = share if total is None else total + share
+    gate_proj = row_scale * jnp.dot(rows, gate, preferred_element_type=jnp.float32)
+    up_proj = row_scale * jnp.dot(rows, up, preferred_element_type=jnp.float32)
+    hidden = (gate_proj / (1.0 + jnp.exp(-gate_proj)) * up_proj).astype(jnp.bfloat16)
+    return lax.dot_general(hidden, down, (((1,), (1,)), ((), ())), preferred_element_type=jnp.float32)
+
+
+def sums_kernel(orders, weights, begun, *refs):
+    count = len(orders)
+    rows_refs, weights_refs, refs = refs[:count], refs[count : count + weights], refs[count + weights :]
+    begun_refs, out_refs = refs[:begun], refs[begun:]
+    rows = jnp.concatenate([block for order, ref in zip(orders, rows_refs) for block in order(ref)], axis=0)
+    total = begun_refs[0][...] if begun else None
+    for ref in weights_refs:
+        added = share(rows, ref)
+        total = added if total is None else total + added
     at = 0
     for ref in out_refs:
         ref[...] = total[at : at + ref.shape[0]].astype(ref.dtype)
         at += ref.shape[0]
 
 
-def partial_sums(parts, twos, weights, counts, dtype):
-    units = 2 * weights[0].shape[-1]
+def partial_sums(parts, orders, weights, counts, dtype, begun=()):
+    units = len(weights) * weights[0].shape[-1]
     count, width = sum(counts), parts[0].shape[1]
     return local(
-        lambda *refs: sums_kernel(len(parts), twos, *refs),
+        lambda *refs: sums_kernel(orders, len(weights), len(begun), *refs),
         tuple(jax.ShapeDtypeStruct((k, width), dtype) for k in counts),
         *parts,
         *weights,
+        *begun,
         flops=6 * count * width * units,
         transcendentals=count * units,
     )
@@ -165,9 +164,8 @@
 def step(tokens, norm_gain, gate_master, up_master, down_master):
     copies = weight_copies(norm_gain, gate_master, up_master, down_master, lax.axis_size("fs"))
     packed = lax.all_to_all(copies, "fs", split_axis=0, concat_axis=0, tiled=True)
-    spread = lax.all_gather(tokens, "zh", axis=0, tiled=True)
+    held = lax.all_gather(tokens, "zh", axis=0, tiled=True)
     rows, width = tokens.shape
-    (held,) = local(order_kernel, (jax.ShapeDtypeStruct((4 * rows, width), tokens.dtype),), spread)
     from_next = move(held, -1)
     from_prev = move(held, 1)
     from_twos = move_by_core(held, -2)
@@ -175,13 +173,18 @@
     partner = lax.ppermute(packed, "c", [(0, 1), (1, 0)])
     weights = (packed, partner)
 
-    for_next, for_prev = partial_sums((from_next, from_prev), 0, weights, (4 * rows, 4 * rows), jnp.bfloat16)
+    def around(by):
+        return lambda ref: blocks_of(ref, by, (0, 2, 1, 3))
+
+    sides, orders = (from_next, from_prev), (around(1), around(-1))
+    half = partial_sums(sides, orders, weights[:1], (8 * rows,), jnp.float32)
+    for_next, for_prev = partial_sums(sides, orders, weights[1:], (4 * rows, 4 * rows), jnp.bfloat16, half)
     to_next = move(for_next, 1)
     to_prev = move(for_prev, -1)
-    for_next2, for_prev2 = partial_sums((from_twos,), 1, weights, (2 * rows, 2 * rows), jnp.bfloat16)
+    for_next2, for_prev2 = partial_sums((from_twos,), (blocks_of_twos,), weights, (2 * rows, 2 * rows), jnp.bfloat16)
     to_next2 = move(for_next2, 2)
     to_prev2 = move(for_prev2, -2)
-    (own,) = partial_sums((held,), 0, weights, (4 * rows,), jnp.float32)
+    (own,) = partial_sums((held,), (around(0),), weights, (4 * rows,), jnp.float32)
 
     block = jax.ShapeDtypeStruct((rows, width), jnp.bfloat16)
     (sum_far,) = local(fold_far_kernel, (block,), own, to_next, to_prev)

time: 169 us -> 169 us (level)
  no operation moved by 1% of the time
where the time goes in v11:
time: 169 us; the launch traced here: 168 us
  blocking collectives  78.8 us (47%)
  starting transfers between devices  44.5 us (26%)
  waiting for transfers between devices  33.4 us (20%)
  Pallas kernels  8.97 us (5%)
  local copies, waits for them, and re-layouts  1.76 us (1%)
    all_to_all x1, blocking collectives, step(): lax.all_to_all(copies, 'fs', split_axis=0, concat_axis=0, tiled=True)  46.8 us
    all_gather x1, blocking collectives, step(): held = lax.all_gather(tokens, 'zh', axis=0, tiled=True)  32 us
    ppermute x6, starting transfers between devices, move(): lax.ppermute(array, Z, [(i, (i + by) % planes) for i in range(planes)])  23.1 us
    ppermute x6, waiting for transfers between devices, move(): lax.ppermute(array, Z, [(i, (i + by) % planes) for i in range(planes)])  22.7 us
    ppermute x4, starting transfers between devices, move_by_core(): return lax.ppermute(array, TP, pairs)  19.4 us
    ppermute x4, waiting for transfers between devices, move_by_core(): return lax.ppermute(array, TP, pairs)  10.7 us
    pallas_call x8, Pallas kernels, local(): pl.pallas_call(kernel, out_shape=outs, in_specs=[VMEM] * len(args), out_s...  6.11 us
  transfers between devices with their start and end apart: 11, of which 6 were waited for; matrix products, arithmetic and copies ran while one was open for 1% of the time, Pallas kernels for 3%

profile of v11, /device:TPU:64, one launch (start us, length us, event | category | flops | bytes accessed | tf_op | source)
XLA Modules:
  0.0 168.2 jit_solution(14691681514532245515)
XLA Ops:
  0.6 2.9 %prepare.1 = bf16[16,3,128,256]{3,2,1,0:T(8,128)(2,1)} custom-call(f32[1,128]{1,0:T(1,128)} %bitcast.7, f32[128,256]{1,0:T(8,128)} %gate_hbm.1, f32[128,256]{1,0:T(8,128)} %up_hbm.1, f32[128,256]{1,0:T(8,128)} %down_hbm.1), custom_call_target="tpu_custom_call" | custom-call | flops 1000000 | bytes 4000000 | tf_op jit(solution)/shard_map/prepare/pallas_call | solution.py:65
  3.5 0.0 copy-start
  3.5 46.8 %all_to_all.5.refs_1_.refs_2_ = bf16[16,3,128,256]{3,2,1,0:T(8,128)(2,1)S(1)} all-to-all(bf16[16,3,128,256]{3,2,1,0:T(8,128)(2,1)} %prepare.1), channel_id=1, replica_groups=mesh['fs'=16,'zh'=4,'zl'=4,'c'=2] {'fs'}, dimensions={0} | all-to-all | bytes 6291456 | tf_op jit(solution)/shard_map/all_to_all | solution.py:166
  50.3 1.9 %collective-permute-start = (bf16[16,3,128,256]{3,2,1,0:T(8,128)(2,1)S(1)}, bf16[16,3,128,256]{3,2,1,0:T(8,128)(2,1)S(1)}, u32[]{:S(2)}, u32[]{:S(2)}) collective-permute-start(bf16[16,3,128,256]{3,2,1,0:T(8,128)(2,1)S(1)} %all_to_all.5.refs_1_.refs_2_), channel_id=1, source_target_pairs={{0,1},{1,0},{2,3},{3,2},{4,5},{5,4},{6,7},{7,6},{8,9},{9,8},{10,11... | collective-permute-start | bytes 9437192 | tf_op jit(solution)/shard_map/ppermute | solution.py:173
  52.2 0.0 copy-done
  52.2 32.0 %all_gather.3.refs_0_ = bf16[128,2048]{1,0:T(8,128)(2,1)S(1)} all-gather(bf16[32,2048]{1,0:T(8,128)(2,1)S(1)} %copy-done), channel_id=1, replica_groups=mesh['fs'=16,'zh'=4,'zl'=4,'c'=2] {'zh'}, dimensions={0}, use_global_device_ids=true | all-gather | bytes 655360 | tf_op jit(solution)/shard_map/all_gather | solution.py:167
  84.3 3.4 %collective-permute-start.1 = (bf16[128,2048]{1,0:T(8,128)(2,1)S(1)}, bf16[128,2048]{1,0:T(8,128)(2,1)S(1)}, u32[]{:S(2)}, u32[]{:S(2)}) collective-permute-start(bf16[128,2048]{1,0:T(8,128)(2,1)S(1)} %all_gather.3.refs_0_), channel_id=1, source_target_pairs={{0,30},{2,0},{4,2},{6,4},{8,6},{10,8},{12,10},{14,12},{16,14},{18,... | collective-permute-start | bytes 1572872 | tf_op jit(solution)/shard_map/ppermute | solution.py:31
  87.7 2.5 %collective-permute-start.2 = (bf16[128,2048]{1,0:T(8,128)(2,1)S(1)}, bf16[128,2048]{1,0:T(8,128)(2,1)S(1)}, u32[]{:S(2)}, u32[]{:S(2)}) collective-permute-start(bf16[128,2048]{1,0:T(8,128)(2,1)S(1)} %all_gather.3.refs_0_), channel_id=1, source_target_pairs={{0,2},{2,4},{4,6},{6,8},{8,10},{10,12},{12,14},{14,16},{16,18},{18... | collective-permute-start | bytes 1572872 | tf_op jit(solution)/shard_map/ppermute | solution.py:31
  90.2 4.1 %collective-permute-start.5 = (bf16[128,2048]{1,0:T(8,128)(2,1)S(1)}, bf16[128,2048]{1,0:T(8,128)(2,1)S(1)}, u32[]{:S(2)}, u32[]{:S(2)}) collective-permute-start(bf16[128,2048]{1,0:T(8,128)(2,1)S(1)} %all_gather.3.refs_0_), channel_id=1, source_target_pairs={{0,28},{2,30},{4,0},{6,2},{8,4},{10,6},{12,8},{14,10},{16,12},{18,... | collective-permute-start | bytes 1572872 | tf_op jit(solution)/shard_map/ppermute | solution.py:37
  94.3 2.2 %collective-permute-done.1.refs_0_ = bf16[128,2048]{1,0:T(8,128)(2,1)S(1)} collective-permute-done((bf16[128,2048]{1,0:T(8,128)(2,1)S(1)}, bf16[128,2048]{1,0:T(8,128)(2,1)S(1)}, u32[]{:S(2)}, u32[]{:S(2)}) %collective-permute-start.1) | collective-permute-done | bytes 524320 | tf_op jit(solution)/shard_map/ppermute | solution.py:31
  96.5 11.6 %collective-permute-done.2.refs_1_ = bf16[128,2048]{1,0:T(8,128)(2,1)S(1)} collective-permute-done((bf16[128,2048]{1,0:T(8,128)(2,1)S(1)}, bf16[128,2048]{1,0:T(8,128)(2,1)S(1)}, u32[]{:S(2)}, u32[]{:S(2)}) %collective-permute-start.2) | collective-permute-done | bytes 524320 | tf_op jit(solution)/shard_map/ppermute | solution.py:31
  108.1 1.1 shard_map.85.refs_3_
  109.2 0.0 collective-permute-done.refs_2_
  109.2 1.1 shard_map.86
  110.3 5.0 %collective-permute-start.3 = (bf16[128,2048]{1,0:T(8,128)(2,1)S(1)}, bf16[128,2048]{1,0:T(8,128)(2,1)S(1)}, u32[]{:S(2)}, u32[]{:S(2)}) collective-permute-start(bf16[128,2048]{1,0:T(8,128)(2,1)S(1)} %get-tuple-element.8), channel_id=1, source_target_pairs={{0,2},{2,4},{4,6},{6,8},{8,10},{10,12},{12,14},{14,16},{16,18},{18... | collective-permute-start | bytes 1572872 | tf_op jit(solution)/shard_map/ppermute | solution.py:31
  115.2 1.9 %collective-permute-start.4 = (bf16[128,2048]{1,0:T(8,128)(2,1)S(1)}, bf16[128,2048]{1,0:T(8,128)(2,1)S(1)}, u32[]{:S(2)}, u32[]{:S(2)}) collective-permute-start(bf16[128,2048]{1,0:T(8,128)(2,1)S(1)} %get-tuple-element.9), channel_id=1, source_target_pairs={{0,30},{2,0},{4,2},{6,4},{8,6},{10,8},{12,10},{14,12},{16,14},{18,... | collective-permute-start | bytes 1572872 | tf_op jit(solution)/shard_map/ppermute | solution.py:31
  117.2 0.0 collective-permute-done.5.refs_0_
  117.2 1.5 shard_map.87
  118.6 8.4 %collective-permute-start.6 = (bf16[64,2048]{1,0:T(8,128)(2,1)S(1)}, bf16[64,2048]{1,0:T(8,128)(2,1)S(1)}, u32[]{:S(2)}, u32[]{:S(2)}) collective-permute-start(bf16[64,2048]{1,0:T(8,128)(2,1)S(1)} %get-tuple-element.10), channel_id=1, source_target_pairs={{0,4},{2,6},{4,8},{6,10},{8,12},{10,14},{12,16},{14,18},{16,20},{1... | collective-permute-start | bytes 786440 | tf_op jit(solution)/shard_map/ppermute | solution.py:31
  127.0 1.9 %collective-permute-start.7 = (bf16[64,2048]{1,0:T(8,128)(2,1)S(1)}, bf16[64,2048]{1,0:T(8,128)(2,1)S(1)}, u32[]{:S(2)}, u32[]{:S(2)}) collective-permute-start(bf16[64,2048]{1,0:T(8,128)(2,1)S(1)} %get-tuple-element.11), channel_id=1, source_target_pairs={{0,28},{2,30},{4,0},{6,2},{8,4},{10,6},{12,8},{14,10},{16,12},{18,... | collective-permute-start | bytes 786440 | tf_op jit(solution)/shard_map/ppermute | solution.py:31
  129.0 1.5 shard_map.84.refs_0_.own_ref
  130.4 0.0 collective-permute-done.3.refs_1_.next_ref
  130.4 8.9 %collective-permute-done.4.refs_2_.prev_ref = bf16[128,2048]{1,0:T(8,128)(2,1)S(1)} collective-permute-done((bf16[128,2048]{1,0:T(8,128)(2,1)S(1)}, bf16[128,2048]{1,0:T(8,128)(2,1)S(1)}, u32[]{:S(2)}, u32[]{:S(2)}) %collective-permute-start.4) | collective-permute-done | bytes 524320 | tf_op jit(solution)/shard_map/ppermute | solution.py:31
  139.4 3.8 %collective-permute-start.9 = (bf16[32,2048]{1,0:T(8,128)(2,1)S(1)}, bf16[32,2048]{1,0:T(8,128)(2,1)S(1)}, u32[]{:S(2)}, u32[]{:S(2)}) collective-permute-start(bf16[32,2048]{1,0:T(8,128)(2,1)S(1)} %shard_map.89), channel_id=1, source_target_pairs={{0,8},{2,10},{4,12},{6,14},{8,16},{10,18},{12,20},{14,22},{16,24},... | collective-permute-start | bytes 393224 | tf_op jit(solution)/shard_map/ppermute | solution.py:37
  143.3 0.0 collective-permute-done.6.refs_3_.next2_ref
  143.3 0.0 collective-permute-done.7.refs_4_.prev2_ref
  143.3 0.1 shard_map.88
  143.4 9.6 %collective-permute-start.8 = (bf16[32,2048]{1,0:T(8,128)(2,1)S(1)}, bf16[32,2048]{1,0:T(8,128)(2,1)S(1)}, u32[]{:S(2)}, u32[]{:S(2)}) collective-permute-start(bf16[32,2048]{1,0:T(8,128)(2,1)S(1)} %shard_map.88), channel_id=1, source_target_pairs={{0,24},{2,26},{4,28},{6,30},{8,0},{10,2},{12,4},{14,6},{16,8},{18,... | collective-permute-start | bytes 393224 | tf_op jit(solution)/shard_map/ppermute | solution.py:37
  153.0 3.4 %collective-permute-done.9.refs_5_ = bf16[32,2048]{1,0:T(8,128)(2,1)S(1)} collective-permute-done((bf16[32,2048]{1,0:T(8,128)(2,1)S(1)}, bf16[32,2048]{1,0:T(8,128)(2,1)S(1)}, u32[]{:S(2)}, u32[]{:S(2)}) %collective-permute-start.9) | collective-permute-done | bytes 131104 | tf_op jit(solution)/shard_map/ppermute | solution.py:37
  156.3 0.1 shard_map.90
  156.4 1.9 %collective-permute-start.10 = (bf16[32,2048]{1,0:T(8,128)(2,1)S(1)}, bf16[32,2048]{1,0:T(8,128)(2,1)S(1)}, u32[]{:S(2)}, u32[]{:S(2)}) collective-permute-start(bf16[32,2048]{1,0:T(8,128)(2,1)S(1)} %shard_map.90), channel_id=1, source_target_pairs={{0,8},{2,10},{4,12},{6,14},{8,16},{10,18},{12,20},{14,22},{16,24},... | collective-permute-start | bytes 393224 | tf_op jit(solution)/shard_map/ppermute | solution.py:37
  158.3 1.8 %fusion = (bf16[16,1,128,256]{3,2,1,0:T(8,128)(2,1)}, bf16[16,1,128,256]{3,2,1,0:T(8,128)(2,1)}, bf16[16,1,128,256]{3,2,1,0:T(8,128)(2,1)}) fusion(bf16[16,3,128,256]{3,2,1,0:T(8,128)(2,1)S(1)} %all_to_all.5.refs_1_.refs_2_), kind=kLoop, calls=%fused_computation | loop fusion | bytes 6291456 | tf_op jit(solution)/shard_map/slice | solution.py:198
  160.1 1.6 collective-permute-done.8.above_ref
  161.7 5.7 %collective-permute-done.10.below_ref = bf16[32,2048]{1,0:T(8,128)(2,1)S(1)} collective-permute-done((bf16[32,2048]{1,0:T(8,128)(2,1)S(1)}, bf16[32,2048]{1,0:T(8,128)(2,1)S(1)}, u32[]{:S(2)}, u32[]{:S(2)}) %collective-permute-start.10) | collective-permute-done | bytes 131104 | tf_op jit(solution)/shard_map/ppermute | solution.py:37
  167.4 0.8 shard_map.91
  (1 shorter events, 0.0 us)
Async XLA Ops:
  3.5 48.7 %copy-start = (bf16[32,2048]{1,0:T(8,128)(2,1)S(1)}, bf16[32,2048]{1,0:T(8,128)(2,1)}, u32[]{:S(2)}) copy-start(bf16[32,2048]{1,0:T(8,128)(2,1)} %tokens_ref.1) | copy-start | bytes 393220
  50.3 58.8 %collective-permute-start = (bf16[16,3,128,256]{3,2,1,0:T(8,128)(2,1)S(1)}, bf16[16,3,128,256]{3,2,1,0:T(8,128)(2,1)S(1)}, u32[]{:S(2)}, u32[]{:S(2)}) collective-permute-start(bf16[16,3,128,256]{3,2,1,0:T(8,128)(2,1)S(1)} %all_to_all.5.refs_1_.refs_2_), channel_id=1, source_target_pairs={{0,1},{1,0},{2,3},{3,2},{4,5},{5,4},{6,7},{7,6},{8,9},{9,8},{10,11... | collective-permute-start | bytes 9437192 | tf_op jit(solution)/shard_map/ppermute | solution.py:173
  84.3 12.3 %collective-permute-start.1 = (bf16[128,2048]{1,0:T(8,128)(2,1)S(1)}, bf16[128,2048]{1,0:T(8,128)(2,1)S(1)}, u32[]{:S(2)}, u32[]{:S(2)}) collective-permute-start(bf16[128,2048]{1,0:T(8,128)(2,1)S(1)} %all_gather.3.refs_0_), channel_id=1, source_target_pairs={{0,30},{2,0},{4,2},{6,4},{8,6},{10,8},{12,10},{14,12},{16,14},{18,... | collective-permute-start | bytes 1572872 | tf_op jit(solution)/shard_map/ppermute | solution.py:31
  87.7 20.4 %collective-permute-start.2 = (bf16[128,2048]{1,0:T(8,128)(2,1)S(1)}, bf16[128,2048]{1,0:T(8,128)(2,1)S(1)}, u32[]{:S(2)}, u32[]{:S(2)}) collective-permute-start(bf16[128,2048]{1,0:T(8,128)(2,1)S(1)} %all_gather.3.refs_0_), channel_id=1, source_target_pairs={{0,2},{2,4},{4,6},{6,8},{8,10},{10,12},{12,14},{14,16},{16,18},{18... | collective-permute-start | bytes 1572872 | tf_op jit(solution)/shard_map/ppermute | solution.py:31
  90.2 27.0 %collective-permute-start.5 = (bf16[128,2048]{1,0:T(8,128)(2,1)S(1)}, bf16[128,2048]{1,0:T(8,128)(2,1)S(1)}, u32[]{:S(2)}, u32[]{:S(2)}) collective-permute-start(bf16[128,2048]{1,0:T(8,128)(2,1)S(1)} %all_gather.3.refs_0_), channel_id=1, source_target_pairs={{0,28},{2,30},{4,0},{6,2},{8,4},{10,6},{12,8},{14,10},{16,12},{18,... | collective-permute-start | bytes 1572872 | tf_op jit(solution)/shard_map/ppermute | solution.py:37
  110.3 20.2 %collective-permute-start.3 = (bf16[128,2048]{1,0:T(8,128)(2,1)S(1)}, bf16[128,2048]{1,0:T(8,128)(2,1)S(1)}, u32[]{:S(2)}, u32[]{:S(2)}) collective-permute-start(bf16[128,2048]{1,0:T(8,128)(2,1)S(1)} %get-tuple-element.8), channel_id=1, source_target_pairs={{0,2},{2,4},{4,6},{6,8},{8,10},{10,12},{12,14},{14,16},{16,18},{18... | collective-permute-start | bytes 1572872 | tf_op jit(solution)/shard_map/ppermute | solution.py:31
  115.2 24.1 %collective-permute-start.4 = (bf16[128,2048]{1,0:T(8,128)(2,1)S(1)}, bf16[128,2048]{1,0:T(8,128)(2,1)S(1)}, u32[]{:S(2)}, u32[]{:S(2)}) collective-permute-start(bf16[128,2048]{1,0:T(8,128)(2,1)S(1)} %get-tuple-element.9), channel_id=1, source_target_pairs={{0,30},{2,0},{4,2},{6,4},{8,6},{10,8},{12,10},{14,12},{16,14},{18,... | collective-permute-start | bytes 1572872 | tf_op jit(solution)/shard_map/ppermute | solution.py:31
  118.6 24.6 %collective-permute-start.6 = (bf16[64,2048]{1,0:T(8,128)(2,1)S(1)}, bf16[64,2048]{1,0:T(8,128)(2,1)S(1)}, u32[]{:S(2)}, u32[]{:S(2)}) collective-permute-start(bf16[64,2048]{1,0:T(8,128)(2,1)S(1)} %get-tuple-element.10), channel_id=1, source_target_pairs={{0,4},{2,6},{4,8},{6,10},{8,12},{10,14},{12,16},{14,18},{16,20},{1... | collective-permute-start | bytes 786440 | tf_op jit(solution)/shard_map/ppermute | solution.py:31
  127.0 16.2 %collective-permute-start.7 = (bf16[64,2048]{1,0:T(8,128)(2,1)S(1)}, bf16[64,2048]{1,0:T(8,128)(2,1)S(1)}, u32[]{:S(2)}, u32[]{:S(2)}) collective-permute-start(bf16[64,2048]{1,0:T(8,128)(2,1)S(1)} %get-tuple-element.11), channel_id=1, source_target_pairs={{0,28},{2,30},{4,0},{6,2},{8,4},{10,6},{12,8},{14,10},{16,12},{18,... | collective-permute-start | bytes 786440 | tf_op jit(solution)/shard_map/ppermute | solution.py:31
  139.4 16.9 %collective-permute-start.9 = (bf16[32,2048]{1,0:T(8,128)(2,1)S(1)}, bf16[32,2048]{1,0:T(8,128)(2,1)S(1)}, u32[]{:S(2)}, u32[]{:S(2)}) collective-permute-start(bf16[32,2048]{1,0:T(8,128)(2,1)S(1)} %shard_map.89), channel_id=1, source_target_pairs={{0,8},{2,10},{4,12},{6,14},{8,16},{10,18},{12,20},{14,22},{16,24},... | collective-permute-start | bytes 393224 | tf_op jit(solution)/shard_map/ppermute | solution.py:37
  143.4 18.3 %collective-permute-start.8 = (bf16[32,2048]{1,0:T(8,128)(2,1)S(1)}, bf16[32,2048]{1,0:T(8,128)(2,1)S(1)}, u32[]{:S(2)}, u32[]{:S(2)}) collective-permute-start(bf16[32,2048]{1,0:T(8,128)(2,1)S(1)} %shard_map.88), channel_id=1, source_target_pairs={{0,24},{2,26},{4,28},{6,30},{8,0},{10,2},{12,4},{14,6},{16,8},{18,... | collective-permute-start | bytes 393224 | tf_op jit(solution)/shard_map/ppermute | solution.py:37
  156.4 11.0 %collective-permute-start.10 = (bf16[32,2048]{1,0:T(8,128)(2,1)S(1)}, bf16[32,2048]{1,0:T(8,128)(2,1)S(1)}, u32[]{:S(2)}, u32[]{:S(2)}) collective-permute-start(bf16[32,2048]{1,0:T(8,128)(2,1)S(1)} %shard_map.90), channel_id=1, source_target_pairs={{0,8},{2,10},{4,12},{6,14},{8,16},{10,18},{12,20},{14,22},{16,24},... | collective-permute-start | bytes 393224 | tf_op jit(solution)/shard_map/ppermute | solution.py:37

commit v12 on v10

--- a/solution.py
+++ b/solution.py
@@ -80,25 +80,22 @@
     )(norm_gain.reshape(1, -1), gate_master, up_master, down_master)
 
 
-def order_kernel(from_ref, held_ref):
-    rows = from_ref.shape[0] // 4
-    here = lax.axis_index("zh")
-    for k, by in enumerate((0, 2, 1, 3)):
-        held_ref[k * rows : (k + 1) * rows] = from_ref[pl.ds(pl.multiple_of((here + by) % 4 * rows, rows), rows)]
-
-
-def plane_twos(ref):
+def blocks_of(ref, by, order):
     rows = ref.shape[0] // 4
-    core = lax.axis_index("c")
-    return [ref[pl.ds(pl.multiple_of(jnp.where(core == 0, up, down) * rows, rows), rows)] for up, down in ((0, 2), (2, 1), (3, 0), (1, 3))]
-
-
-def sums_kernel(count, twos, *refs):
+    plane = lax.rem(lax.axis_index("zh") * 4 + lax.axis_index("zl") + by + 16, 16)
+    first = lax.div(plane, 4)
+    return [ref[pl.ds(pl.multiple_of(lax.rem(first + j, 4) * rows, rows), rows)] for j in order]
+
+
+def blocks_of_twos(ref):
+    up = lax.axis_index("c") == 0
+    return blocks_of(ref, jnp.where(up, 2, -2), [jnp.where(up, a, b) for a, b in ((0, 1), (1, 2), (3, 0), (2, 3))])
+
+
+def sums_kernel(orders, *refs):
+    count = len(orders)
     rows_refs, (own_ref, partner_ref), out_refs = refs[:count], refs[count : count + 2], refs[count + 2 :]
-    blocks = [ref[...] for ref in rows_refs[: count - twos]]
-    for ref in rows_refs[count - twos :]:
-        blocks += plane_twos(ref)
-    rows = jnp.concatenate(blocks, axis=0)
+    rows = jnp.concatenate([block for order, ref in zip(orders, rows_refs) for block in order(ref)], axis=0)
     width = rows.shape[1]
     wide = rows.astype(jnp.float32)
     row_scale = lax.rsqrt(jnp.mean(wide * wide, axis=1, keepdims=True) + 1e-06)
@@ -120,12 +117,12 @@
         at += ref.shape[0]
 
 
-def partial_sums(parts, twos, weights, counts, dtype):
+def partial_sums(parts, orders, weights, counts, dtypes):
     units = 2 * weights[0].shape[-1]
     count, width = sum(counts), parts[0].shape[1]
     return local(
-        lambda *refs: sums_kernel(len(parts), twos, *refs),
-        tuple(jax.ShapeDtypeStruct((k, width), dtype) for k in counts),
+        lambda *refs: sums_kernel(orders, *refs),
+        tuple(jax.ShapeDtypeStruct((k, width), dtype) for k, dtype in zip(counts, dtypes)),
         *parts,
         *weights,
         flops=6 * count * width * units,
@@ -165,9 +162,8 @@
 def step(tokens, norm_gain, gate_master, up_master, down_master):
     copies = weight_copies(norm_gain, gate_master, up_master, down_master, lax.axis_size("fs"))
     packed = lax.all_to_all(copies, "fs", split_axis=0, concat_axis=0, tiled=True)
-    spread = lax.all_gather(tokens, "zh", axis=0, tiled=True)
+    held = lax.all_gather(tokens, "zh", axis=0, tiled=True)
     rows, width = tokens.shape
-    (held,) = local(order_kernel, (jax.ShapeDtypeStruct((4 * rows, width), tokens.dtype),), spread)
     from_next = move(held, -1)
     from_prev = move(held, 1)
     from_twos = move_by_core(held, -2)
@@ -175,13 +171,18 @@
     partner = lax.ppermute(packed, "c", [(0, 1), (1, 0)])
     weights = (packed, partner)
 
-    for_next, for_prev = partial_sums((from_next, from_prev), 0, weights, (4 * rows, 4 * rows), jnp.bfloat16)
+    def around(by):
+        return lambda ref: blocks_of(ref, by, (0, 2, 1, 3))
+
+    narrow = jnp.bfloat16
+    for_next, for_prev, own = partial_sums(
+        (from_next, from_prev, held), (around(1), around(-1), around(0)), weights, (4 * rows,) * 3, (narrow, narrow, jnp.float32)
+    )
     to_next = move(for_next, 1)
     to_prev = move(for_prev, -1)
-    for_next2, for_prev2 = partial_sums((from_twos,), 1, weights, (2 * rows, 2 * rows), jnp.bfloat16)
+    for_next2, for_prev2 = partial_sums((from_twos,), (blocks_of_twos,), weights, (2 * rows,) * 2, (narrow, narrow))
+    to_prev2 = move(for_prev2, -2)
     to_next2 = move(for_next2, 2)
-    to_prev2 = move(for_prev2, -2)
-    (own,) = partial_sums((held,), 0, weights, (4 * rows,), jnp.float32)
 
     block = jax.ShapeDtypeStruct((rows, width), jnp.bfloat16)
     (sum_far,) = local(fold_far_kernel, (block,), own, to_next, to_prev)

time: 169 us -> 169 us (level)
    ppermute x4, waiting for transfers between devices: 11.6 us -> 8.42 us  [move_by_core(): return lax.ppermute(array, TP, pairs)]
    ppermute x6, waiting for transfers between devices: 22.7 us -> 24.8 us  [move(): lax.ppermute(array, Z, [(i, (i + by) % planes) for i in range(planes)])]
    pallas_call x8 -> x6, Pallas kernels: 5.87 us -> 5.18 us  [local(): pl.pallas_call(kernel, out_shape=outs, in_specs=[VMEM] * len(args), out_s...]
  transfers between devices with their start and end apart: 11 -> 11, of which waited for: 6 -> 7; matrix products, arithmetic and copies ran while one was open for 1% -> 1% of each run, Pallas kernels for 3% -> 3%
where the time goes in v12:
time: 169 us
  blocking collectives  78.8 us (47%)
  starting transfers between devices  46 us (27%)
  waiting for transfers between devices  33.2 us (20%)
  Pallas kernels  8.04 us (5%)
  local copies, waits for them, and re-layouts  1.76 us (1%)
    all_to_all x1, blocking collectives, step(): lax.all_to_all(copies, 'fs', split_axis=0, concat_axis=0, tiled=True)  46.8 us
    all_gather x1, blocking collectives, step(): held = lax.all_gather(tokens, 'zh', axis=0, tiled=True)  32 us
    ppermute x6, waiting for transfers between devices, move(): lax.ppermute(array, Z, [(i, (i + by) % planes) for i in range(planes)])  24.8 us
    ppermute x6, starting transfers between devices, move(): lax.ppermute(array, Z, [(i, (i + by) % planes) for i in range(planes)])  23.1 us
    ppermute x4, starting transfers between devices, move_by_core(): return lax.ppermute(array, TP, pairs)  21 us
    ppermute x4, waiting for transfers between devices, move_by_core(): return lax.ppermute(array, TP, pairs)  8.42 us
    pallas_call x6, Pallas kernels, local(): pl.pallas_call(kernel, out_shape=outs, in_specs=[VMEM] * len(args), out_s...  5.18 us
  transfers between devices with their start and end apart: 11, of which 7 were waited for; matrix products, arithmetic and copies ran while one was open for 1% of the time, Pallas kernels for 3%

profile of v12, /device:TPU:64, one launch (start us, length us, event | category | flops | bytes accessed | tf_op | source)
XLA Modules:
  0.0 168.6 jit_solution(6630025667420149134)
XLA Ops:
  0.6 2.9 %prepare.1 = bf16[16,3,128,256]{3,2,1,0:T(8,128)(2,1)} custom-call(f32[1,128]{1,0:T(1,128)} %bitcast.7, f32[128,256]{1,0:T(8,128)} %gate_hbm.1, f32[128,256]{1,0:T(8,128)} %up_hbm.1, f32[128,256]{1,0:T(8,128)} %down_hbm.1), custom_call_target="tpu_custom_call" | custom-call | flops 1000000 | bytes 4000000 | tf_op jit(solution)/shard_map/prepare/pallas_call | solution.py:65
  3.5 0.0 copy-start
  3.5 46.8 %all_to_all.5.refs_3_.refs_1_ = bf16[16,3,128,256]{3,2,1,0:T(8,128)(2,1)S(1)} all-to-all(bf16[16,3,128,256]{3,2,1,0:T(8,128)(2,1)} %prepare.1), channel_id=1, replica_groups=mesh['fs'=16,'zh'=4,'zl'=4,'c'=2] {'fs'}, dimensions={0} | all-to-all | bytes 6291456 | tf_op jit(solution)/shard_map/all_to_all | solution.py:164
  50.3 1.9 %collective-permute-start.2 = (bf16[16,3,128,256]{3,2,1,0:T(8,128)(2,1)S(1)}, bf16[16,3,128,256]{3,2,1,0:T(8,128)(2,1)S(1)}, u32[]{:S(2)}, u32[]{:S(2)}) collective-permute-start(bf16[16,3,128,256]{3,2,1,0:T(8,128)(2,1)S(1)} %all_to_all.5.refs_3_.refs_1_), channel_id=1, source_target_pairs={{0,1},{1,0},{2,3},{3,2},{4,5},{5,4},{6,7},{7,6},{8,9},{9,8},{10,11... | collective-permute-start | bytes 9437192 | tf_op jit(solution)/shard_map/ppermute | solution.py:171
  52.2 0.0 copy-done
  52.2 32.0 %all_gather.3.refs_2_ = bf16[128,2048]{1,0:T(8,128)(2,1)S(1)} all-gather(bf16[32,2048]{1,0:T(8,128)(2,1)S(1)} %copy-done), channel_id=1, replica_groups=mesh['fs'=16,'zh'=4,'zl'=4,'c'=2] {'zh'}, dimensions={0}, use_global_device_ids=true | all-gather | bytes 655360 | tf_op jit(solution)/shard_map/all_gather | solution.py:165
  84.3 3.4 %collective-permute-start = (bf16[128,2048]{1,0:T(8,128)(2,1)S(1)}, bf16[128,2048]{1,0:T(8,128)(2,1)S(1)}, u32[]{:S(2)}, u32[]{:S(2)}) collective-permute-start(bf16[128,2048]{1,0:T(8,128)(2,1)S(1)} %all_gather.3.refs_2_), channel_id=1, source_target_pairs={{0,30},{2,0},{4,2},{6,4},{8,6},{10,8},{12,10},{14,12},{16,14},{18,... | collective-permute-start | bytes 1572872 | tf_op jit(solution)/shard_map/ppermute | solution.py:31
  87.7 2.5 %collective-permute-start.1 = (bf16[128,2048]{1,0:T(8,128)(2,1)S(1)}, bf16[128,2048]{1,0:T(8,128)(2,1)S(1)}, u32[]{:S(2)}, u32[]{:S(2)}) collective-permute-start(bf16[128,2048]{1,0:T(8,128)(2,1)S(1)} %all_gather.3.refs_2_), channel_id=1, source_target_pairs={{0,2},{2,4},{4,6},{6,8},{8,10},{10,12},{12,14},{14,16},{16,18},{18... | collective-permute-start | bytes 1572872 | tf_op jit(solution)/shard_map/ppermute | solution.py:31
  90.2 4.1 %collective-permute-start.5 = (bf16[128,2048]{1,0:T(8,128)(2,1)S(1)}, bf16[128,2048]{1,0:T(8,128)(2,1)S(1)}, u32[]{:S(2)}, u32[]{:S(2)}) collective-permute-start(bf16[128,2048]{1,0:T(8,128)(2,1)S(1)} %all_gather.3.refs_2_), channel_id=1, source_target_pairs={{0,28},{2,30},{4,0},{6,2},{8,4},{10,6},{12,8},{14,10},{16,12},{18,... | collective-permute-start | bytes 1572872 | tf_op jit(solution)/shard_map/ppermute | solution.py:37
  94.3 2.2 %collective-permute-done.refs_0_ = bf16[128,2048]{1,0:T(8,128)(2,1)S(1)} collective-permute-done((bf16[128,2048]{1,0:T(8,128)(2,1)S(1)}, bf16[128,2048]{1,0:T(8,128)(2,1)S(1)}, u32[]{:S(2)}, u32[]{:S(2)}) %collective-permute-start) | collective-permute-done | bytes 524320 | tf_op jit(solution)/shard_map/ppermute | solution.py:31
  96.5 11.6 %collective-permute-done.1.refs_1_ = bf16[128,2048]{1,0:T(8,128)(2,1)S(1)} collective-permute-done((bf16[128,2048]{1,0:T(8,128)(2,1)S(1)}, bf16[128,2048]{1,0:T(8,128)(2,1)S(1)}, u32[]{:S(2)}, u32[]{:S(2)}) %collective-permute-start.1) | collective-permute-done | bytes 524320 | tf_op jit(solution)/shard_map/ppermute | solution.py:31
  108.1 0.0 collective-permute-done.2.refs_4_.refs_2_
  108.1 2.7 %shard_map.84 = (bf16[128,2048]{1,0:T(8,128)(2,1)S(1)}, bf16[128,2048]{1,0:T(8,128)(2,1)S(1)}, f32[128,2048]{1,0:T(8,128)S(1)}) custom-call(bf16[128,2048]{1,0:T(8,128)(2,1)S(1)} %collective-permute-done.refs_0_, bf16[128,2048]{1,0:T(8,128)(2,1)S(1)} %collective-permute-done.1.refs_1_, bf16[128,2048]{1,0:T(8,128)(2,1)S(1)} %all_gather.3.refs_2_, ...), custom_call_target="tpu_custom_call" | custom-call | flops 2415919104 | bytes 9961472 | tf_op jit(solution)/shard_map/pallas_call | solution.py:19
  110.8 5.0 %collective-permute-start.3 = (bf16[128,2048]{1,0:T(8,128)(2,1)S(1)}, bf16[128,2048]{1,0:T(8,128)(2,1)S(1)}, u32[]{:S(2)}, u32[]{:S(2)}) collective-permute-start(bf16[128,2048]{1,0:T(8,128)(2,1)S(1)} %get-tuple-element.10), channel_id=1, source_target_pairs={{0,2},{2,4},{4,6},{6,8},{8,10},{10,12},{12,14},{14,16},{16,18},{18... | collective-permute-start | bytes 1572872 | tf_op jit(solution)/shard_map/ppermute | solution.py:31
  115.8 1.9 %collective-permute-start.4 = (bf16[128,2048]{1,0:T(8,128)(2,1)S(1)}, bf16[128,2048]{1,0:T(8,128)(2,1)S(1)}, u32[]{:S(2)}, u32[]{:S(2)}) collective-permute-start(bf16[128,2048]{1,0:T(8,128)(2,1)S(1)} %get-tuple-element.11), channel_id=1, source_target_pairs={{0,30},{2,0},{4,2},{6,4},{8,6},{10,8},{12,10},{14,12},{16,14},{18,... | collective-permute-start | bytes 1572872 | tf_op jit(solution)/shard_map/ppermute | solution.py:31
  117.7 0.0 collective-permute-done.5.refs_0_
  117.7 1.5 shard_map.85
  119.1 8.4 %collective-permute-start.6 = (bf16[64,2048]{1,0:T(8,128)(2,1)S(1)}, bf16[64,2048]{1,0:T(8,128)(2,1)S(1)}, u32[]{:S(2)}, u32[]{:S(2)}) collective-permute-start(bf16[64,2048]{1,0:T(8,128)(2,1)S(1)} %get-tuple-element.12), channel_id=1, source_target_pairs={{0,4},{2,6},{4,8},{6,10},{8,12},{10,14},{12,16},{14,18},{16,20},{1... | collective-permute-start | bytes 786440 | tf_op jit(solution)/shard_map/ppermute | solution.py:31
  127.6 1.9 %collective-permute-start.7 = (bf16[64,2048]{1,0:T(8,128)(2,1)S(1)}, bf16[64,2048]{1,0:T(8,128)(2,1)S(1)}, u32[]{:S(2)}, u32[]{:S(2)}) collective-permute-start(bf16[64,2048]{1,0:T(8,128)(2,1)S(1)} %get-tuple-element.13), channel_id=1, source_target_pairs={{0,28},{2,30},{4,0},{6,2},{8,4},{10,6},{12,8},{14,10},{16,12},{18,... | collective-permute-start | bytes 786440 | tf_op jit(solution)/shard_map/ppermute | solution.py:31
  129.5 0.8 collective-permute-done.3.refs_1_.next_ref
  130.2 10.2 %collective-permute-done.4.refs_2_.prev_ref = bf16[128,2048]{1,0:T(8,128)(2,1)S(1)} collective-permute-done((bf16[128,2048]{1,0:T(8,128)(2,1)S(1)}, bf16[128,2048]{1,0:T(8,128)(2,1)S(1)}, u32[]{:S(2)}, u32[]{:S(2)}) %collective-permute-start.4) | collective-permute-done | bytes 524320 | tf_op jit(solution)/shard_map/ppermute | solution.py:31
  140.5 3.4 %collective-permute-start.9 = (bf16[32,2048]{1,0:T(8,128)(2,1)S(1)}, bf16[32,2048]{1,0:T(8,128)(2,1)S(1)}, u32[]{:S(2)}, u32[]{:S(2)}) collective-permute-start(bf16[32,2048]{1,0:T(8,128)(2,1)S(1)} %shard_map.87), channel_id=1, source_target_pairs={{0,8},{2,10},{4,12},{6,14},{8,16},{10,18},{12,20},{14,22},{16,24},... | collective-permute-start | bytes 393224 | tf_op jit(solution)/shard_map/ppermute | solution.py:37
  143.9 0.0 collective-permute-done.6.refs_3_.next2_ref
  143.9 0.0 collective-permute-done.7.refs_4_.prev2_ref
  143.9 0.1 shard_map.86
  144.0 9.7 %collective-permute-start.8 = (bf16[32,2048]{1,0:T(8,128)(2,1)S(1)}, bf16[32,2048]{1,0:T(8,128)(2,1)S(1)}, u32[]{:S(2)}, u32[]{:S(2)}) collective-permute-start(bf16[32,2048]{1,0:T(8,128)(2,1)S(1)} %shard_map.86), channel_id=1, source_target_pairs={{0,24},{2,26},{4,28},{6,30},{8,0},{10,2},{12,4},{14,6},{16,8},{18,... | collective-permute-start | bytes 393224 | tf_op jit(solution)/shard_map/ppermute | solution.py:37
  153.7 2.8 %collective-permute-done.9.refs_5_ = bf16[32,2048]{1,0:T(8,128)(2,1)S(1)} collective-permute-done((bf16[32,2048]{1,0:T(8,128)(2,1)S(1)}, bf16[32,2048]{1,0:T(8,128)(2,1)S(1)}, u32[]{:S(2)}, u32[]{:S(2)}) %collective-permute-start.9) | collective-permute-done | bytes 131104 | tf_op jit(solution)/shard_map/ppermute | solution.py:37
  156.5 0.1 shard_map.88
  156.6 3.8 %collective-permute-start.10 = (bf16[32,2048]{1,0:T(8,128)(2,1)S(1)}, bf16[32,2048]{1,0:T(8,128)(2,1)S(1)}, u32[]{:S(2)}, u32[]{:S(2)}) collective-permute-start(bf16[32,2048]{1,0:T(8,128)(2,1)S(1)} %shard_map.88), channel_id=1, source_target_pairs={{0,8},{2,10},{4,12},{6,14},{8,16},{10,18},{12,20},{14,22},{16,24},... | collective-permute-start | bytes 393224 | tf_op jit(solution)/shard_map/ppermute | solution.py:37
  160.4 1.8 %fusion = (bf16[16,1,128,256]{3,2,1,0:T(8,128)(2,1)}, bf16[16,1,128,256]{3,2,1,0:T(8,128)(2,1)}, bf16[16,1,128,256]{3,2,1,0:T(8,128)(2,1)}) fusion(bf16[16,3,128,256]{3,2,1,0:T(8,128)(2,1)S(1)} %all_to_all.5.refs_3_.refs_1_), kind=kLoop, calls=%fused_computation | loop fusion | bytes 6291456 | tf_op jit(solution)/shard_map/slice | solution.py:196
  162.2 0.1 collective-permute-done.8.above_ref
  162.3 5.6 %collective-permute-done.10.below_ref = bf16[32,2048]{1,0:T(8,128)(2,1)S(1)} collective-permute-done((bf16[32,2048]{1,0:T(8,128)(2,1)S(1)}, bf16[32,2048]{1,0:T(8,128)(2,1)S(1)}, u32[]{:S(2)}, u32[]{:S(2)}) %collective-permute-start.10) | collective-permute-done | bytes 131104 | tf_op jit(solution)/shard_map/ppermute | solution.py:37
  167.8 0.8 shard_map.89
  (1 shorter events, 0.0 us)
Async XLA Ops:
  3.5 48.7 %copy-start = (bf16[32,2048]{1,0:T(8,128)(2,1)S(1)}, bf16[32,2048]{1,0:T(8,128)(2,1)}, u32[]{:S(2)}) copy-start(bf16[32,2048]{1,0:T(8,128)(2,1)} %tokens_ref.1) | copy-start | bytes 393220
  50.3 57.8 %collective-permute-start.2 = (bf16[16,3,128,256]{3,2,1,0:T(8,128)(2,1)S(1)}, bf16[16,3,128,256]{3,2,1,0:T(8,128)(2,1)S(1)}, u32[]{:S(2)}, u32[]{:S(2)}) collective-permute-start(bf16[16,3,128,256]{3,2,1,0:T(8,128)(2,1)S(1)} %all_to_all.5.refs_3_.refs_1_), channel_id=1, source_target_pairs={{0,1},{1,0},{2,3},{3,2},{4,5},{5,4},{6,7},{7,6},{8,9},{9,8},{10,11... | collective-permute-start | bytes 9437192 | tf_op jit(solution)/shard_map/ppermute | solution.py:171
  84.3 12.3 %collective-permute-start = (bf16[128,2048]{1,0:T(8,128)(2,1)S(1)}, bf16[128,2048]{1,0:T(8,128)(2,1)S(1)}, u32[]{:S(2)}, u32[]{:S(2)}) collective-permute-start(bf16[128,2048]{1,0:T(8,128)(2,1)S(1)} %all_gather.3.refs_2_), channel_id=1, source_target_pairs={{0,30},{2,0},{4,2},{6,4},{8,6},{10,8},{12,10},{14,12},{16,14},{18,... | collective-permute-start | bytes 1572872 | tf_op jit(solution)/shard_map/ppermute | solution.py:31
  87.7 20.4 %collective-permute-start.1 = (bf16[128,2048]{1,0:T(8,128)(2,1)S(1)}, bf16[128,2048]{1,0:T(8,128)(2,1)S(1)}, u32[]{:S(2)}, u32[]{:S(2)}) collective-permute-start(bf16[128,2048]{1,0:T(8,128)(2,1)S(1)} %all_gather.3.refs_2_), channel_id=1, source_target_pairs={{0,2},{2,4},{4,6},{6,8},{8,10},{10,12},{12,14},{14,16},{16,18},{18... | collective-permute-start | bytes 1572872 | tf_op jit(solution)/shard_map/ppermute | solution.py:31
  90.2 27.5 %collective-permute-start.5 = (bf16[128,2048]{1,0:T(8,128)(2,1)S(1)}, bf16[128,2048]{1,0:T(8,128)(2,1)S(1)}, u32[]{:S(2)}, u32[]{:S(2)}) collective-permute-start(bf16[128,2048]{1,0:T(8,128)(2,1)S(1)} %all_gather.3.refs_2_), channel_id=1, source_target_pairs={{0,28},{2,30},{4,0},{6,2},{8,4},{10,6},{12,8},{14,10},{16,12},{18,... | collective-permute-start | bytes 1572872 | tf_op jit(solution)/shard_map/ppermute | solution.py:37
  110.8 19.5 %collective-permute-start.3 = (bf16[128,2048]{1,0:T(8,128)(2,1)S(1)}, bf16[128,2048]{1,0:T(8,128)(2,1)S(1)}, u32[]{:S(2)}, u32[]{:S(2)}) collective-permute-start(bf16[128,2048]{1,0:T(8,128)(2,1)S(1)} %get-tuple-element.10), channel_id=1, source_target_pairs={{0,2},{2,4},{4,6},{6,8},{8,10},{10,12},{12,14},{14,16},{16,18},{18... | collective-permute-start | bytes 1572872 | tf_op jit(solution)/shard_map/ppermute | solution.py:31
  115.8 24.7 %collective-permute-start.4 = (bf16[128,2048]{1,0:T(8,128)(2,1)S(1)}, bf16[128,2048]{1,0:T(8,128)(2,1)S(1)}, u32[]{:S(2)}, u32[]{:S(2)}) collective-permute-start(bf16[128,2048]{1,0:T(8,128)(2,1)S(1)} %get-tuple-element.11), channel_id=1, source_target_pairs={{0,30},{2,0},{4,2},{6,4},{8,6},{10,8},{12,10},{14,12},{16,14},{18,... | collective-permute-start | bytes 1572872 | tf_op jit(solution)/shard_map/ppermute | solution.py:31
  119.1 24.8 %collective-permute-start.6 = (bf16[64,2048]{1,0:T(8,128)(2,1)S(1)}, bf16[64,2048]{1,0:T(8,128)(2,1)S(1)}, u32[]{:S(2)}, u32[]{:S(2)}) collective-permute-start(bf16[64,2048]{1,0:T(8,128)(2,1)S(1)} %get-tuple-element.12), channel_id=1, source_target_pairs={{0,4},{2,6},{4,8},{6,10},{8,12},{10,14},{12,16},{14,18},{16,20},{1... | collective-permute-start | bytes 786440 | tf_op jit(solution)/shard_map/ppermute | solution.py:31
  127.6 16.4 %collective-permute-start.7 = (bf16[64,2048]{1,0:T(8,128)(2,1)S(1)}, bf16[64,2048]{1,0:T(8,128)(2,1)S(1)}, u32[]{:S(2)}, u32[]{:S(2)}) collective-permute-start(bf16[64,2048]{1,0:T(8,128)(2,1)S(1)} %get-tuple-element.13), channel_id=1, source_target_pairs={{0,28},{2,30},{4,0},{6,2},{8,4},{10,6},{12,8},{14,10},{16,12},{18,... | collective-permute-start | bytes 786440 | tf_op jit(solution)/shard_map/ppermute | solution.py:31
  140.5 16.0 %collective-permute-start.9 = (bf16[32,2048]{1,0:T(8,128)(2,1)S(1)}, bf16[32,2048]{1,0:T(8,128)(2,1)S(1)}, u32[]{:S(2)}, u32[]{:S(2)}) collective-permute-start(bf16[32,2048]{1,0:T(8,128)(2,1)S(1)} %shard_map.87), channel_id=1, source_target_pairs={{0,8},{2,10},{4,12},{6,14},{8,16},{10,18},{12,20},{14,22},{16,24},... | collective-permute-start | bytes 393224 | tf_op jit(solution)/shard_map/ppermute | solution.py:37
  144.0 18.2 %collective-permute-start.8 = (bf16[32,2048]{1,0:T(8,128)(2,1)S(1)}, bf16[32,2048]{1,0:T(8,128)(2,1)S(1)}, u32[]{:S(2)}, u32[]{:S(2)}) collective-permute-start(bf16[32,2048]{1,0:T(8,128)(2,1)S(1)} %shard_map.86), channel_id=1, source_target_pairs={{0,24},{2,26},{4,28},{6,30},{8,0},{10,2},{12,4},{14,6},{16,8},{18,... | collective-permute-start | bytes 393224 | tf_op jit(solution)/shard_map/ppermute | solution.py:37
  156.6 11.2 %collective-permute-start.10 = (bf16[32,2048]{1,0:T(8,128)(2,1)S(1)}, bf16[32,2048]{1,0:T(8,128)(2,1)S(1)}, u32[]{:S(2)}, u32[]{:S(2)}) collective-permute-start(bf16[32,2048]{1,0:T(8,128)(2,1)S(1)} %shard_map.88), channel_id=1, source_target_pairs={{0,8},{2,10},{4,12},{6,14},{8,16},{10,18},{12,20},{14,22},{16,24},... | collective-permute-start | bytes 393224 | tf_op jit(solution)/shard_map/ppermute | solution.py:37

commit v13 on v12

--- a/solution.py
+++ b/solution.py
@@ -117,12 +117,12 @@
         at += ref.shape[0]
 
 
-def partial_sums(parts, orders, weights, counts, dtypes):
+def partial_sums(parts, orders, weights, counts, dtype):
     units = 2 * weights[0].shape[-1]
     count, width = sum(counts), parts[0].shape[1]
     return local(
         lambda *refs: sums_kernel(orders, *refs),
-        tuple(jax.ShapeDtypeStruct((k, width), dtype) for k, dtype in zip(counts, dtypes)),
+        tuple(jax.ShapeDtypeStruct((k, width), dtype) for k in counts),
         *parts,
         *weights,
         flops=6 * count * width * units,
@@ -174,15 +174,14 @@
     def around(by):
         return lambda ref: blocks_of(ref, by, (0, 2, 1, 3))
 
-    narrow = jnp.bfloat16
-    for_next, for_prev, own = partial_sums(
-        (from_next, from_prev, held), (around(1), around(-1), around(0)), weights, (4 * rows,) * 3, (narrow, narrow, jnp.float32)
-    )
+    (for_next,) = partial_sums((from_next,), (around(1),), weights, (4 * rows,), jnp.bfloat16)
     to_next = move(for_next, 1)
+    (for_prev,) = partial_sums((from_prev,), (around(-1),), weights, (4 * rows,), jnp.bfloat16)
     to_prev = move(for_prev, -1)
-    for_next2, for_prev2 = partial_sums((from_twos,), (blocks_of_twos,), weights, (2 * rows,) * 2, (narrow, narrow))
+    for_next2, for_prev2 = partial_sums((from_twos,), (blocks_of_twos,), weights, (2 * rows, 2 * rows), jnp.bfloat16)
+    to_next2 = move(for_next2, 2)
     to_prev2 = move(for_prev2, -2)
-    to_next2 = move(for_next2, 2)
+    (own,) = partial_sums((held,), (around(0),), weights, (4 * rows,), jnp.float32)
 
     block = jax.ShapeDtypeStruct((rows, width), jnp.bfloat16)
     (sum_far,) = local(fold_far_kernel, (block,), own, to_next, to_prev)

time: 169 us -> 163 us (0.964)
  the two profiles are of different devices: /device:TPU:64 before, /device:TPU:6 now
where the time goes in v13:
time: 163 us; the launch traced here: 161 us
  blocking collectives  78 us (48%)
  starting transfers between devices  39 us (24%)
  waiting for transfers between devices  31.5 us (19%)
  Pallas kernels  9.69 us (6%)
  local copies, waits for them, and re-layouts  1.76 us (1%)
    all_to_all x1, blocking collectives, step(): lax.all_to_all(copies, 'fs', split_axis=0, concat_axis=0, tiled=True)  44.6 us
    all_gather x1, blocking collectives, step(): held = lax.all_gather(tokens, 'zh', axis=0, tiled=True)  33.4 us
    ppermute x6, waiting for transfers between devices, move(): lax.ppermute(array, Z, [(i, (i + by) % planes) for i in range(planes)])  19.8 us
    ppermute x6, starting transfers between devices, move(): lax.ppermute(array, Z, [(i, (i + by) % planes) for i in range(planes)])  18.8 us
    ppermute x4, starting transfers between devices, move_by_core(): return lax.ppermute(array, TP, pairs)  18.2 us
    ppermute x4, waiting for transfers between devices, move_by_core(): return lax.ppermute(array, TP, pairs)  11.8 us
    pallas_call x8, Pallas kernels, local(): pl.pallas_call(kernel, out_shape=outs, in_specs=[VMEM] * len(args), out_s...  6.83 us
  transfers between devices with their start and end apart: 11, of which 5 were waited for; matrix products, arithmetic and copies ran while one was open for 1% of the time, Pallas kernels for 4%

profile of v13, /device:TPU:6, one launch (start us, length us, event | category | flops | bytes accessed | tf_op | source)
XLA Modules:
  0.0 160.8 jit_solution(11826564908392524391)
XLA Ops:
  0.6 2.9 %prepare.1 = bf16[16,3,128,256]{3,2,1,0:T(8,128)(2,1)} custom-call(f32[1,128]{1,0:T(1,128)} %bitcast.7, f32[128,256]{1,0:T(8,128)} %gate_hbm.1, f32[128,256]{1,0:T(8,128)} %up_hbm.1, f32[128,256]{1,0:T(8,128)} %down_hbm.1), custom_call_target="tpu_custom_call" | custom-call | flops 1000000 | bytes 4000000 | tf_op jit(solution)/shard_map/prepare/pallas_call | solution.py:65
  3.5 0.0 copy-start
  3.5 44.6 %all_to_all.5.refs_1_ = bf16[16,3,128,256]{3,2,1,0:T(8,128)(2,1)S(1)} all-to-all(bf16[16,3,128,256]{3,2,1,0:T(8,128)(2,1)} %prepare.1), channel_id=1, replica_groups=mesh['fs'=16,'zh'=4,'zl'=4,'c'=2] {'fs'}, dimensions={0} | all-to-all | bytes 6291456 | tf_op jit(solution)/shard_map/all_to_all | solution.py:164
  48.1 1.9 %collective-permute-start = (bf16[16,3,128,256]{3,2,1,0:T(8,128)(2,1)S(1)}, bf16[16,3,128,256]{3,2,1,0:T(8,128)(2,1)S(1)}, u32[]{:S(2)}, u32[]{:S(2)}) collective-permute-start(bf16[16,3,128,256]{3,2,1,0:T(8,128)(2,1)S(1)} %all_to_all.5.refs_1_), channel_id=1, source_target_pairs={{0,1},{1,0},{2,3},{3,2},{4,5},{5,4},{6,7},{7,6},{8,9},{9,8},{10,11... | collective-permute-start | bytes 9437192 | tf_op jit(solution)/shard_map/ppermute | solution.py:171
  50.0 0.0 copy-done
  50.0 33.4 %all_gather.3.refs_0_ = bf16[128,2048]{1,0:T(8,128)(2,1)S(1)} all-gather(bf16[32,2048]{1,0:T(8,128)(2,1)S(1)} %copy-done), channel_id=1, replica_groups=mesh['fs'=16,'zh'=4,'zl'=4,'c'=2] {'zh'}, dimensions={0}, use_global_device_ids=true | all-gather | bytes 655360 | tf_op jit(solution)/shard_map/all_gather | solution.py:165
  83.4 5.1 %collective-permute-start.1 = (bf16[128,2048]{1,0:T(8,128)(2,1)S(1)}, bf16[128,2048]{1,0:T(8,128)(2,1)S(1)}, u32[]{:S(2)}, u32[]{:S(2)}) collective-permute-start(bf16[128,2048]{1,0:T(8,128)(2,1)S(1)} %all_gather.3.refs_0_), channel_id=1, source_target_pairs={{0,30},{2,0},{4,2},{6,4},{8,6},{10,8},{12,10},{14,12},{16,14},{18,... | collective-permute-start | bytes 1572872 | tf_op jit(solution)/shard_map/ppermute | solution.py:31
  88.6 1.9 %collective-permute-start.3 = (bf16[128,2048]{1,0:T(8,128)(2,1)S(1)}, bf16[128,2048]{1,0:T(8,128)(2,1)S(1)}, u32[]{:S(2)}, u32[]{:S(2)}) collective-permute-start(bf16[128,2048]{1,0:T(8,128)(2,1)S(1)} %all_gather.3.refs_0_), channel_id=1, source_target_pairs={{0,2},{2,4},{4,6},{6,8},{8,10},{10,12},{12,14},{14,16},{16,18},{18... | collective-permute-start | bytes 1572872 | tf_op jit(solution)/shard_map/ppermute | solution.py:31
  90.5 3.5 %collective-permute-start.5 = (bf16[128,2048]{1,0:T(8,128)(2,1)S(1)}, bf16[128,2048]{1,0:T(8,128)(2,1)S(1)}, u32[]{:S(2)}, u32[]{:S(2)}) collective-permute-start(bf16[128,2048]{1,0:T(8,128)(2,1)S(1)} %all_gather.3.refs_0_), channel_id=1, source_target_pairs={{0,28},{2,30},{4,0},{6,2},{8,4},{10,6},{12,8},{14,10},{16,12},{18,... | collective-permute-start | bytes 1572872 | tf_op jit(solution)/shard_map/ppermute | solution.py:37
  94.0 5.5 %collective-permute-done.1.refs_0_ = bf16[128,2048]{1,0:T(8,128)(2,1)S(1)} collective-permute-done((bf16[128,2048]{1,0:T(8,128)(2,1)S(1)}, bf16[128,2048]{1,0:T(8,128)(2,1)S(1)}, u32[]{:S(2)}, u32[]{:S(2)}) %collective-permute-start.1) | collective-permute-done | bytes 524320 | tf_op jit(solution)/shard_map/ppermute | solution.py:31
  99.5 0.0 collective-permute-done.refs_2_
  99.5 1.4 shard_map.85
  100.9 1.9 %collective-permute-start.2 = (bf16[128,2048]{1,0:T(8,128)(2,1)S(1)}, bf16[128,2048]{1,0:T(8,128)(2,1)S(1)}, u32[]{:S(2)}, u32[]{:S(2)}) collective-permute-start(bf16[128,2048]{1,0:T(8,128)(2,1)S(1)} %shard_map.85), channel_id=1, source_target_pairs={{0,2},{2,4},{4,6},{6,8},{8,10},{10,12},{12,14},{14,16},{16,18},{18... | collective-permute-start | bytes 1572872 | tf_op jit(solution)/shard_map/ppermute | solution.py:31
  102.9 7.4 %collective-permute-done.3.refs_0_ = bf16[128,2048]{1,0:T(8,128)(2,1)S(1)} collective-permute-done((bf16[128,2048]{1,0:T(8,128)(2,1)S(1)}, bf16[128,2048]{1,0:T(8,128)(2,1)S(1)}, u32[]{:S(2)}, u32[]{:S(2)}) %collective-permute-start.3) | collective-permute-done | bytes 524320 | tf_op jit(solution)/shard_map/ppermute | solution.py:31
  110.3 1.5 shard_map.86
  111.7 1.9 %collective-permute-start.4 = (bf16[128,2048]{1,0:T(8,128)(2,1)S(1)}, bf16[128,2048]{1,0:T(8,128)(2,1)S(1)}, u32[]{:S(2)}, u32[]{:S(2)}) collective-permute-start(bf16[128,2048]{1,0:T(8,128)(2,1)S(1)} %shard_map.86), channel_id=1, source_target_pairs={{0,30},{2,0},{4,2},{6,4},{8,6},{10,8},{12,10},{14,12},{16,14},{18,... | collective-permute-start | bytes 1572872 | tf_op jit(solution)/shard_map/ppermute | solution.py:31
  113.6 0.0 collective-permute-done.5.refs_0_
  113.7 1.5 shard_map.87
  115.1 1.9 %collective-permute-start.6 = (bf16[64,2048]{1,0:T(8,128)(2,1)S(1)}, bf16[64,2048]{1,0:T(8,128)(2,1)S(1)}, u32[]{:S(2)}, u32[]{:S(2)}) collective-permute-start(bf16[64,2048]{1,0:T(8,128)(2,1)S(1)} %get-tuple-element.6), channel_id=1, source_target_pairs={{0,4},{2,6},{4,8},{6,10},{8,12},{10,14},{12,16},{14,18},{16,20},{1... | collective-permute-start | bytes 786440 | tf_op jit(solution)/shard_map/ppermute | solution.py:31
  117.0 6.0 %collective-permute-start.7 = (bf16[64,2048]{1,0:T(8,128)(2,1)S(1)}, bf16[64,2048]{1,0:T(8,128)(2,1)S(1)}, u32[]{:S(2)}, u32[]{:S(2)}) collective-permute-start(bf16[64,2048]{1,0:T(8,128)(2,1)S(1)} %get-tuple-element.7), channel_id=1, source_target_pairs={{0,28},{2,30},{4,0},{6,2},{8,4},{10,6},{12,8},{14,10},{16,12},{18,... | collective-permute-start | bytes 786440 | tf_op jit(solution)/shard_map/ppermute | solution.py:31
  123.1 1.5 shard_map.84.refs_0_.own_ref
  124.5 0.0 collective-permute-done.2.refs_1_.next_ref
  124.6 0.0 collective-permute-done.4.refs_2_.prev_ref
  124.6 6.5 %collective-permute-start.9 = (bf16[32,2048]{1,0:T(8,128)(2,1)S(1)}, bf16[32,2048]{1,0:T(8,128)(2,1)S(1)}, u32[]{:S(2)}, u32[]{:S(2)}) collective-permute-start(bf16[32,2048]{1,0:T(8,128)(2,1)S(1)} %shard_map.89), channel_id=1, source_target_pairs={{0,8},{2,10},{4,12},{6,14},{8,16},{10,18},{12,20},{14,22},{16,24},... | collective-permute-start | bytes 393224 | tf_op jit(solution)/shard_map/ppermute | solution.py:37
  131.1 0.0 collective-permute-done.6.refs_3_.next2_ref
  131.1 6.9 %collective-permute-done.7.refs_4_.prev2_ref = bf16[64,2048]{1,0:T(8,128)(2,1)S(1)} collective-permute-done((bf16[64,2048]{1,0:T(8,128)(2,1)S(1)}, bf16[64,2048]{1,0:T(8,128)(2,1)S(1)}, u32[]{:S(2)}, u32[]{:S(2)}) %collective-permute-start.7) | collective-permute-done | bytes 262176 | tf_op jit(solution)/shard_map/ppermute | solution.py:31
  138.0 0.1 shard_map.88
  138.1 1.9 %collective-permute-start.8 = (bf16[32,2048]{1,0:T(8,128)(2,1)S(1)}, bf16[32,2048]{1,0:T(8,128)(2,1)S(1)}, u32[]{:S(2)}, u32[]{:S(2)}) collective-permute-start(bf16[32,2048]{1,0:T(8,128)(2,1)S(1)} %shard_map.88), channel_id=1, source_target_pairs={{0,24},{2,26},{4,28},{6,30},{8,0},{10,2},{12,4},{14,6},{16,8},{18,... | collective-permute-start | bytes 393224 | tf_op jit(solution)/shard_map/ppermute | solution.py:37
  140.0 3.1 %collective-permute-done.9.refs_5_ = bf16[32,2048]{1,0:T(8,128)(2,1)S(1)} collective-permute-done((bf16[32,2048]{1,0:T(8,128)(2,1)S(1)}, bf16[32,2048]{1,0:T(8,128)(2,1)S(1)}, u32[]{:S(2)}, u32[]{:S(2)}) %collective-permute-start.9) | collective-permute-done | bytes 131104 | tf_op jit(solution)/shard_map/ppermute | solution.py:37
  143.1 0.1 shard_map.90
  143.2 6.3 %collective-permute-start.10 = (bf16[32,2048]{1,0:T(8,128)(2,1)S(1)}, bf16[32,2048]{1,0:T(8,128)(2,1)S(1)}, u32[]{:S(2)}, u32[]{:S(2)}) collective-permute-start(bf16[32,2048]{1,0:T(8,128)(2,1)S(1)} %shard_map.90), channel_id=1, source_target_pairs={{0,8},{2,10},{4,12},{6,14},{8,16},{10,18},{12,20},{14,22},{16,24},... | collective-permute-start | bytes 393224 | tf_op jit(solution)/shard_map/ppermute | solution.py:37
  149.5 1.8 %fusion = (bf16[16,1,128,256]{3,2,1,0:T(8,128)(2,1)}, bf16[16,1,128,256]{3,2,1,0:T(8,128)(2,1)}, bf16[16,1,128,256]{3,2,1,0:T(8,128)(2,1)}) fusion(bf16[16,3,128,256]{3,2,1,0:T(8,128)(2,1)S(1)} %all_to_all.5.refs_1_), kind=kLoop, calls=%fused_computation | loop fusion | bytes 6291456 | tf_op jit(solution)/shard_map/slice | solution.py:195
  151.3 0.0 collective-permute-done.8.above_ref
  151.3 8.7 %collective-permute-done.10.below_ref = bf16[32,2048]{1,0:T(8,128)(2,1)S(1)} collective-permute-done((bf16[32,2048]{1,0:T(8,128)(2,1)S(1)}, bf16[32,2048]{1,0:T(8,128)(2,1)S(1)}, u32[]{:S(2)}, u32[]{:S(2)}) %collective-permute-start.10) | collective-permute-done | bytes 131104 | tf_op jit(solution)/shard_map/ppermute | solution.py:37
  160.0 0.8 shard_map.91
  (1 shorter events, 0.0 us)
Async XLA Ops:
  3.5 46.5 %copy-start = (bf16[32,2048]{1,0:T(8,128)(2,1)S(1)}, bf16[32,2048]{1,0:T(8,128)(2,1)}, u32[]{:S(2)}) copy-start(bf16[32,2048]{1,0:T(8,128)(2,1)} %tokens_ref.1) | copy-start | bytes 393220
  48.1 51.4 %collective-permute-start = (bf16[16,3,128,256]{3,2,1,0:T(8,128)(2,1)S(1)}, bf16[16,3,128,256]{3,2,1,0:T(8,128)(2,1)S(1)}, u32[]{:S(2)}, u32[]{:S(2)}) collective-permute-start(bf16[16,3,128,256]{3,2,1,0:T(8,128)(2,1)S(1)} %all_to_all.5.refs_1_), channel_id=1, source_target_pairs={{0,1},{1,0},{2,3},{3,2},{4,5},{5,4},{6,7},{7,6},{8,9},{9,8},{10,11... | collective-permute-start | bytes 9437192 | tf_op jit(solution)/shard_map/ppermute | solution.py:171
  83.4 16.1 %collective-permute-start.1 = (bf16[128,2048]{1,0:T(8,128)(2,1)S(1)}, bf16[128,2048]{1,0:T(8,128)(2,1)S(1)}, u32[]{:S(2)}, u32[]{:S(2)}) collective-permute-start(bf16[128,2048]{1,0:T(8,128)(2,1)S(1)} %all_gather.3.refs_0_), channel_id=1, source_target_pairs={{0,30},{2,0},{4,2},{6,4},{8,6},{10,8},{12,10},{14,12},{16,14},{18,... | collective-permute-start | bytes 1572872 | tf_op jit(solution)/shard_map/ppermute | solution.py:31
  88.6 21.7 %collective-permute-start.3 = (bf16[128,2048]{1,0:T(8,128)(2,1)S(1)}, bf16[128,2048]{1,0:T(8,128)(2,1)S(1)}, u32[]{:S(2)}, u32[]{:S(2)}) collective-permute-start(bf16[128,2048]{1,0:T(8,128)(2,1)S(1)} %all_gather.3.refs_0_), channel_id=1, source_target_pairs={{0,2},{2,4},{4,6},{6,8},{8,10},{10,12},{12,14},{14,16},{16,18},{18... | collective-permute-start | bytes 1572872 | tf_op jit(solution)/shard_map/ppermute | solution.py:31
  90.5 23.2 %collective-permute-start.5 = (bf16[128,2048]{1,0:T(8,128)(2,1)S(1)}, bf16[128,2048]{1,0:T(8,128)(2,1)S(1)}, u32[]{:S(2)}, u32[]{:S(2)}) collective-permute-start(bf16[128,2048]{1,0:T(8,128)(2,1)S(1)} %all_gather.3.refs_0_), channel_id=1, source_target_pairs={{0,28},{2,30},{4,0},{6,2},{8,4},{10,6},{12,8},{14,10},{16,12},{18,... | collective-permute-start | bytes 1572872 | tf_op jit(solution)/shard_map/ppermute | solution.py:37
  100.9 23.6 %collective-permute-start.2 = (bf16[128,2048]{1,0:T(8,128)(2,1)S(1)}, bf16[128,2048]{1,0:T(8,128)(2,1)S(1)}, u32[]{:S(2)}, u32[]{:S(2)}) collective-permute-start(bf16[128,2048]{1,0:T(8,128)(2,1)S(1)} %shard_map.85), channel_id=1, source_target_pairs={{0,2},{2,4},{4,6},{6,8},{8,10},{10,12},{12,14},{14,16},{16,18},{18... | collective-permute-start | bytes 1572872 | tf_op jit(solution)/shard_map/ppermute | solution.py:31
  111.7 12.8 %collective-permute-start.4 = (bf16[128,2048]{1,0:T(8,128)(2,1)S(1)}, bf16[128,2048]{1,0:T(8,128)(2,1)S(1)}, u32[]{:S(2)}, u32[]{:S(2)}) collective-permute-start(bf16[128,2048]{1,0:T(8,128)(2,1)S(1)} %shard_map.86), channel_id=1, source_target_pairs={{0,30},{2,0},{4,2},{6,4},{8,6},{10,8},{12,10},{14,12},{16,14},{18,... | collective-permute-start | bytes 1572872 | tf_op jit(solution)/shard_map/ppermute | solution.py:31
  115.1 16.0 %collective-permute-start.6 = (bf16[64,2048]{1,0:T(8,128)(2,1)S(1)}, bf16[64,2048]{1,0:T(8,128)(2,1)S(1)}, u32[]{:S(2)}, u32[]{:S(2)}) collective-permute-start(bf16[64,2048]{1,0:T(8,128)(2,1)S(1)} %get-tuple-element.6), channel_id=1, source_target_pairs={{0,4},{2,6},{4,8},{6,10},{8,12},{10,14},{12,16},{14,18},{16,20},{1... | collective-permute-start | bytes 786440 | tf_op jit(solution)/shard_map/ppermute | solution.py:31
  117.0 21.0 %collective-permute-start.7 = (bf16[64,2048]{1,0:T(8,128)(2,1)S(1)}, bf16[64,2048]{1,0:T(8,128)(2,1)S(1)}, u32[]{:S(2)}, u32[]{:S(2)}) collective-permute-start(bf16[64,2048]{1,0:T(8,128)(2,1)S(1)} %get-tuple-element.7), channel_id=1, source_target_pairs={{0,28},{2,30},{4,0},{6,2},{8,4},{10,6},{12,8},{14,10},{16,12},{18,... | collective-permute-start | bytes 786440 | tf_op jit(solution)/shard_map/ppermute | solution.py:31
  124.6 18.5 %collective-permute-start.9 = (bf16[32,2048]{1,0:T(8,128)(2,1)S(1)}, bf16[32,2048]{1,0:T(8,128)(2,1)S(1)}, u32[]{:S(2)}, u32[]{:S(2)}) collective-permute-start(bf16[32,2048]{1,0:T(8,128)(2,1)S(1)} %shard_map.89), channel_id=1, source_target_pairs={{0,8},{2,10},{4,12},{6,14},{8,16},{10,18},{12,20},{14,22},{16,24},... | collective-permute-start | bytes 393224 | tf_op jit(solution)/shard_map/ppermute | solution.py:37
  138.1 13.1 %collective-permute-start.8 = (bf16[32,2048]{1,0:T(8,128)(2,1)S(1)}, bf16[32,2048]{1,0:T(8,128)(2,1)S(1)}, u32[]{:S(2)}, u32[]{:S(2)}) collective-permute-start(bf16[32,2048]{1,0:T(8,128)(2,1)S(1)} %shard_map.88), channel_id=1, source_target_pairs={{0,24},{2,26},{4,28},{6,30},{8,0},{10,2},{12,4},{14,6},{16,8},{18,... | collective-permute-start | bytes 393224 | tf_op jit(solution)/shard_map/ppermute | solution.py:37
  143.2 16.7 %collective-permute-start.10 = (bf16[32,2048]{1,0:T(8,128)(2,1)S(1)}, bf16[32,2048]{1,0:T(8,128)(2,1)S(1)}, u32[]{:S(2)}, u32[]{:S(2)}) collective-permute-start(bf16[32,2048]{1,0:T(8,128)(2,1)S(1)} %shard_map.90), channel_id=1, source_target_pairs={{0,8},{2,10},{4,12},{6,14},{8,16},{10,18},{12,20},{14,22},{16,24},... | collective-permute-start | bytes 393224 | tf_op jit(solution)/shard_map/ppermute | solution.py:37
